TPU v7x, 512 devices: a whole 4x4x16 slice. The times are simulated.
512 devices in a mesh: ep: 128 (over z, x, core), tp: 4 (over y).
Axes of the slice: x: 4, y: 4, z: 16, core: 2. Of those that a mesh axis runs over, the one named last changes fastest.
Arguments:
- tokens: bfloat16 [1664, 1024], P('ep'), may hold values from -60 to 60
- attn_gain: float32 [1024], replicated, may hold values from 0.1 to 1.9
- query_weight: bfloat16 [1024, 512], P(None, 'tp'), may hold values from -0.1875 to 0.1875
- key_weight: bfloat16 [1024, 256], P(None, 'tp'), may hold values from -0.1875 to 0.1875
- value_weight: bfloat16 [1024, 256], P(None, 'tp'), may hold values from -0.1875 to 0.1875
- forget_weight: bfloat16 [1024, 8], P(None, 'tp'), may hold values from -0.5 to 0.5
- forget_bias: float32 [8], P('tp'), may hold values from -3 to 3
- out_weight: bfloat16 [512, 1024], P('tp'), may hold values from -0.75 to 0.75
- key_cache: bfloat16 [1664, 4, 64, 1024], P('ep', 'tp'), may hold values from -300 to 300
- value_cache: bfloat16 [1664, 4, 64, 1024], P('ep', 'tp'), may hold values from -12 to 12
- cum_forget: float32 [1664, 8, 1024], P('ep', 'tp'), may hold values from -131 to 0, as said below
- lengths: int32 [1664], P('ep'), may hold values from 256 to 1024
- ffn_gain: float32 [1024], replicated, may hold values from 0.1 to 1.9
- routes: int32 [1664, 2], P('ep'), may hold values from 0 to 31, all different within a row; in each aligned block of 13 rows (0 to 12, 13 to 25, ...) at most 2 rows name the same one
- route_weights: float32 [1664, 2], P('ep'), may hold values from 0.2 to 1
- gate_weight: bfloat16 [128, 1024, 512], P('ep', None, 'tp'), may hold values from -0.1875 to 0.1875
- up_weight: bfloat16 [128, 1024, 512], P('ep', None, 'tp'), may hold values from -0.1875 to 0.1875
- down_weight: bfloat16 [128, 512, 1024], P('ep', 'tp'), may hold values from -0.25 to 0.25
Outputs:
- layer_out: bfloat16 [1664, 1024], P('ep', 'tp')
Inputs may be any that keep to these rules, and one draw needn't show every extreme that they name: `routes`: the experts of a row differ; in each aligned block of 13 rows (the rows of one index of ep) no expert is named by more than 2 rows. `cum_forget`: for each sequence and head the entries do not increase along positions.
All inputs are finite; a program needn't handle non-finite values.
Results may differ from a plain program's by a relative error of at most 0.0085.
Values may be sent and summed in bfloat16 or wider, within the bound.
No kernel may reach another device: no remote copies, remote signals or barrier semaphores. Data moves between devices by JAX's collectives and lax.ppermute only.
A program may use at most 64 MiB of HBM per device.

v0:
```python
import jax
import jax.numpy as jnp
from jax import lax
from jax.sharding import PartitionSpec as P

HEADS = 8
KVH = 4
HD = 64
SLICES = 4
TOP_K = 2
STORED_SPAN = 1024


EPSILON = 1e-06


def copy_for_each(shard, axis):
    copies = jnp.broadcast_to(shard, (lax.axis_size(axis), *shard.shape))
    return lax.all_to_all(copies, axis, split_axis=0, concat_axis=0, tiled=True)


def of_everyone(shard, axis):
    everything = copy_for_each(shard, axis)
    return jnp.sum(everything.astype(jnp.float32), axis=0)


def in_blocks(shard, dim, devices):
    before, after = (shard.shape[:dim], shard.shape[dim + 1 :])
    return jnp.moveaxis(shard.reshape(*before, devices, -1, *after), dim, 0)


def sent_and_summed(shard, axis, dim):
    devices = lax.axis_size(axis)
    blocks = lax.all_to_all(in_blocks(shard, dim, devices), axis, 0, 0, tiled=True)
    return jnp.sum(blocks.astype(jnp.float32), axis=0)


def round_trip(values):
    return lax.optimization_barrier(values.astype(jnp.bfloat16)).astype(jnp.float32)


def inverse_rms(values, width):
    return lax.rsqrt(jnp.sum(values * values, axis=-1, keepdims=True) / width + EPSILON)


def body(
    tokens,
    attn_gain,
    query_weight,
    key_weight,
    value_weight,
    forget_weight,
    forget_bias,
    out_weight,
    key_cache,
    value_cache,
    cum_forget,
    lengths,
    ffn_gain,
    routes,
    route_weights,
    gate_weight,
    up_weight,
    down_weight,
):
    tp_count = lax.axis_size("tp")
    ep_count = lax.axis_size("ep")
    tp_rank = lax.axis_index("tp")
    seq_rows = tokens.shape[0]
    width = tokens.shape[1]
    cols = width // tp_count
    experts = ep_count // SLICES
    capacity = min(seq_rows, max(2, (2 * seq_rows * TOP_K + experts - 1) // experts))
    kv_local = key_cache.shape[1]
    group = HEADS // KVH
    score_scale = HD ** (-0.5)
    token_f = tokens.astype(jnp.float32)
    normed = (token_f * inverse_rms(token_f, width) * attn_gain).astype(jnp.bfloat16)
    query_rows = jnp.dot(normed, query_weight, preferred_element_type=jnp.float32).astype(
        jnp.bfloat16
    )
    query_rows = query_rows.reshape(seq_rows, kv_local, group, HD)
    fresh_keys = jnp.dot(normed, key_weight, preferred_element_type=jnp.float32).astype(
        jnp.bfloat16
    )
    fresh_keys = fresh_keys.reshape(seq_rows, kv_local, HD)
    new_values = jnp.dot(normed, value_weight, preferred_element_type=jnp.float32).astype(
        jnp.bfloat16
    )
    new_values = new_values.reshape(seq_rows, kv_local, HD)
    log_forget = jax.nn.log_sigmoid(
        jnp.dot(normed, forget_weight, preferred_element_type=jnp.float32) + forget_bias
    )
    log_forget = log_forget.reshape(seq_rows, kv_local, group)
    scores = (
        jnp.einsum("bkgd,bkdl->bkgl", query_rows, key_cache, preferred_element_type=jnp.float32)
        * score_scale
    )
    cumul = cum_forget.reshape(seq_rows, kv_local, group, STORED_SPAN)
    last_index = jnp.broadcast_to(
        (lengths - 1)[:, None, None, None], (seq_rows, kv_local, group, 1)
    )
    last = jnp.take_along_axis(cumul, last_index, axis=3)
    positions = lax.broadcasted_iota(jnp.int32, (1, 1, 1, STORED_SPAN), 3)
    valid = positions < lengths[:, None, None, None]
    scores = jnp.where(valid, scores + (last - cumul) + log_forget[..., None], -jnp.inf)
    self_score = (
        jnp.einsum("qvml,qvl->qvm", query_rows, fresh_keys, preferred_element_type=jnp.float32)
        * score_scale
    )
    top = jnp.maximum(jnp.max(scores, axis=3), self_score)
    expo = jnp.exp(scores - top[..., None])
    own_exp = jnp.exp(self_score - top)
    total = jnp.sum(expo, axis=3) + own_exp
    attn_weights = (expo / total[..., None]).astype(jnp.bfloat16)
    own_weight = round_trip(own_exp / total)
    heads_out = jnp.einsum(
        "bkgl,bkdl->bkgd", attn_weights, value_cache, preferred_element_type=jnp.float32
    )
    heads_out = heads_out + own_weight[..., None] * new_values.astype(jnp.float32)[:, :, None, :]
    heads_out = heads_out.astype(jnp.bfloat16).reshape(seq_rows, -1)
    partial_value = jnp.dot(heads_out, out_weight, preferred_element_type=jnp.float32)
    mixed = of_everyone(partial_value.astype(jnp.bfloat16), "tp").astype(jnp.float32)
    residual = round_trip(token_f + mixed)
    sent = (residual * inverse_rms(residual, width) * ffn_gain).astype(jnp.bfloat16)
    residual_cols = lax.dynamic_slice_in_dim(residual, tp_rank * cols, cols, 1)
    assigned = routes.reshape(-1)
    member = (assigned[:, None] == lax.broadcasted_iota(jnp.int32, (1, experts), 1)).astype(
        jnp.int32
    )
    earlier = jnp.cumsum(member, axis=0) - member
    slots = assigned * capacity + jnp.sum(earlier * member, axis=1)
    place = (slots[None, :] == lax.broadcasted_iota(jnp.int32, (experts * capacity, 1), 0)).astype(
        jnp.bfloat16
    )
    spread_rows = jnp.repeat(sent, TOP_K, axis=0)
    outgoing = jnp.dot(place, spread_rows, preferred_element_type=jnp.float32).astype(jnp.bfloat16)
    row_width = outgoing.shape[1]
    outgoing = jnp.broadcast_to(
        outgoing.reshape(experts, 1, capacity, row_width), (experts, SLICES, capacity, row_width)
    ).reshape(ep_count, capacity, row_width)
    gate_local = gate_weight[0]
    up_local = up_weight[0]
    down_local = down_weight[0]
    arrived = lax.all_to_all(outgoing, "ep", split_axis=0, concat_axis=0, tiled=True)
    slot_count = arrived.shape[1]
    flat = arrived.reshape(-1, width)
    gate = jnp.dot(flat, gate_local, preferred_element_type=jnp.float32)
    up = jnp.dot(flat, up_local, preferred_element_type=jnp.float32)
    hidden = (jax.nn.silu(gate) * up).astype(jnp.bfloat16)
    part = jnp.dot(hidden, down_local, preferred_element_type=jnp.float32)
    part = part.reshape(arrived.shape[0], slot_count, width)
    summed = sent_and_summed(part.astype(jnp.bfloat16), "tp", 2).astype(jnp.bfloat16)
    returned = lax.all_to_all(summed, "ep", split_axis=0, concat_axis=0, tiled=True)
    per_slot = jnp.sum(
        returned.astype(jnp.float32).reshape(experts, SLICES, capacity, cols), axis=1
    )
    per_slot = per_slot.reshape(experts * capacity, cols)
    picked = jnp.take(per_slot, slots, axis=0).reshape(seq_rows, TOP_K, cols)
    routed = jnp.sum(route_weights[:, :, None] * picked, axis=1)
    return (residual_cols + routed).astype(jnp.bfloat16)


def solution(mesh):
    return jax.shard_map(
        body,
        mesh=mesh,
        in_specs=(
            P("ep", None),
            P(),
            P(None, "tp"),
            P(None, "tp"),
            P(None, "tp"),
            P(None, "tp"),
            P("tp"),
            P("tp", None),
            P("ep", "tp", None, None),
            P("ep", "tp", None, None),
            P("ep", "tp", None),
            P("ep"),
            P(),
            P("ep", None),
            P("ep", None),
            P("ep", None, "tp"),
            P("ep", None, "tp"),
            P("ep", "tp", None),
        ),
        out_specs=P("ep", "tp"),
        check_vma=False,
    )
```

profile of v0, /device:TPU:1, one launch (start us, length us, event | category | flops | bytes accessed | tf_op | source)
XLA Modules:
  0.0 115.6 jit_solution(6360549392074428414)
XLA Ops:
  0.0 0.8 broadcast_add_fusion
  0.8 0.7 broadcast_compare_fusion
  1.4 0.7 iota_compare_fusion
  2.5 1.9 %gather_fusion.1 = f32[26]{0:T(128)S(1)} fusion(f32[13,2,1024]{2,1,0:T(2,128)} %param.28, s32[26]{0:T(128)S(1)} %reshape.376), kind=kCustom, calls=%fused_computation.1 | custom fusion | bytes 520 | tf_op jit(solution)/shard_map/jit(take_along_axis)/gather | solution.py:103
  5.4 0.2 fusion.24
  5.8 0.4 fusion.57
  6.2 0.2 fusion.35
  6.9 2.1 %fusion.20 = bf16[13,2,64]{2,1,0:T(2,128)(2,1)S(1)} fusion(bf16[13,1,64,1024]{3,2,1,0:T(8,128)(2,1)} %param.27, f32[13,2,1024]{2,1,0:T(2,128)S(1)} %get-tuple-element.10, f32[13,2]{1,0:T(8,128)S(1)} %get-tuple-element.6, f32[13,2]{1,0:T(8,128)S(1)} %fusion.42, f32[13,64]{1,0:T(8,128)S(1)} %fusion.23, f32[13,2]{1,0:T(8,128)S(1)} %copy.76), kind=kOutput, calls=%fused_computation.16 | convolution fusion | flops 3492736 | bytes 1817400 | tf_op jit(solution)/shard_map/bkgl,bkdl->bkgd/dot_general | solution.py:117
  9.2 0.7 broadcast_in_dim.73
  9.9 5.0 %all-to-all-start = ((bf16[4,13,1024]{2,1,0:T(8,128)(2,1)}), bf16[4,13,1024]{2,1,0:T(8,128)(2,1)S(1)}, u32[]{:S(2)}, u32[]{:S(2)}) async-start(bf16[4,13,1024]{2,1,0:T(8,128)(2,1)} %broadcast_in_dim.73), calls=%async_computation | async-start | bytes 262144 | tf_op jit(solution)/shard_map/all_to_all | solution.py:19
  15.4 4.3 %all-to-all-done = bf16[4,13,1024]{2,1,0:T(8,128)(2,1)S(1)} async-done(((bf16[4,13,1024]{2,1,0:T(8,128)(2,1)}), bf16[4,13,1024]{2,1,0:T(8,128)(2,1)S(1)}, u32[]{:S(2)}, u32[]{:S(2)}) %all-to-all-start) | async-done | bytes 106528 | tf_op jit(solution)/shard_map/all_to_all | solution.py:19
  20.3 0.3 broadcast_in_dim.77
  20.6 51.5 %all_to_all.20 = bf16[128,2,1024]{2,1,0:T(2,128)(2,1)S(1)} all-to-all(bf16[128,2,1024]{2,1,0:T(2,128)(2,1)S(1)} %bitcast.85), channel_id=1, replica_groups=mesh['ep'=128,'tp'=4] {'ep'}, dimensions={0} | all-to-all | bytes 1048576 | tf_op jit(solution)/shard_map/all_to_all | solution.py:145
  72.3 0.3 fusion.28
  72.6 1.2 %fusion.16 = bf16[256,128]{1,0:T(8,128)(2,1)S(1)} fusion(bf16[256,1024]{1,0:T(8,128)(2,1)S(1)} %reshape.356, bf16[1,1024,128]{2,1,0:T(8,128)(2,1)} %param.34, f32[256,128]{1,0:T(8,128)S(1)} %fusion.28), kind=kOutput, calls=%fused_computation.13 | convolution fusion | flops 67305472 | bytes 983040 | tf_op jit(solution)/shard_map/dot_general | solution.py:149
  73.8 0.3 convolution_convert_fusion
  74.1 0.8 copy.113
  74.9 3.5 %all-to-all-start.2 = ((bf16[4,128,2,256]{3,1,2,0:T(8,128)(2,1)}), bf16[4,128,2,256]{3,1,2,0:T(8,128)(2,1)S(1)}, u32[]{:S(2)}, u32[]{:S(2)}) async-start(bf16[4,128,2,256]{3,1,2,0:T(8,128)(2,1)} %bitcast.84), calls=%async_computation.2 | async-start | bytes 1048576 | tf_op jit(solution)/shard_map/all_to_all | solution.py:34
  78.7 7.9 %all-to-all-done.2 = bf16[4,128,2,256]{3,1,2,0:T(8,128)(2,1)S(1)} async-done(((bf16[4,128,2,256]{3,1,2,0:T(8,128)(2,1)}), bf16[4,128,2,256]{3,1,2,0:T(8,128)(2,1)S(1)}, u32[]{:S(2)}, u32[]{:S(2)}) %all-to-all-start.2) | async-done | bytes 524320 | tf_op jit(solution)/shard_map/all_to_all | solution.py:34
  86.6 0.8 copy.84
  87.4 10.7 %all-to-all-start.3 = ((bf16[128,2,256]{2,1,0:T(2,128)(2,1)}), bf16[128,2,256]{2,1,0:T(2,128)(2,1)S(1)}, u32[]{:S(2)}, u32[]{:S(2)}) async-start(bf16[128,2,256]{2,1,0:T(2,128)(2,1)} %copy.84), calls=%async_computation.3 | async-start | bytes 262144 | tf_op jit(solution)/shard_map/all_to_all | solution.py:154
  98.2 15.9 %all-to-all-done.3 = bf16[128,2,256]{2,1,0:T(2,128)(2,1)S(1)} async-done(((bf16[128,2,256]{2,1,0:T(2,128)(2,1)}), bf16[128,2,256]{2,1,0:T(2,128)(2,1)S(1)}, u32[]{:S(2)}, u32[]{:S(2)}) %all-to-all-start.3) | async-done | bytes 131104 | tf_op jit(solution)/shard_map/all_to_all | solution.py:154
  114.3 0.6 gather_fusion
  115.0 0.6 add_convert_fusion
  (83 shorter events, 3.9 us)
Async XLA Ops:
  0.0 5.8 %copy-start = (bf16[13,1,64,1024]{3,2,1,0:T(8,128)(2,1)S(1)}, bf16[13,1,64,1024]{3,2,1,0:T(8,128)(2,1)}, u32[]{:S(2)}) copy-start(bf16[13,1,64,1024]{3,2,1,0:T(8,128)(2,1)} %param.26) | copy-start | bytes 5111812
  2.4 2.2 %copy-start.5 = (bf16[13,1024]{1,0:T(8,128)(2,1)S(1)}, bf16[13,1024]{1,0:T(8,128)(2,1)}, u32[]{:S(2)}) copy-start(bf16[13,1024]{1,0:T(8,128)(2,1)} %param.18) | copy-start | bytes 79876
  2.4 2.3 %copy-start.9 = (bf16[1024,128]{1,0:T(8,128)(2,1)S(1)}, bf16[1024,128]{1,0:T(8,128)(2,1)}, u32[]{:S(2)}) copy-start(bf16[1024,128]{1,0:T(8,128)(2,1)} %param.20) | copy-start | bytes 786436
  2.5 2.3 %copy-start.13 = (f32[1024]{0:T(1024)S(1)}, f32[1024]{0:T(1024)}, u32[]{:S(2)}) copy-start(f32[1024]{0:T(1024)} %param.19) | copy-start | bytes 12292
  2.5 2.6 %copy-start.12 = (bf16[1024,2]{0,1:T(2,128)(2,1)S(1)}, bf16[1024,2]{0,1:T(2,128)(2,1)}, u32[]{:S(2)}) copy-start(bf16[1024,2]{0,1:T(2,128)(2,1)} %param.23) | copy-start | bytes 12292
  2.5 2.6 %copy-start.14 = (f32[2]{0:T(128)S(1)}, f32[2]{0:T(128)}, u32[]{:S(2)}) copy-start(f32[2]{0:T(128)} %param.24) | copy-start | bytes 28
  2.5 2.9 %copy-start.10 = (bf16[1024,64]{0,1:T(8,128)(2,1)S(1)}, bf16[1024,64]{0,1:T(8,128)(2,1)}, u32[]{:S(2)}) copy-start(bf16[1024,64]{0,1:T(8,128)(2,1)} %param.21) | copy-start | bytes 393220
  2.5 3.3 %copy-start.1 = (f32[13,2,1024]{2,1,0:T(2,128)S(1)}, f32[13,2,1024]{2,1,0:T(2,128)}, u32[]{:S(2)}) copy-start(f32[13,2,1024]{2,1,0:T(2,128)} %param.28) | copy-start | bytes 319492
  4.5 2.2 %copy-start.11 = (bf16[1024,64]{0,1:T(8,128)(2,1)S(1)}, bf16[1024,64]{0,1:T(8,128)(2,1)}, u32[]{:S(2)}) copy-start(bf16[1024,64]{0,1:T(8,128)(2,1)} %param.22) | copy-start | bytes 393220
  6.2 2.9 %copy-start.3 = (bf16[128,1024]{1,0:T(8,128)(2,1)S(1)}, bf16[128,1024]{1,0:T(8,128)(2,1)}, u32[]{:S(2)}) copy-start(bf16[128,1024]{1,0:T(8,128)(2,1)} %param.25) | copy-start | bytes 786436
  6.9 8.0 %copy-start.7 = (s32[13,2]{0,1:T(2,128)S(1)}, s32[13,2]{0,1:T(2,128)}, u32[]{:S(2)}) copy-start(s32[13,2]{0,1:T(2,128)} %param.31) | copy-start | bytes 316
  6.9 13.0 %copy-start.6 = (f32[1024]{0:T(1024)S(1)}, f32[1024]{0:T(1024)}, u32[]{:S(2)}) copy-start(f32[1024]{0:T(1024)} %param.30) | copy-start | bytes 12292
  9.9 9.8 %all-to-all-start = ((bf16[4,13,1024]{2,1,0:T(8,128)(2,1)}), bf16[4,13,1024]{2,1,0:T(8,128)(2,1)S(1)}, u32[]{:S(2)}, u32[]{:S(2)}) async-start(bf16[4,13,1024]{2,1,0:T(8,128)(2,1)} %broadcast_in_dim.73), calls=%async_computation | async-start | bytes 262144 | tf_op jit(solution)/shard_map/all_to_all | solution.py:19
  20.0 52.3 %copy-start.2 = (bf16[1,1024,128]{2,1,0:T(8,128)(2,1)S(1)}, bf16[1,1024,128]{2,1,0:T(8,128)(2,1)}, u32[]{:S(2)}) copy-start(bf16[1,1024,128]{2,1,0:T(8,128)(2,1)} %param.33) | copy-start | bytes 786436
  72.1 1.8 %copy-start.4 = (bf16[1,128,1024]{2,1,0:T(8,128)(2,1)S(1)}, bf16[1,128,1024]{2,1,0:T(8,128)(2,1)}, u32[]{:S(2)}) copy-start(bf16[1,128,1024]{2,1,0:T(8,128)(2,1)} %param.35) | copy-start | bytes 786436
  73.8 4.8 %copy-start.8 = (f32[13,2]{0,1:T(2,128)S(1)}, f32[13,2]{0,1:T(2,128)}, u32[]{:S(2)}) copy-start(f32[13,2]{0,1:T(2,128)} %param.32) | copy-start | bytes 316
  74.9 11.6 %all-to-all-start.2 = ((bf16[4,128,2,256]{3,1,2,0:T(8,128)(2,1)}), bf16[4,128,2,256]{3,1,2,0:T(8,128)(2,1)S(1)}, u32[]{:S(2)}, u32[]{:S(2)}) async-start(bf16[4,128,2,256]{3,1,2,0:T(8,128)(2,1)} %bitcast.84), calls=%async_computation.2 | async-start | bytes 1048576 | tf_op jit(solution)/shard_map/all_to_all | solution.py:34
  87.4 26.7 %all-to-all-start.3 = ((bf16[128,2,256]{2,1,0:T(2,128)(2,1)}), bf16[128,2,256]{2,1,0:T(2,128)(2,1)S(1)}, u32[]{:S(2)}, u32[]{:S(2)}) async-start(bf16[128,2,256]{2,1,0:T(2,128)(2,1)} %copy.84), calls=%async_computation.3 | async-start | bytes 262144 | tf_op jit(solution)/shard_map/all_to_all | solution.py:154
where the time goes:
time: 116 us
  blocking collectives  51.5 us (44%)
  waiting for transfers between devices  28.1 us (24%)
  starting transfers between devices  19.1 us (16%)
  local copies, waits for them, and re-layouts  6.73 us (6%)
  matrix products  5.61 us (5%)
  other arithmetic  4.16 us (4%)
    all_to_all x1, blocking collectives, body(): lax.all_to_all(outgoing, 'ep', split_axis=0, concat_axis=0, tiled=True)  51.5 us
    all_to_all x1, waiting for transfers between devices, body(): lax.all_to_all(summed, 'ep', split_axis=0, concat_axis=0, tiled=True)  15.9 us
    all_to_all x1, starting transfers between devices, body(): lax.all_to_all(summed, 'ep', split_axis=0, concat_axis=0, tiled=True)  10.7 us
    all_to_all x1, waiting for transfers between devices, sent_and_summed(): lax.all_to_all(in_blocks(shard, dim, devices), axis, 0, 0, tiled=True)  7.86 us
    all_to_all x1, starting transfers between devices, copy_for_each(): return lax.all_to_all(copies, axis, split_axis=0, concat_axis=0, tiled=True)  5 us
    all_to_all x1, waiting for transfers between devices, copy_for_each(): return lax.all_to_all(copies, axis, split_axis=0, concat_axis=0, tiled=True)  4.32 us
    all_to_all x1, starting transfers between devices, sent_and_summed(): lax.all_to_all(in_blocks(shard, dim, devices), axis, 0, 0, tiled=True)  3.47 us
  transfers between devices with their start and end apart: 3, of which 3 were waited for; matrix products, arithmetic and copies ran while one was open for 1% of the time, Pallas kernels for 0%

commit v1 on v0

--- a/solution.py
+++ b/solution.py
@@ -1,6 +1,7 @@
 import jax
 import jax.numpy as jnp
 from jax import lax
+from jax.sharding import Mesh
 from jax.sharding import PartitionSpec as P
 
 HEADS = 8
@@ -12,16 +13,15 @@
 
 
 EPSILON = 1e-06
+EXPERT_AXES = ("z", "xh")
+SLICE_AXES = ("xl", "core")
+EP_AXES = EXPERT_AXES + SLICE_AXES
+GROUP_AXES = SLICE_AXES + ("tp",)
 
 
 def copy_for_each(shard, axis):
     copies = jnp.broadcast_to(shard, (lax.axis_size(axis), *shard.shape))
     return lax.all_to_all(copies, axis, split_axis=0, concat_axis=0, tiled=True)
-
-
-def of_everyone(shard, axis):
-    everything = copy_for_each(shard, axis)
-    return jnp.sum(everything.astype(jnp.float32), axis=0)
 
 
 def in_blocks(shard, dim, devices):
@@ -41,6 +41,22 @@
 
 def inverse_rms(values, width):
     return lax.rsqrt(jnp.sum(values * values, axis=-1, keepdims=True) / width + EPSILON)
+
+
+def slot_tables(routes, route_weights, experts, capacity):
+    seq_rows = routes.shape[0]
+    expert = lax.broadcasted_iota(jnp.int32, (experts, 1, 1), 0)
+    chosen = routes[None] == expert
+    named = jnp.any(chosen, axis=2).astype(jnp.float32)
+    share = jnp.sum(jnp.where(chosen, route_weights[None], 0.0), axis=2)
+    first = lax.broadcasted_iota(jnp.int32, (seq_rows, seq_rows), 0)
+    second = lax.broadcasted_iota(jnp.int32, (seq_rows, seq_rows), 1)
+    earlier = jnp.dot(named, (first < second).astype(jnp.float32))
+    slot = lax.broadcasted_iota(jnp.int32, (1, capacity, 1), 1).astype(jnp.float32)
+    here = (earlier[:, None, :] == slot) & (named[:, None, :] > 0.0)
+    place = here.astype(jnp.bfloat16).reshape(experts * capacity, seq_rows)
+    weighted = jnp.where(here, share[:, None, :], 0.0).reshape(experts * capacity, seq_rows)
+    return place, weighted.T
 
 
 def body(
@@ -64,7 +80,7 @@
     down_weight,
 ):
     tp_count = lax.axis_size("tp")
-    ep_count = lax.axis_size("ep")
+    ep_count = lax.axis_size(EXPERT_AXES) * SLICES
     tp_rank = lax.axis_index("tp")
     seq_rows = tokens.shape[0]
     width = tokens.shape[1]
@@ -120,53 +136,45 @@
     heads_out = heads_out + own_weight[..., None] * new_values.astype(jnp.float32)[:, :, None, :]
     heads_out = heads_out.astype(jnp.bfloat16).reshape(seq_rows, -1)
     partial_value = jnp.dot(heads_out, out_weight, preferred_element_type=jnp.float32)
-    mixed = of_everyone(partial_value.astype(jnp.bfloat16), "tp").astype(jnp.float32)
-    residual = round_trip(token_f + mixed)
-    sent = (residual * inverse_rms(residual, width) * ffn_gain).astype(jnp.bfloat16)
-    residual_cols = lax.dynamic_slice_in_dim(residual, tp_rank * cols, cols, 1)
-    assigned = routes.reshape(-1)
-    member = (assigned[:, None] == lax.broadcasted_iota(jnp.int32, (1, experts), 1)).astype(
-        jnp.int32
+    mixed_cols = sent_and_summed(partial_value.astype(jnp.bfloat16), "tp", 1)
+    token_cols = lax.dynamic_slice_in_dim(token_f, tp_rank * cols, cols, 1)
+    residual_cols = (token_cols + mixed_cols).astype(jnp.bfloat16)
+    place, weighted = slot_tables(routes, route_weights, experts, capacity)
+    outgoing = jnp.dot(place, residual_cols, preferred_element_type=jnp.float32)
+    outgoing = outgoing.astype(jnp.bfloat16).reshape(experts, capacity, cols)
+    arrived = lax.all_to_all(outgoing, EXPERT_AXES, split_axis=0, concat_axis=0, tiled=True)
+    arrived = arrived.reshape(experts * capacity, cols)
+    gathered = copy_for_each(arrived, GROUP_AXES)
+    gathered = gathered.reshape(SLICES, tp_count, experts * capacity, cols)
+    rows = jnp.transpose(gathered, (0, 2, 1, 3)).reshape(-1, width).astype(jnp.float32)
+    flat = (rows * inverse_rms(rows, width) * ffn_gain).astype(jnp.bfloat16)
+    gate = jnp.dot(flat, gate_weight[0], preferred_element_type=jnp.float32)
+    up = jnp.dot(flat, up_weight[0], preferred_element_type=jnp.float32)
+    hidden = (jax.nn.silu(gate) * up).astype(jnp.bfloat16)
+    part = jnp.dot(hidden, down_weight[0], preferred_element_type=jnp.float32)
+    part = part.astype(jnp.bfloat16).reshape(SLICES, experts * capacity, tp_count, cols)
+    part = jnp.transpose(part, (0, 2, 1, 3)).reshape(-1, experts * capacity, cols)
+    parts = lax.all_to_all(part, GROUP_AXES, split_axis=0, concat_axis=0, tiled=True)
+    summed = jnp.sum(parts.astype(jnp.float32), axis=0).astype(jnp.bfloat16)
+    summed = summed.reshape(experts, capacity, cols)
+    returned = lax.all_to_all(summed, EXPERT_AXES, split_axis=0, concat_axis=0, tiled=True)
+    returned = returned.reshape(experts * capacity, cols).astype(jnp.float32)
+    routed = jnp.dot(
+        weighted, returned, precision=lax.Precision.HIGHEST, preferred_element_type=jnp.float32
     )
-    earlier = jnp.cumsum(member, axis=0) - member
-    slots = assigned * capacity + jnp.sum(earlier * member, axis=1)
-    place = (slots[None, :] == lax.broadcasted_iota(jnp.int32, (experts * capacity, 1), 0)).astype(
-        jnp.bfloat16
-    )
-    spread_rows = jnp.repeat(sent, TOP_K, axis=0)
-    outgoing = jnp.dot(place, spread_rows, preferred_element_type=jnp.float32).astype(jnp.bfloat16)
-    row_width = outgoing.shape[1]
-    outgoing = jnp.broadcast_to(
-        outgoing.reshape(experts, 1, capacity, row_width), (experts, SLICES, capacity, row_width)
-    ).reshape(ep_count, capacity, row_width)
-    gate_local = gate_weight[0]
-    up_local = up_weight[0]
-    down_local = down_weight[0]
-    arrived = lax.all_to_all(outgoing, "ep", split_axis=0, concat_axis=0, tiled=True)
-    slot_count = arrived.shape[1]
-    flat = arrived.reshape(-1, width)
-    gate = jnp.dot(flat, gate_local, preferred_element_type=jnp.float32)
-    up = jnp.dot(flat, up_local, preferred_element_type=jnp.float32)
-    hidden = (jax.nn.silu(gate) * up).astype(jnp.bfloat16)
-    part = jnp.dot(hidden, down_local, preferred_element_type=jnp.float32)
-    part = part.reshape(arrived.shape[0], slot_count, width)
-    summed = sent_and_summed(part.astype(jnp.bfloat16), "tp", 2).astype(jnp.bfloat16)
-    returned = lax.all_to_all(summed, "ep", split_axis=0, concat_axis=0, tiled=True)
-    per_slot = jnp.sum(
-        returned.astype(jnp.float32).reshape(experts, SLICES, capacity, cols), axis=1
-    )
-    per_slot = per_slot.reshape(experts * capacity, cols)
-    picked = jnp.take(per_slot, slots, axis=0).reshape(seq_rows, TOP_K, cols)
-    routed = jnp.sum(route_weights[:, :, None] * picked, axis=1)
-    return (residual_cols + routed).astype(jnp.bfloat16)
+    return (residual_cols.astype(jnp.float32) + routed).astype(jnp.bfloat16)
 
 
 def solution(mesh):
+    half = mesh.shape["ep"] // (2 * SLICES)
+    fine = Mesh(
+        mesh.devices.reshape(half, 2, 2, 2, mesh.shape["tp"]), EP_AXES + ("tp",)
+    )
     return jax.shard_map(
         body,
-        mesh=mesh,
+        mesh=fine,
         in_specs=(
-            P("ep", None),
+            P(EP_AXES, None),
             P(),
             P(None, "tp"),
             P(None, "tp"),
@@ -174,17 +182,17 @@
             P(None, "tp"),
             P("tp"),
             P("tp", None),
-            P("ep", "tp", None, None),
-            P("ep", "tp", None, None),
-            P("ep", "tp", None),
-            P("ep"),
+            P(EP_AXES, "tp", None, None),
+            P(EP_AXES, "tp", None, None),
+            P(EP_AXES, "tp", None),
+            P(EP_AXES),
             P(),
-            P("ep", None),
-            P("ep", None),
-            P("ep", None, "tp"),
-            P("ep", None, "tp"),
-            P("ep", "tp", None),
+            P(EP_AXES, None),
+            P(EP_AXES, None),
+            P(EP_AXES, None, "tp"),
+            P(EP_AXES, None, "tp"),
+            P(EP_AXES, "tp", None),
         ),
-        out_specs=P("ep", "tp"),
+        out_specs=P(EP_AXES, "tp"),
         check_vma=False,
     )

time: 116 us -> 106 us (0.914)
  blocking collectives: 51.5 us -> 31.2 us
  waiting for transfers between devices: 28.1 us -> 37.4 us
    all_to_all x1, blocking collectives: 51.5 us -> 31.2 us  [body(): lax.all_to_all(outgoing, EXPERT_AXES, split_axis=0, concat_axis=0, tiled=...]
    all_to_all x1 -> x2, waiting for transfers between devices: 15.9 us -> 23.5 us  [the longest x1 13.6 us: body(): lax.all_to_all(summed, EXPERT_AXES, split_axis=0, concat_axis=0, tiled=True)]
    all_to_all x1, waiting for transfers between devices: 4.32 us -> 10.2 us  [copy_for_each(): return lax.all_to_all(copies, axis, split_axis=0, concat_axis=0, tiled=True)]
    all_to_all x1, waiting for transfers between devices: 7.86 us -> 3.59 us  [sent_and_summed(): lax.all_to_all(in_blocks(shard, dim, devices), axis, 0, 0, tiled=True)]
    all_to_all x1 -> x2, starting transfers between devices: 10.7 us -> 7.72 us  [the longest x1 3.92 us: body(): lax.all_to_all(part, GROUP_AXES, split_axis=0, concat_axis=0, tiled=True)]
    all_to_all x1, starting transfers between devices: 5 us -> 6.9 us  [copy_for_each(): return lax.all_to_all(copies, axis, split_axis=0, concat_axis=0, tiled=True)]
    reshape x4 -> x5, local copies, waits for them, and re-layouts: 0.36 us -> 1.91 us  [the longest x2 1.25 us: body(): part.astype(jnp.bfloat16)]
    all_to_all x1, starting transfers between devices: 3.47 us -> 5 us  [sent_and_summed(): lax.all_to_all(in_blocks(shard, dim, devices), axis, 0, 0, tiled=True)]
  transfers between devices with their start and end apart: 3 -> 4, of which waited for: 3 -> 4; matrix products, arithmetic and copies ran while one was open for 1% -> 1% of each run, Pallas kernels for 0% -> 0%
where the time goes in v1:
time: 106 us; the launch traced here: 105 us
  waiting for transfers between devices  37.4 us (35%)
  blocking collectives  31.2 us (29%)
  starting transfers between devices  19.6 us (18%)
  local copies, waits for them, and re-layouts  7.45 us (7%)
  matrix products  5.6 us (5%)
  other arithmetic  3.45 us (3%)
    all_to_all x1, blocking collectives, body(): lax.all_to_all(outgoing, EXPERT_AXES, split_axis=0, concat_axis=0, tiled=...  31.2 us
    all_to_all x1, waiting for transfers between devices, body(): lax.all_to_all(summed, EXPERT_AXES, split_axis=0, concat_axis=0, tiled=True)  13.6 us
    all_to_all x1, waiting for transfers between devices, copy_for_each(): return lax.all_to_all(copies, axis, split_axis=0, concat_axis=0, tiled=True)  10.2 us
    all_to_all x1, waiting for transfers between devices, body(): lax.all_to_all(part, GROUP_AXES, split_axis=0, concat_axis=0, tiled=True)  9.95 us
    all_to_all x1, starting transfers between devices, copy_for_each(): return lax.all_to_all(copies, axis, split_axis=0, concat_axis=0, tiled=True)  6.9 us
    all_to_all x1, starting transfers between devices, sent_and_summed(): lax.all_to_all(in_blocks(shard, dim, devices), axis, 0, 0, tiled=True)  5 us
    all_to_all x1, starting transfers between devices, body(): lax.all_to_all(part, GROUP_AXES, split_axis=0, concat_axis=0, tiled=True)  3.92 us
    all_to_all x1, starting transfers between devices, body(): lax.all_to_all(summed, EXPERT_AXES, split_axis=0, concat_axis=0, tiled=True)  3.8 us
  transfers between devices with their start and end apart: 4, of which 4 were waited for; matrix products, arithmetic and copies ran while one was open for 1% of the time, Pallas kernels for 0%

profile of v1, /device:TPU:1, one launch (start us, length us, event | category | flops | bytes accessed | tf_op | source)
XLA Modules:
  0.0 105.1 jit_solution(5459939611976518200)
XLA Ops:
  0.0 0.8 broadcast_add_fusion
  0.8 0.7 broadcast_compare_fusion
  1.4 0.7 iota_compare_fusion
  2.5 1.9 %gather_fusion = f32[26]{0:T(128)S(1)} fusion(f32[13,2,1024]{2,1,0:T(2,128)} %param.28, s32[26]{0:T(128)S(1)} %reshape.351), kind=kCustom, calls=%fused_computation | custom fusion | bytes 520 | tf_op jit(solution)/shard_map/jit(take_along_axis)/gather | solution.py:119
  5.8 0.4 fusion.66
  6.9 2.1 %fusion.22 = bf16[13,2,64]{2,1,0:T(2,128)(2,1)S(1)} fusion(bf16[13,1,64,1024]{3,2,1,0:T(8,128)(2,1)} %param.27, f32[13,2,1024]{2,1,0:T(2,128)S(1)} %get-tuple-element.10, f32[13,2]{1,0:T(8,128)S(1)} %get-tuple-element.6, f32[13,2]{1,0:T(8,128)S(1)} %fusion.55, f32[13,64]{1,0:T(8,128)S(1)} %fusion.25, f32[13,2]{1,0:T(8,128)S(1)} %copy.64), kind=kOutput, calls=%fused_computation.20 | convolution fusion | flops 3492736 | bytes 1817400 | tf_op jit(solution)/shard_map/bkgl,bkdl->bkgd/dot_general | solution.py:133
  9.3 0.6 copy.103
  9.9 5.0 %all-to-all-start = ((bf16[4,13,256]{2,1,0:T(8,128)(2,1)}), bf16[4,13,256]{2,1,0:T(8,128)(2,1)S(1)}, u32[]{:S(2)}, u32[]{:S(2)}) async-start(bf16[4,13,256]{2,1,0:T(8,128)(2,1)} %bitcast.88), calls=%async_computation | async-start | bytes 65536 | tf_op jit(solution)/shard_map/all_to_all | solution.py:34
  15.6 3.6 %all-to-all-done = bf16[4,13,256]{2,1,0:T(8,128)(2,1)S(1)} async-done(((bf16[4,13,256]{2,1,0:T(8,128)(2,1)}), bf16[4,13,256]{2,1,0:T(8,128)(2,1)S(1)}, u32[]{:S(2)}, u32[]{:S(2)}) %all-to-all-start) | async-done | bytes 26656 | tf_op jit(solution)/shard_map/all_to_all | solution.py:34
  19.4 31.2 %all_to_all.25 = bf16[32,2,256]{2,1,0:T(2,128)(2,1)S(1)} all-to-all(bf16[32,2,256]{2,1,0:T(2,128)(2,1)S(1)} %reshape.340), channel_id=1, replica_groups=mesh['z'=16,'xh'=2,'xl'=2,'core'=2,'tp'=4] {'z','xh'}, dimensions={0} | all-to-all | bytes 65536 | tf_op jit(solution)/shard_map/all_to_all | solution.py:145
  50.7 0.8 broadcast_in_dim.84
  51.5 6.9 %all-to-all-start.2 = ((bf16[16,64,256]{2,1,0:T(8,128)(2,1)}), bf16[16,64,256]{2,1,0:T(8,128)(2,1)S(1)}, u32[]{:S(2)}, u32[]{:S(2)}) async-start(bf16[16,64,256]{2,1,0:T(8,128)(2,1)} %broadcast_in_dim.84), calls=%async_computation.2 | async-start | bytes 1048576 | tf_op jit(solution)/shard_map/all_to_all | solution.py:24
  58.5 10.2 %all-to-all-done.2 = bf16[16,64,256]{2,1,0:T(8,128)(2,1)S(1)} async-done(((bf16[16,64,256]{2,1,0:T(8,128)(2,1)}), bf16[16,64,256]{2,1,0:T(8,128)(2,1)S(1)}, u32[]{:S(2)}, u32[]{:S(2)}) %all-to-all-start.2) | async-done | bytes 524320 | tf_op jit(solution)/shard_map/all_to_all | solution.py:24
  69.1 0.4 copy.72
  69.8 0.3 fusion.35
  70.1 0.5 convolution_convert_fusion
  70.7 0.4 reshape.342
  71.0 0.9 copy.73
  71.9 3.9 %all-to-all-start.3 = ((bf16[16,64,256]{2,1,0:T(8,128)(2,1)}), bf16[16,64,256]{2,1,0:T(8,128)(2,1)S(1)}, u32[]{:S(2)}, u32[]{:S(2)}) async-start(bf16[16,64,256]{2,1,0:T(8,128)(2,1)} %bitcast.16), calls=%async_computation.3 | async-start | bytes 1048576 | tf_op jit(solution)/shard_map/all_to_all | solution.py:157
  76.1 9.9 %all-to-all-done.3 = bf16[16,64,256]{2,1,0:T(8,128)(2,1)S(1)} async-done(((bf16[16,64,256]{2,1,0:T(8,128)(2,1)}), bf16[16,64,256]{2,1,0:T(8,128)(2,1)S(1)}, u32[]{:S(2)}, u32[]{:S(2)}) %all-to-all-start.3) | async-done | bytes 524320 | tf_op jit(solution)/shard_map/all_to_all | solution.py:157
  86.2 0.6 reshape.344
  86.8 3.8 %all-to-all-start.4 = ((bf16[32,2,256]{2,1,0:T(2,128)(2,1)}), bf16[32,2,256]{2,1,0:T(2,128)(2,1)S(1)}, u32[]{:S(2)}, u32[]{:S(2)}) async-start(bf16[32,2,256]{2,1,0:T(2,128)(2,1)} %reshape.344), calls=%async_computation.4 | async-start | bytes 65536 | tf_op jit(solution)/shard_map/all_to_all | solution.py:160
  90.7 13.6 %all-to-all-done.4 = bf16[32,2,256]{2,1,0:T(2,128)(2,1)S(1)} async-done(((bf16[32,2,256]{2,1,0:T(2,128)(2,1)}), bf16[32,2,256]{2,1,0:T(2,128)(2,1)S(1)}, u32[]{:S(2)}, u32[]{:S(2)}) %all-to-all-start.4) | async-done | bytes 32800 | tf_op jit(solution)/shard_map/all_to_all | solution.py:160
  104.3 0.8 fusion.21
  (86 shorter events, 4.5 us)
Async XLA Ops:
  0.0 5.8 %copy-start = (bf16[13,1,64,1024]{3,2,1,0:T(8,128)(2,1)S(1)}, bf16[13,1,64,1024]{3,2,1,0:T(8,128)(2,1)}, u32[]{:S(2)}) copy-start(bf16[13,1,64,1024]{3,2,1,0:T(8,128)(2,1)} %param.26) | copy-start | bytes 5111812
  2.4 2.2 %copy-start.6 = (bf16[13,1024]{1,0:T(8,128)(2,1)S(1)}, bf16[13,1024]{1,0:T(8,128)(2,1)}, u32[]{:S(2)}) copy-start(bf16[13,1024]{1,0:T(8,128)(2,1)} %param.18) | copy-start | bytes 79876
  2.4 2.3 %copy-start.10 = (bf16[1024,128]{1,0:T(8,128)(2,1)S(1)}, bf16[1024,128]{1,0:T(8,128)(2,1)}, u32[]{:S(2)}) copy-start(bf16[1024,128]{1,0:T(8,128)(2,1)} %param.20) | copy-start | bytes 786436
  2.5 2.3 %copy-start.14 = (f32[1024]{0:T(1024)S(1)}, f32[1024]{0:T(1024)}, u32[]{:S(2)}) copy-start(f32[1024]{0:T(1024)} %param.19) | copy-start | bytes 12292
  2.5 2.6 %copy-start.13 = (bf16[1024,2]{0,1:T(2,128)(2,1)S(1)}, bf16[1024,2]{0,1:T(2,128)(2,1)}, u32[]{:S(2)}) copy-start(bf16[1024,2]{0,1:T(2,128)(2,1)} %param.23) | copy-start | bytes 12292
  2.5 2.6 %copy-start.15 = (f32[2]{0:T(128)S(1)}, f32[2]{0:T(128)}, u32[]{:S(2)}) copy-start(f32[2]{0:T(128)} %param.24) | copy-start | bytes 28
  2.5 2.9 %copy-start.11 = (bf16[1024,64]{0,1:T(8,128)(2,1)S(1)}, bf16[1024,64]{0,1:T(8,128)(2,1)}, u32[]{:S(2)}) copy-start(bf16[1024,64]{0,1:T(8,128)(2,1)} %param.21) | copy-start | bytes 393220
  2.5 3.3 %copy-start.1 = (f32[13,2,1024]{2,1,0:T(2,128)S(1)}, f32[13,2,1024]{2,1,0:T(2,128)}, u32[]{:S(2)}) copy-start(f32[13,2,1024]{2,1,0:T(2,128)} %param.28) | copy-start | bytes 319492
  4.5 2.2 %copy-start.12 = (bf16[1024,64]{0,1:T(8,128)(2,1)S(1)}, bf16[1024,64]{0,1:T(8,128)(2,1)}, u32[]{:S(2)}) copy-start(bf16[1024,64]{0,1:T(8,128)(2,1)} %param.22) | copy-start | bytes 393220
  6.2 2.8 %copy-start.3 = (bf16[128,1024]{1,0:T(8,128)(2,1)S(1)}, bf16[128,1024]{1,0:T(8,128)(2,1)}, u32[]{:S(2)}) copy-start(bf16[128,1024]{1,0:T(8,128)(2,1)} %param.25) | copy-start | bytes 786436
  6.7 8.2 %copy-start.8 = (s32[13,2]{0,1:T(2,128)S(1)}, s32[13,2]{0,1:T(2,128)}, u32[]{:S(2)}) copy-start(s32[13,2]{0,1:T(2,128)} %param.31) | copy-start | bytes 316
  9.0 49.5 %copy-start.7 = (f32[1024]{0:T(1024)S(1)}, f32[1024]{0:T(1024)}, u32[]{:S(2)}) copy-start(f32[1024]{0:T(1024)} %param.30) | copy-start | bytes 12292
  9.9 9.3 %all-to-all-start = ((bf16[4,13,256]{2,1,0:T(8,128)(2,1)}), bf16[4,13,256]{2,1,0:T(8,128)(2,1)S(1)}, u32[]{:S(2)}, u32[]{:S(2)}) async-start(bf16[4,13,256]{2,1,0:T(8,128)(2,1)} %bitcast.88), calls=%async_computation | async-start | bytes 65536 | tf_op jit(solution)/shard_map/all_to_all | solution.py:34
  51.5 17.1 %all-to-all-start.2 = ((bf16[16,64,256]{2,1,0:T(8,128)(2,1)}), bf16[16,64,256]{2,1,0:T(8,128)(2,1)S(1)}, u32[]{:S(2)}, u32[]{:S(2)}) async-start(bf16[16,64,256]{2,1,0:T(8,128)(2,1)} %broadcast_in_dim.84), calls=%async_computation.2 | async-start | bytes 1048576 | tf_op jit(solution)/shard_map/all_to_all | solution.py:24
  68.9 1.0 copy-start.2
  69.1 1.0 copy-start.4
  69.1 1.0 copy-start.5
  70.6 5.2 %copy-start.9 = (f32[13,2]{0,1:T(2,128)S(1)}, f32[13,2]{0,1:T(2,128)}, u32[]{:S(2)}) copy-start(f32[13,2]{0,1:T(2,128)} %param.32) | copy-start | bytes 316
  71.9 14.2 %all-to-all-start.3 = ((bf16[16,64,256]{2,1,0:T(8,128)(2,1)}), bf16[16,64,256]{2,1,0:T(8,128)(2,1)S(1)}, u32[]{:S(2)}, u32[]{:S(2)}) async-start(bf16[16,64,256]{2,1,0:T(8,128)(2,1)} %bitcast.16), calls=%async_computation.3 | async-start | bytes 1048576 | tf_op jit(solution)/shard_map/all_to_all | solution.py:157
  86.8 17.5 %all-to-all-start.4 = ((bf16[32,2,256]{2,1,0:T(2,128)(2,1)}), bf16[32,2,256]{2,1,0:T(2,128)(2,1)S(1)}, u32[]{:S(2)}, u32[]{:S(2)}) async-start(bf16[32,2,256]{2,1,0:T(2,128)(2,1)} %reshape.344), calls=%async_computation.4 | async-start | bytes 65536 | tf_op jit(solution)/shard_map/all_to_all | solution.py:160

commit v2 on v1

v2 whole, which is shorter than its diff:
```python
import functools

import jax
import jax.numpy as jnp
from jax import lax
from jax.experimental import pallas as pl
from jax.experimental.pallas import tpu as pltpu
from jax.sharding import Mesh
from jax.sharding import PartitionSpec as P

HEADS = 8
KVH = 4
HD = 64
SLICES = 4
TOP_K = 2
STORED_SPAN = 1024


EPSILON = 1e-06
EXPERT_AXES = ("z", "xh")
SLICE_AXES = ("xl", "core")
EP_AXES = EXPERT_AXES + SLICE_AXES
GROUP_AXES = SLICE_AXES + ("tp",)


def copy_for_each(shard, axis):
    copies = jnp.broadcast_to(shard, (lax.axis_size(axis), *shard.shape))
    return lax.all_to_all(copies, axis, split_axis=0, concat_axis=0, tiled=True)


def attention_kernel(
    lengths,
    bias,
    tokens,
    gain,
    wq,
    wk,
    wv,
    wf,
    wo,
    cumul,
    keys,
    values,
    out,
    key_buf,
    value_buf,
    cum_rows,
    token_rows,
    key_sems,
    value_sems,
    *,
    seq_rows,
    pad,
    chunk,
):
    span = keys.shape[1]
    total_rows = seq_rows * HD
    width = tokens.shape[1]
    starts = list(range(0, total_rows, chunk))

    def copies(source, buf, sems):
        return [
            pltpu.make_async_copy(
                source.at[pl.ds(r, min(chunk, total_rows - r))],
                buf.at[pl.ds(r, min(chunk, total_rows - r))],
                sems.at[i],
            )
            for i, r in enumerate(starts)
        ]

    key_copies = copies(keys, key_buf, key_sems)
    value_copies = copies(values, value_buf, value_sems)
    for copy in key_copies + value_copies:
        copy.start()

    f32 = jnp.float32
    bf16 = jnp.bfloat16
    nt = (((1,), (1,)), ((), ()))
    token_rows[...] = jnp.zeros_like(token_rows)
    token_rows[0:seq_rows, :] = tokens[...].astype(f32)
    cum_rows[...] = jnp.zeros_like(cum_rows)
    for b in range(seq_rows):
        pair = cumul[b]
        cum_rows[b : b + 1, :] = pair[0:1, :]
        cum_rows[pad + b : pad + b + 1, :] = pair[1:2, :]

    rows = token_rows[...]
    inv = lax.rsqrt(jnp.sum(rows * rows, axis=-1, keepdims=True) / width + EPSILON)
    normed_f = (rows * inv * gain[...]).astype(bf16).astype(f32)
    normed = normed_f.astype(bf16)
    query = jnp.dot(normed, wq[...], preferred_element_type=f32).astype(bf16).astype(f32)
    fresh = lax.dot_general(normed, wk[...], nt, preferred_element_type=f32)
    fresh = fresh.astype(bf16).astype(f32)
    new_values = lax.dot_general(normed, wv[...], nt, preferred_element_type=f32)
    new_values = new_values.astype(bf16).astype(f32)
    wf_rows = wf[...].astype(f32)
    forget = []
    for g in range(2):
        raw = jnp.sum(normed_f * wf_rows[g : g + 1, :], axis=-1, keepdims=True) + bias[g]
        forget.append(jnp.minimum(raw, 0.0) - jnp.log1p(jnp.exp(-jnp.abs(raw))))
    log_forget = jnp.concatenate(forget, axis=0)

    scale = HD ** (-0.5)
    own = jnp.concatenate(
        [
            jnp.sum(query[:, g * HD : (g + 1) * HD] * fresh, axis=-1, keepdims=True)
            for g in range(2)
        ],
        axis=0,
    )
    own = own * scale

    swapped = pltpu.roll(query, HD, 1)
    low = lax.broadcasted_iota(jnp.int32, query.shape, 1) < HD
    both = jnp.concatenate([jnp.where(low, query, swapped), jnp.where(low, swapped, query)], axis=0)
    both = both * scale
    row_seq = lax.broadcasted_iota(jnp.int32, (2 * pad, 1), 0)
    row_seq = jnp.where(row_seq >= pad, row_seq - pad, row_seq)
    scores = jnp.zeros((2 * pad, span), f32)
    for i, r in enumerate(starts):
        size = min(chunk, total_rows - r)
        parts = [both] * (size // (2 * HD)) + ([both[:, :HD]] if size % (2 * HD) else [])
        left = jnp.concatenate(parts, axis=1) if len(parts) > 1 else parts[0]
        seq = lax.broadcasted_iota(jnp.int32, (1, size), 1) // HD + r // HD
        left = jnp.where(seq == row_seq, left, 0.0).astype(bf16)
        key_copies[i].wait()
        scores = scores + jnp.dot(left, key_buf[r : r + size, :], preferred_element_type=f32)

    limit = jnp.zeros((2 * pad, 1), jnp.int32)
    for b in range(seq_rows):
        limit = jnp.where(row_seq == b, lengths[b], limit)
    position = lax.broadcasted_iota(jnp.int32, (1, span), 1)
    cum = cum_rows[...]
    last = jnp.sum(jnp.where(position == limit - 1, cum, 0.0), axis=-1, keepdims=True)
    scores = jnp.where(position < limit, scores + (last - cum) + log_forget, -jnp.inf)
    top = jnp.maximum(jnp.max(scores, axis=-1, keepdims=True), own)
    expo = jnp.exp(scores - top)
    own_exp = jnp.exp(own - top)
    total = jnp.sum(expo, axis=-1, keepdims=True) + own_exp
    weights = (expo / total).astype(bf16)
    own_weight = (own_exp / total).astype(bf16).astype(f32)

    folded = jnp.zeros((2 * pad, 2 * HD), f32)
    for i, r in enumerate(starts):
        size = min(chunk, total_rows - r)
        value_copies[i].wait()
        wide = lax.dot_general(
            weights, value_buf[r : r + size, :], nt, preferred_element_type=f32
        )
        seq = lax.broadcasted_iota(jnp.int32, (1, size), 1) // HD + r // HD
        wide = jnp.where(seq == row_seq, wide, 0.0)
        for c in range(0, size, 2 * HD):
            piece = wide[:, c : min(c + 2 * HD, size)]
            if piece.shape[1] < 2 * HD:
                piece = jnp.concatenate([piece, jnp.zeros_like(piece)], axis=1)
            folded = folded + piece
    mixed = folded + pltpu.roll(folded, HD, 1)
    mixed = mixed + own_weight * jnp.concatenate(
        [jnp.concatenate([new_values, new_values], axis=1)] * 2, axis=0
    )
    heads = jnp.where(low, mixed[0:pad, :], mixed[pad : 2 * pad, :]).astype(bf16)
    partial = jnp.dot(heads, wo[...], preferred_element_type=f32).astype(bf16)
    blocks = out.shape[0]
    cols = out.shape[2]
    for n in range(blocks):
        out[n] = partial[0:seq_rows, n * cols : (n + 1) * cols]


def attention_call(
    tokens,
    gain,
    wq,
    wk,
    wv,
    wf,
    bias,
    wo,
    keys,
    values,
    cumul,
    lengths,
    blocks,
):
    seq_rows, width = tokens.shape
    span = keys.shape[3]
    pad = 16
    chunk = 4 * HD
    count = -(-seq_rows * HD // chunk)
    vmem = pl.BlockSpec(memory_space=pltpu.VMEM)
    smem = pl.BlockSpec(memory_space=pltpu.SMEM)
    hbm = pl.BlockSpec(memory_space=pl.ANY)
    kernel = functools.partial(attention_kernel, seq_rows=seq_rows, pad=pad, chunk=chunk)
    return pl.pallas_call(
        kernel,
        out_shape=jax.ShapeDtypeStruct((blocks, seq_rows, width // blocks), jnp.bfloat16),
        in_specs=[smem, smem] + [vmem] * 8 + [hbm, hbm],
        out_specs=vmem,
        scratch_shapes=[
            pltpu.VMEM((seq_rows * HD, span), jnp.bfloat16),
            pltpu.VMEM((seq_rows * HD, span), jnp.bfloat16),
            pltpu.VMEM((2 * pad, span), jnp.float32),
            pltpu.VMEM((pad, width), jnp.float32),
            pltpu.SemaphoreType.DMA((count,)),
            pltpu.SemaphoreType.DMA((count,)),
        ],
        name="attention",
    )(
        lengths,
        bias,
        tokens,
        gain.reshape(1, width),
        wq,
        wk.T,
        wv.T,
        wf.T,
        wo,
        cumul,
        keys.reshape(seq_rows * HD, span),
        values.reshape(seq_rows * HD, span),
    )


def expert_kernel(rows, gain, wg, wu, wd, out):
    f32 = jnp.float32
    bf16 = jnp.bfloat16
    peers, count, cols = rows.shape
    blocks = peers // SLICES
    width = blocks * cols
    pieces = []
    squares = 0.0
    for n in range(blocks):
        piece = jnp.concatenate([rows[s * blocks + n] for s in range(SLICES)], axis=0).astype(f32)
        squares = squares + jnp.sum(piece * piece, axis=-1, keepdims=True)
        pieces.append(piece)
    inv = lax.rsqrt(squares / width + EPSILON)
    gate = 0.0
    up = 0.0
    for n in range(blocks):
        span = slice(n * cols, (n + 1) * cols)
        flat = (pieces[n] * inv * gain[:, span]).astype(bf16)
        gate = gate + jnp.dot(flat, wg[span, :], preferred_element_type=f32)
        up = up + jnp.dot(flat, wu[span, :], preferred_element_type=f32)
    hidden = (gate / (1.0 + jnp.exp(-gate)) * up).astype(bf16)
    for n in range(blocks):
        span = slice(n * cols, (n + 1) * cols)
        part = jnp.dot(hidden, wd[:, span], preferred_element_type=f32).astype(bf16)
        for s in range(SLICES):
            out[s * blocks + n] = part[s * count : (s + 1) * count, :]


def expert_call(rows, gain, wg, wu, wd):
    vmem = pl.BlockSpec(memory_space=pltpu.VMEM)
    return pl.pallas_call(
        expert_kernel,
        out_shape=jax.ShapeDtypeStruct(rows.shape, jnp.bfloat16),
        in_specs=[vmem] * 5,
        out_specs=vmem,
        name="expert",
    )(rows, gain.reshape(1, -1), wg, wu, wd)


def slot_tables(routes, route_weights, experts, capacity):
    seq_rows = routes.shape[0]
    expert = lax.broadcasted_iota(jnp.int32, (experts, 1, 1), 0)
    chosen = routes[None] == expert
    named = jnp.any(chosen, axis=2).astype(jnp.float32)
    share = jnp.sum(jnp.where(chosen, route_weights[None], 0.0), axis=2)
    first = lax.broadcasted_iota(jnp.int32, (seq_rows, seq_rows), 0)
    second = lax.broadcasted_iota(jnp.int32, (seq_rows, seq_rows), 1)
    earlier = jnp.dot(named, (first < second).astype(jnp.float32))
    slot = lax.broadcasted_iota(jnp.int32, (1, capacity, 1), 1).astype(jnp.float32)
    here = (earlier[:, None, :] == slot) & (named[:, None, :] > 0.0)
    place = here.astype(jnp.bfloat16).reshape(experts * capacity, seq_rows)
    weighted = jnp.where(here, share[:, None, :], 0.0).reshape(experts * capacity, seq_rows)
    return place, weighted.T


def body(
    tokens,
    attn_gain,
    query_weight,
    key_weight,
    value_weight,
    forget_weight,
    forget_bias,
    out_weight,
    key_cache,
    value_cache,
    cum_forget,
    lengths,
    ffn_gain,
    routes,
    route_weights,
    gate_weight,
    up_weight,
    down_weight,
):
    tp_count = lax.axis_size("tp")
    ep_count = lax.axis_size(EXPERT_AXES) * SLICES
    tp_rank = lax.axis_index("tp")
    seq_rows = tokens.shape[0]
    width = tokens.shape[1]
    cols = width // tp_count
    experts = ep_count // SLICES
    capacity = min(seq_rows, max(2, (2 * seq_rows * TOP_K + experts - 1) // experts))
    partial = attention_call(
        tokens,
        attn_gain,
        query_weight,
        key_weight,
        value_weight,
        forget_weight,
        forget_bias,
        out_weight,
        key_cache,
        value_cache,
        cum_forget,
        lengths,
        tp_count,
    )
    blocks = lax.all_to_all(partial, "tp", 0, 0, tiled=True)
    mixed_cols = jnp.sum(blocks.astype(jnp.float32), axis=0)
    token_f = tokens.astype(jnp.float32)
    token_cols = lax.dynamic_slice_in_dim(token_f, tp_rank * cols, cols, 1)
    residual_cols = (token_cols + mixed_cols).astype(jnp.bfloat16)
    place, weighted = slot_tables(routes, route_weights, experts, capacity)
    outgoing = jnp.dot(place, residual_cols, preferred_element_type=jnp.float32)
    outgoing = outgoing.astype(jnp.bfloat16).reshape(experts, capacity, cols)
    arrived = lax.all_to_all(outgoing, EXPERT_AXES, split_axis=0, concat_axis=0, tiled=True)
    arrived = arrived.reshape(experts * capacity, cols)
    gathered = copy_for_each(arrived, GROUP_AXES)
    part = expert_call(gathered, ffn_gain, gate_weight[0], up_weight[0], down_weight[0])
    parts = lax.all_to_all(part, GROUP_AXES, split_axis=0, concat_axis=0, tiled=True)
    summed = jnp.sum(parts.astype(jnp.float32), axis=0).astype(jnp.bfloat16)
    summed = summed.reshape(experts, capacity, cols)
    returned = lax.all_to_all(summed, EXPERT_AXES, split_axis=0, concat_axis=0, tiled=True)
    returned = returned.reshape(experts * capacity, cols).astype(jnp.float32)
    routed = jnp.dot(
        weighted, returned, precision=lax.Precision.HIGHEST, preferred_element_type=jnp.float32
    )
    return (residual_cols.astype(jnp.float32) + routed).astype(jnp.bfloat16)


def solution(mesh):
    half = mesh.shape["ep"] // (2 * SLICES)
    fine = Mesh(
        mesh.devices.reshape(half, 2, 2, 2, mesh.shape["tp"]), EP_AXES + ("tp",)
    )
    return jax.shard_map(
        body,
        mesh=fine,
        in_specs=(
            P(EP_AXES, None),
            P(),
            P(None, "tp"),
            P(None, "tp"),
            P(None, "tp"),
            P(None, "tp"),
            P("tp"),
            P("tp", None),
            P(EP_AXES, "tp", None, None),
            P(EP_AXES, "tp", None, None),
            P(EP_AXES, "tp", None),
            P(EP_AXES),
            P(),
            P(EP_AXES, None),
            P(EP_AXES, None),
            P(EP_AXES, None, "tp"),
            P(EP_AXES, None, "tp"),
            P(EP_AXES, "tp", None),
        ),
        out_specs=P(EP_AXES, "tp"),
        check_vma=False,
    )
```

time: 106 us -> 101 us (0.953)
  blocking collectives: 31.2 us -> 48.1 us
  waiting for transfers between devices: 37.4 us -> 27.1 us
  Pallas kernels: 0 us -> 8.74 us
  starting transfers between devices: 19.6 us -> 12.8 us
  local copies, waits for them, and re-layouts: 7.45 us -> 1.25 us
  matrix products: 5.6 us -> 1.19 us
  other arithmetic: 3.45 us -> 1.11 us
    all_to_all x0 -> x1, blocking collectives: none -> 16.9 us  [copy_for_each(): return lax.all_to_all(copies, axis, split_axis=0, concat_axis=0, tiled=True)]
    all_to_all x2 -> x1, waiting for transfers between devices: 13.8 us -> 3.61 us  [body(): blocks = lax.all_to_all(partial, 'tp', 0, 0, tiled=True)]
    pallas_call x0 -> x2, Pallas kernels: none -> 8.74 us  [the longest x1 5.83 us: attention_call(): pl.pallas_call(kernel, out_shape=jax.ShapeDtypeStruct((blocks, seq_rows,...]
    all_to_all x2 -> x1, starting transfers between devices: 11.9 us -> 5.01 us  [body(): blocks = lax.all_to_all(partial, 'tp', 0, 0, tiled=True)]
    dot_general x10 -> x0, matrix products: 4.4 us -> none  [the longest x1 2.07 us: body(): jnp.einsum('bkgl,bkdl->bkgd', attn_weights, value_cache, preferred_elemen...]
    gather x4 -> x0, local copies, waits for them, and re-layouts: 2.21 us -> none  [body(): last = jnp.take_along_axis(cumul, last_index, axis=3)]
    reshape x5 -> x0, local copies, waits for them, and re-layouts: 1.99 us -> none  [the longest x2 1.25 us: body(): part.astype(jnp.bfloat16)]
    lt x2 -> x0, other arithmetic: 1.39 us -> none  [the longest x1 0.73 us: body(): valid = positions < lengths[:, None, None, None]]
  transfers between devices with their start and end apart: 4 -> 3, of which waited for: 4 -> 3; matrix products, arithmetic and copies ran while one was open for 1% -> 1% of each run, Pallas kernels for 0% -> 0%
where the time goes in v2:
time: 101 us; the launch traced here: 100 us
  blocking collectives  48.1 us (48%)
  waiting for transfers between devices  27.1 us (27%)
  starting transfers between devices  12.8 us (13%)
  Pallas kernels  8.74 us (9%)
  local copies, waits for them, and re-layouts  1.25 us (1%)
  matrix products  1.19 us (1%)
  other arithmetic  1.11 us (1%)
    all_to_all x1, blocking collectives, body(): lax.all_to_all(outgoing, EXPERT_AXES, split_axis=0, concat_axis=0, tiled=...  31.2 us
    all_to_all x1, blocking collectives, copy_for_each(): return lax.all_to_all(copies, axis, split_axis=0, concat_axis=0, tiled=True)  16.9 us
    all_to_all x1, waiting for transfers between devices, body(): lax.all_to_all(summed, EXPERT_AXES, split_axis=0, concat_axis=0, tiled=True)  13.6 us
    all_to_all x1, waiting for transfers between devices, body(): lax.all_to_all(part, GROUP_AXES, split_axis=0, concat_axis=0, tiled=True)  9.95 us
    pallas_call x1, Pallas kernels, attention_call(): pl.pallas_call(kernel, out_shape=jax.ShapeDtypeStruct((blocks, seq_rows,...  5.83 us
    all_to_all x1, starting transfers between devices, body(): blocks = lax.all_to_all(partial, 'tp', 0, 0, tiled=True)  5.01 us
    all_to_all x1, starting transfers between devices, body(): lax.all_to_all(part, GROUP_AXES, split_axis=0, concat_axis=0, tiled=True)  3.92 us
    all_to_all x1, starting transfers between devices, body(): lax.all_to_all(summed, EXPERT_AXES, split_axis=0, concat_axis=0, tiled=True)  3.85 us
  transfers between devices with their start and end apart: 3, of which 3 were waited for; matrix products, arithmetic and copies ran while one was open for 1% of the time, Pallas kernels for 0%

profile of v2, /device:TPU:1, one launch (start us, length us, event | category | flops | bytes accessed | tf_op | source)
XLA Modules:
  0.0 100.4 jit_solution(1717776565049382417)
XLA Ops:
  0.0 5.8 %attention.1 = bf16[4,13,256]{2,1,0:T(8,128)(2,1)} custom-call(s32[13]{0:T(128)} %lengths.1, f32[2]{0:T(128)} %bias.1, bf16[13,1024]{1,0:T(8,128)(2,1)} %tokens.1, f32[1,1024]{1,0:T(1,128)} %bitcast.27, bf16[1024,128]{1,0:T(8,128)(2,1)} %wq.1, bf16[64,1024]{1,0:T(8,128)(2,1)} %bitcast.24, bf16[64,1024]{1,0:T(8,128)(2,1)} %bitcast.25, ...), custom_call_target="tpu_custom_call" | custom-call | tf_op jit(solution)/shard_map/attention/pallas_call | solution.py:193
  5.8 5.0 %all-to-all-start = ((bf16[4,13,256]{2,1,0:T(8,128)(2,1)}), bf16[4,13,256]{2,1,0:T(8,128)(2,1)S(1)}, u32[]{:S(2)}, u32[]{:S(2)}) async-start(bf16[4,13,256]{2,1,0:T(8,128)(2,1)} %attention.1), calls=%async_computation | async-start | bytes 65536 | tf_op jit(solution)/shard_map/all_to_all | solution.py:321
  10.9 0.1 copy.31
  11.0 0.1 fusion.7
  11.1 0.2 fusion.8
  11.3 0.1 copy.34
  11.4 0.1 eq.45
  11.6 3.6 %all-to-all-done = bf16[4,13,256]{2,1,0:T(8,128)(2,1)S(1)} async-done(((bf16[4,13,256]{2,1,0:T(8,128)(2,1)}), bf16[4,13,256]{2,1,0:T(8,128)(2,1)S(1)}, u32[]{:S(2)}, u32[]{:S(2)}) %all-to-all-start) | async-done | bytes 26656 | tf_op jit(solution)/shard_map/all_to_all | solution.py:321
  15.2 0.7 add_convert_fusion
  15.9 0.2 convolution_convert_fusion
  16.1 31.2 %all_to_all.25 = bf16[32,2,256]{2,1,0:T(2,128)(2,1)S(1)} all-to-all(bf16[32,2,256]{2,1,0:T(2,128)(2,1)S(1)} %reshape.44), channel_id=1, replica_groups=mesh['z'=16,'xh'=2,'xl'=2,'core'=2,'tp'=4] {'z','xh'}, dimensions={0} | all-to-all | bytes 65536 | tf_op jit(solution)/shard_map/all_to_all | solution.py:329
  47.4 16.9 %all_to_all.26.rows = bf16[16,64,256]{2,1,0:T(8,128)(2,1)} all-to-all(bf16[16,64,256]{2,1,0:T(8,128)(2,1)S(1)} %broadcast_in_dim.36), channel_id=1, replica_groups=mesh['z'=16,'xh'=2,'xl'=2,'core'=2,'tp'=4] {'xl','core','tp'}, dimensions={0} | all-to-all | bytes 1048576 | tf_op jit(solution)/shard_map/all_to_all | solution.py:28
  64.3 2.9 %expert.1 = bf16[16,64,256]{2,1,0:T(8,128)(2,1)} custom-call(bf16[16,64,256]{2,1,0:T(8,128)(2,1)} %all_to_all.26.rows, f32[1,1024]{1,0:T(1,128)} %bitcast.29, bf16[1024,128]{1,0:T(8,128)(2,1)} %bitcast.21, bf16[1024,128]{1,0:T(8,128)(2,1)} %bitcast.22, bf16[128,1024]{1,0:T(8,128)(2,1)} %bitcast.23), custom_call_target="tpu_custom_call" | custom-call | tf_op jit(solution)/shard_map/expert/pallas_call | solution.py:253
  67.2 3.9 %all-to-all-start.3 = ((bf16[16,64,256]{2,1,0:T(8,128)(2,1)}), bf16[16,64,256]{2,1,0:T(8,128)(2,1)S(1)}, u32[]{:S(2)}, u32[]{:S(2)}) async-start(bf16[16,64,256]{2,1,0:T(8,128)(2,1)} %expert.1), calls=%async_computation.3 | async-start | bytes 1048576 | tf_op jit(solution)/shard_map/all_to_all | solution.py:333
  71.1 0.1 copy.35
  71.2 0.1 select_reduce_fusion
  71.3 0.1 copy.36
  71.4 9.9 %all-to-all-done.3 = bf16[16,64,256]{2,1,0:T(8,128)(2,1)S(1)} async-done(((bf16[16,64,256]{2,1,0:T(8,128)(2,1)}), bf16[16,64,256]{2,1,0:T(8,128)(2,1)S(1)}, u32[]{:S(2)}, u32[]{:S(2)}) %all-to-all-start.3) | async-done | bytes 524320 | tf_op jit(solution)/shard_map/all_to_all | solution.py:333
  81.4 0.1 reduce_sum.32
  81.5 0.6 reshape.47
  82.1 3.9 %all-to-all-start.4 = ((bf16[32,2,256]{2,1,0:T(2,128)(2,1)}), bf16[32,2,256]{2,1,0:T(2,128)(2,1)S(1)}, u32[]{:S(2)}, u32[]{:S(2)}) async-start(bf16[32,2,256]{2,1,0:T(2,128)(2,1)} %reshape.47), calls=%async_computation.4 | async-start | bytes 65536 | tf_op jit(solution)/shard_map/all_to_all | solution.py:336
  85.9 0.1 and_select_fusion
  86.0 13.6 %all-to-all-done.4 = bf16[32,2,256]{2,1,0:T(2,128)(2,1)S(1)} async-done(((bf16[32,2,256]{2,1,0:T(2,128)(2,1)}), bf16[32,2,256]{2,1,0:T(2,128)(2,1)S(1)}, u32[]{:S(2)}, u32[]{:S(2)}) %all-to-all-start.4) | async-done | bytes 32800 | tf_op jit(solution)/shard_map/all_to_all | solution.py:336
  99.6 0.8 fusion.1
  (14 shorter events, 0.2 us)
Async XLA Ops:
  0.0 10.9 %copy-start = (s32[13,2]{0,1:T(2,128)S(1)}, s32[13,2]{0,1:T(2,128)}, u32[]{:S(2)}) copy-start(s32[13,2]{0,1:T(2,128)} %param.31) | copy-start | bytes 316
  5.8 9.3 %all-to-all-start = ((bf16[4,13,256]{2,1,0:T(8,128)(2,1)}), bf16[4,13,256]{2,1,0:T(8,128)(2,1)S(1)}, u32[]{:S(2)}, u32[]{:S(2)}) async-start(bf16[4,13,256]{2,1,0:T(8,128)(2,1)} %attention.1), calls=%async_computation | async-start | bytes 65536 | tf_op jit(solution)/shard_map/all_to_all | solution.py:321
  64.3 6.8 %copy-start.1 = (f32[13,2]{0,1:T(2,128)S(1)}, f32[13,2]{0,1:T(2,128)}, u32[]{:S(2)}) copy-start(f32[13,2]{0,1:T(2,128)} %param.32) | copy-start | bytes 316
  67.2 14.2 %all-to-all-start.3 = ((bf16[16,64,256]{2,1,0:T(8,128)(2,1)}), bf16[16,64,256]{2,1,0:T(8,128)(2,1)S(1)}, u32[]{:S(2)}, u32[]{:S(2)}) async-start(bf16[16,64,256]{2,1,0:T(8,128)(2,1)} %expert.1), calls=%async_computation.3 | async-start | bytes 1048576 | tf_op jit(solution)/shard_map/all_to_all | solution.py:333
  82.1 17.5 %all-to-all-start.4 = ((bf16[32,2,256]{2,1,0:T(2,128)(2,1)}), bf16[32,2,256]{2,1,0:T(2,128)(2,1)S(1)}, u32[]{:S(2)}, u32[]{:S(2)}) async-start(bf16[32,2,256]{2,1,0:T(2,128)(2,1)} %reshape.47), calls=%async_computation.4 | async-start | bytes 65536 | tf_op jit(solution)/shard_map/all_to_all | solution.py:336

commit v3 on v2

--- a/solution.py
+++ b/solution.py
@@ -20,7 +20,7 @@
 EXPERT_AXES = ("z", "xh")
 SLICE_AXES = ("xl", "core")
 EP_AXES = EXPERT_AXES + SLICE_AXES
-GROUP_AXES = SLICE_AXES + ("tp",)
+GROUP_AXES = ("xl", "tp")
 
 
 def copy_for_each(shard, axis):
@@ -41,13 +41,18 @@
     cumul,
     keys,
     values,
+    wg,
+    wu,
+    wd,
     out,
+    pack,
     key_buf,
     value_buf,
     cum_rows,
     token_rows,
     key_sems,
     value_sems,
+    pack_sems,
     *,
     seq_rows,
     pad,
@@ -70,7 +75,19 @@
 
     key_copies = copies(keys, key_buf, key_sems)
     value_copies = copies(values, value_buf, value_sems)
-    for copy in key_copies + value_copies:
+    units = wg.shape[1]
+    pack_copies = [
+        pltpu.make_async_copy(wg, pack.at[0], pack_sems.at[0]),
+        pltpu.make_async_copy(wu, pack.at[1], pack_sems.at[1]),
+    ] + [
+        pltpu.make_async_copy(
+            wd.at[:, pl.ds(j * units, units)],
+            pack.at[2, pl.ds(j * units, units), :],
+            pack_sems.at[2 + j],
+        )
+        for j in range(wd.shape[1] // units)
+    ]
+    for copy in key_copies + value_copies + pack_copies:
         copy.start()
 
     f32 = jnp.float32
@@ -164,6 +181,8 @@
     cols = out.shape[2]
     for n in range(blocks):
         out[n] = partial[0:seq_rows, n * cols : (n + 1) * cols]
+    for copy in pack_copies:
+        copy.wait()
 
 
 def attention_call(
@@ -179,6 +198,9 @@
     values,
     cumul,
     lengths,
+    wg,
+    wu,
+    wd,
     blocks,
 ):
     seq_rows, width = tokens.shape
@@ -192,9 +214,12 @@
     kernel = functools.partial(attention_kernel, seq_rows=seq_rows, pad=pad, chunk=chunk)
     return pl.pallas_call(
         kernel,
-        out_shape=jax.ShapeDtypeStruct((blocks, seq_rows, width // blocks), jnp.bfloat16),
-        in_specs=[smem, smem] + [vmem] * 8 + [hbm, hbm],
-        out_specs=vmem,
+        out_shape=(
+            jax.ShapeDtypeStruct((blocks, seq_rows, width // blocks), jnp.bfloat16),
+            jax.ShapeDtypeStruct((3,) + wg.shape, jnp.bfloat16),
+        ),
+        in_specs=[smem, smem] + [vmem] * 8 + [hbm] * 5,
+        out_specs=(vmem, hbm),
         scratch_shapes=[
             pltpu.VMEM((seq_rows * HD, span), jnp.bfloat16),
             pltpu.VMEM((seq_rows * HD, span), jnp.bfloat16),
@@ -202,6 +227,7 @@
             pltpu.VMEM((pad, width), jnp.float32),
             pltpu.SemaphoreType.DMA((count,)),
             pltpu.SemaphoreType.DMA((count,)),
+            pltpu.SemaphoreType.DMA((2 + width // wg.shape[1],)),
         ],
         name="attention",
     )(
@@ -217,46 +243,88 @@
         cumul,
         keys.reshape(seq_rows * HD, span),
         values.reshape(seq_rows * HD, span),
-    )
-
-
-def expert_kernel(rows, gain, wg, wu, wd, out):
+        wg,
+        wu,
+        wd,
+    )
+
+
+def expert_kernel(
+    rows, gain, own, other, out, row_buf, own_buf, other_buf, row_sem, own_sems, other_sems
+):
     f32 = jnp.float32
     bf16 = jnp.bfloat16
     peers, count, cols = rows.shape
-    blocks = peers // SLICES
-    width = blocks * cols
+    width = gain.shape[1]
+    blocks = width // cols
+    groups = peers // blocks
+    units = own.shape[2]
+    row_copy = pltpu.make_async_copy(rows, row_buf, row_sem)
+    row_copy.start()
+    own_copies = [pltpu.make_async_copy(own.at[i], own_buf.at[i], own_sems.at[i]) for i in range(3)]
+    other_copies = [
+        pltpu.make_async_copy(other.at[i], other_buf.at[i], other_sems.at[i]) for i in range(3)
+    ]
+    for i in range(3):
+        own_copies[i].start()
+        other_copies[i].start()
+    row_copy.wait()
     pieces = []
     squares = 0.0
     for n in range(blocks):
-        piece = jnp.concatenate([rows[s * blocks + n] for s in range(SLICES)], axis=0).astype(f32)
+        piece = jnp.concatenate([row_buf[s * blocks + n] for s in range(groups)], axis=0)
+        piece = piece.astype(f32)
         squares = squares + jnp.sum(piece * piece, axis=-1, keepdims=True)
         pieces.append(piece)
     inv = lax.rsqrt(squares / width + EPSILON)
-    gate = 0.0
-    up = 0.0
+    flats = [
+        (pieces[n] * inv * gain[:, n * cols : (n + 1) * cols]).astype(bf16) for n in range(blocks)
+    ]
+
+    def projected(i):
+        own_copies[i].wait()
+        other_copies[i].wait()
+        total = 0.0
+        for n in range(blocks):
+            span = slice(n * cols, (n + 1) * cols)
+            weight = jnp.concatenate([own_buf[i, span, :], other_buf[i, span, :]], axis=1)
+            total = total + jnp.dot(flats[n], weight, preferred_element_type=f32)
+        return total
+
+    gate = projected(0)
+    up = projected(1)
+    hidden = (gate / (1.0 + jnp.exp(-gate)) * up).astype(bf16)
+    own_copies[2].wait()
+    other_copies[2].wait()
     for n in range(blocks):
-        span = slice(n * cols, (n + 1) * cols)
-        flat = (pieces[n] * inv * gain[:, span]).astype(bf16)
-        gate = gate + jnp.dot(flat, wg[span, :], preferred_element_type=f32)
-        up = up + jnp.dot(flat, wu[span, :], preferred_element_type=f32)
-    hidden = (gate / (1.0 + jnp.exp(-gate)) * up).astype(bf16)
-    for n in range(blocks):
-        span = slice(n * cols, (n + 1) * cols)
-        part = jnp.dot(hidden, wd[:, span], preferred_element_type=f32).astype(bf16)
-        for s in range(SLICES):
+        strips = []
+        for j in range(n * cols // units, (n + 1) * cols // units):
+            span = slice(j * units, (j + 1) * units)
+            strips.append(jnp.concatenate([own_buf[2, span, :], other_buf[2, span, :]], axis=0))
+        weight = jnp.concatenate(strips, axis=1)
+        part = jnp.dot(hidden, weight, preferred_element_type=f32).astype(bf16)
+        for s in range(groups):
             out[s * blocks + n] = part[s * count : (s + 1) * count, :]
 
 
-def expert_call(rows, gain, wg, wu, wd):
+def expert_call(rows, gain, own, other):
     vmem = pl.BlockSpec(memory_space=pltpu.VMEM)
+    hbm = pl.BlockSpec(memory_space=pl.ANY)
     return pl.pallas_call(
         expert_kernel,
         out_shape=jax.ShapeDtypeStruct(rows.shape, jnp.bfloat16),
-        in_specs=[vmem] * 5,
+        in_specs=[hbm, vmem, hbm, hbm],
         out_specs=vmem,
+        scratch_shapes=[
+            pltpu.VMEM(rows.shape, jnp.bfloat16),
+            pltpu.VMEM(own.shape, jnp.bfloat16),
+            pltpu.VMEM(own.shape, jnp.bfloat16),
+            pltpu.SemaphoreType.DMA,
+            pltpu.SemaphoreType.DMA((3,)),
+            pltpu.SemaphoreType.DMA((3,)),
+        ],
         name="expert",
-    )(rows, gain.reshape(1, -1), wg, wu, wd)
+    )(rows, gain.reshape(1, -1), own, other)
 
 
 def slot_tables(routes, route_weights, experts, capacity):
@@ -303,7 +371,7 @@
     cols = width // tp_count
     experts = ep_count // SLICES
     capacity = min(seq_rows, max(2, (2 * seq_rows * TOP_K + experts - 1) // experts))
-    partial = attention_call(
+    partial, own_pack = attention_call(
         tokens,
         attn_gain,
         query_weight,
@@ -316,8 +384,12 @@
         value_cache,
         cum_forget,
         lengths,
+        gate_weight[0],
+        up_weight[0],
+        down_weight[0],
         tp_count,
     )
+    other_pack = lax.ppermute(own_pack, "core", [(0, 1), (1, 0)])
     blocks = lax.all_to_all(partial, "tp", 0, 0, tiled=True)
     mixed_cols = jnp.sum(blocks.astype(jnp.float32), axis=0)
     token_f = tokens.astype(jnp.float32)
@@ -328,8 +400,9 @@
     outgoing = outgoing.astype(jnp.bfloat16).reshape(experts, capacity, cols)
     arrived = lax.all_to_all(outgoing, EXPERT_AXES, split_axis=0, concat_axis=0, tiled=True)
     arrived = arrived.reshape(experts * capacity, cols)
+    arrived, other_pack = lax.optimization_barrier((arrived, other_pack))
     gathered = copy_for_each(arrived, GROUP_AXES)
-    part = expert_call(gathered, ffn_gain, gate_weight[0], up_weight[0], down_weight[0])
+    part = expert_call(gathered, ffn_gain, own_pack, other_pack)
     parts = lax.all_to_all(part, GROUP_AXES, split_axis=0, concat_axis=0, tiled=True)
     summed = jnp.sum(parts.astype(jnp.float32), axis=0).astype(jnp.bfloat16)
     summed = summed.reshape(experts, capacity, cols)

time: 101 us -> 115 us (1.14)
  the two profiles are of different devices: /device:TPU:1 before, /device:TPU:2 now
where the time goes in v3:
time: 115 us; the launch traced here: 114 us
  blocking collectives  42.1 us (37%)
  Pallas kernels  30.7 us (27%)
  waiting for transfers between devices  23.1 us (20%)
  starting transfers between devices  15 us (13%)
  local copies, waits for them, and re-layouts  1.23 us (1%)
  matrix products  1.2 us (1%)
    all_to_all x1, blocking collectives, body(): lax.all_to_all(outgoing, EXPERT_AXES, split_axis=0, concat_axis=0, tiled=...  31.8 us
    pallas_call x1, Pallas kernels, attention_call(): pl.pallas_call(kernel, out_shape=(jax.ShapeDtypeStruct((blocks, seq_rows,...  26.9 us
    all_to_all x1, waiting for transfers between devices, body(): lax.all_to_all(summed, EXPERT_AXES, split_axis=0, concat_axis=0, tiled=True)  14.7 us
    all_to_all x1, blocking collectives, copy_for_each(): return lax.all_to_all(copies, axis, split_axis=0, concat_axis=0, tiled=True)  10.3 us
    all_to_all x1, waiting for transfers between devices, body(): lax.all_to_all(part, GROUP_AXES, split_axis=0, concat_axis=0, tiled=True)  5.55 us
    all_to_all x1, starting transfers between devices, body(): lax.all_to_all(part, GROUP_AXES, split_axis=0, concat_axis=0, tiled=True)  4.75 us
    all_to_all x1, starting transfers between devices, body(): blocks = lax.all_to_all(partial, 'tp', 0, 0, tiled=True)  4.48 us
    all_to_all x1, starting transfers between devices, body(): lax.all_to_all(summed, EXPERT_AXES, split_axis=0, concat_axis=0, tiled=True)  3.85 us
  transfers between devices with their start and end apart: 4, of which 3 were waited for; matrix products, arithmetic and copies ran while one was open for 2% of the time, Pallas kernels for 0%

profile of v3, /device:TPU:2, one launch (start us, length us, event | category | flops | bytes accessed | tf_op | source)
XLA Modules:
  0.0 114.5 jit_solution(5300702407806933333)
XLA Ops:
  0.0 26.9 %attention.1 = (bf16[4,13,256]{2,1,0:T(8,128)(2,1)}, bf16[3,1024,128]{2,1,0:T(8,128)(2,1)}) custom-call(s32[13]{0:T(128)} %lengths.1, f32[2]{0:T(128)} %bias.1, bf16[13,1024]{1,0:T(8,128)(2,1)} %tokens.1, f32[1,1024]{1,0:T(1,128)} %bitcast.28, bf16[1024,128]{1,0:T(8,128)(2,1)} %wq.1, bf16[64,1024]{1,0:T(8,128)(2,1)} %bitcast.24, bf16[64,1024]{1,0:T(8,128)(2,1)} %bitcast.25, ...), custom_call_target="tpu_custom_call" | custom-call | tf_op jit(solution)/shard_map/attention/pallas_call | solution.py:215
  27.0 4.5 %all-to-all-start = ((bf16[4,13,256]{2,1,0:T(8,128)(2,1)}), bf16[4,13,256]{2,1,0:T(8,128)(2,1)S(1)}, u32[]{:S(2)}, u32[]{:S(2)}) async-start(bf16[4,13,256]{2,1,0:T(8,128)(2,1)} %get-tuple-element.9), calls=%async_computation | async-start | bytes 65536 | tf_op jit(solution)/shard_map/all_to_all | solution.py:393
  31.4 1.9 %collective-permute-start = (bf16[3,1024,128]{2,1,0:T(8,128)(2,1)}, bf16[3,1024,128]{2,1,0:T(8,128)(2,1)S(1)}, u32[]{:S(2)}, u32[]{:S(2)}) collective-permute-start(bf16[3,1024,128]{2,1,0:T(8,128)(2,1)} %get-tuple-element.10.own), channel_id=1, source_target_pairs={{0,4},{4,0},{1,5},{5,1},{2,6},{6,2},{3,7},{7,3},{8,12},{12,8},{9,1... | collective-permute-start | bytes 2359304 | tf_op jit(solution)/shard_map/ppermute | solution.py:392
  33.4 0.1 copy.31
  33.5 0.1 fusion.7
  33.6 0.2 fusion.8
  33.8 0.1 copy.34
  33.9 0.1 eq.45
  34.0 2.8 %all-to-all-done = bf16[4,13,256]{2,1,0:T(8,128)(2,1)S(1)} async-done(((bf16[4,13,256]{2,1,0:T(8,128)(2,1)}), bf16[4,13,256]{2,1,0:T(8,128)(2,1)S(1)}, u32[]{:S(2)}, u32[]{:S(2)}) %all-to-all-start) | async-done | bytes 26656 | tf_op jit(solution)/shard_map/all_to_all | solution.py:393
  36.9 0.7 add_convert_fusion
  37.6 0.2 convolution_convert_fusion
  37.8 31.8 %all_to_all.25 = bf16[32,2,256]{2,1,0:T(2,128)(2,1)S(1)} all-to-all(bf16[32,2,256]{2,1,0:T(2,128)(2,1)S(1)} %reshape.44), channel_id=1, replica_groups=mesh['z'=16,'xh'=2,'xl'=2,'core'=2,'tp'=4] {'z','xh'}, dimensions={0} | all-to-all | bytes 65536 | tf_op jit(solution)/shard_map/all_to_all | solution.py:401
  69.7 10.3 %all_to_all.26.rows = bf16[8,64,256]{2,1,0:T(8,128)(2,1)} all-to-all(bf16[8,64,256]{2,1,0:T(8,128)(2,1)S(1)} %broadcast_in_dim.36), channel_id=1, replica_groups=mesh['z'=16,'xh'=2,'xl'=2,'core'=2,'tp'=4] {'xl','tp'}, dimensions={0} | all-to-all | bytes 524288 | tf_op jit(solution)/shard_map/all_to_all | solution.py:28
  80.0 3.7 %expert.1 = bf16[8,64,256]{2,1,0:T(8,128)(2,1)} custom-call(bf16[8,64,256]{2,1,0:T(8,128)(2,1)} %all_to_all.26.rows, f32[1,1024]{1,0:T(1,128)} %bitcast.27, bf16[3,1024,128]{2,1,0:T(8,128)(2,1)} %get-tuple-element.10.own, bf16[3,1024,128]{2,1,0:T(8,128)(2,1)} %copy-done), custom_call_target="tpu_custom_call" | custom-call | tf_op jit(solution)/shard_map/expert/pallas_call | solution.py:313
  83.7 4.7 %all-to-all-start.3 = ((bf16[8,64,256]{2,1,0:T(8,128)(2,1)}), bf16[8,64,256]{2,1,0:T(8,128)(2,1)S(1)}, u32[]{:S(2)}, u32[]{:S(2)}) async-start(bf16[8,64,256]{2,1,0:T(8,128)(2,1)} %expert.1), calls=%async_computation.3 | async-start | bytes 524288 | tf_op jit(solution)/shard_map/all_to_all | solution.py:406
  88.5 0.1 copy.35
  88.6 0.1 select_reduce_fusion
  88.7 0.1 copy.36
  88.8 5.6 %all-to-all-done.3 = bf16[8,64,256]{2,1,0:T(8,128)(2,1)S(1)} async-done(((bf16[8,64,256]{2,1,0:T(8,128)(2,1)}), bf16[8,64,256]{2,1,0:T(8,128)(2,1)S(1)}, u32[]{:S(2)}, u32[]{:S(2)}) %all-to-all-start.3) | async-done | bytes 262176 | tf_op jit(solution)/shard_map/all_to_all | solution.py:406
  94.4 0.6 reshape.47
  95.0 3.9 %all-to-all-start.4 = ((bf16[32,2,256]{2,1,0:T(2,128)(2,1)}), bf16[32,2,256]{2,1,0:T(2,128)(2,1)S(1)}, u32[]{:S(2)}, u32[]{:S(2)}) async-start(bf16[32,2,256]{2,1,0:T(2,128)(2,1)} %reshape.47), calls=%async_computation.4 | async-start | bytes 65536 | tf_op jit(solution)/shard_map/all_to_all | solution.py:409
  98.8 0.1 and_select_fusion
  98.9 14.7 %all-to-all-done.4 = bf16[32,2,256]{2,1,0:T(2,128)(2,1)S(1)} async-done(((bf16[32,2,256]{2,1,0:T(2,128)(2,1)}), bf16[32,2,256]{2,1,0:T(2,128)(2,1)S(1)}, u32[]{:S(2)}, u32[]{:S(2)}) %all-to-all-start.4) | async-done | bytes 32800 | tf_op jit(solution)/shard_map/all_to_all | solution.py:409
  113.7 0.8 fusion.1
  (18 shorter events, 0.2 us)
Async XLA Ops:
  0.0 33.3 %copy-start.1 = (s32[13,2]{0,1:T(2,128)S(1)}, s32[13,2]{0,1:T(2,128)}, u32[]{:S(2)}) copy-start(s32[13,2]{0,1:T(2,128)} %param.31) | copy-start | bytes 316
  27.0 9.9 %all-to-all-start = ((bf16[4,13,256]{2,1,0:T(8,128)(2,1)}), bf16[4,13,256]{2,1,0:T(8,128)(2,1)S(1)}, u32[]{:S(2)}, u32[]{:S(2)}) async-start(bf16[4,13,256]{2,1,0:T(8,128)(2,1)} %get-tuple-element.9), calls=%async_computation | async-start | bytes 65536 | tf_op jit(solution)/shard_map/all_to_all | solution.py:393
  31.4 38.2 %collective-permute-start = (bf16[3,1024,128]{2,1,0:T(8,128)(2,1)}, bf16[3,1024,128]{2,1,0:T(8,128)(2,1)S(1)}, u32[]{:S(2)}, u32[]{:S(2)}) collective-permute-start(bf16[3,1024,128]{2,1,0:T(8,128)(2,1)} %get-tuple-element.10.own), channel_id=1, source_target_pairs={{0,4},{4,0},{1,5},{5,1},{2,6},{6,2},{3,7},{7,3},{8,12},{12,8},{9,1... | collective-permute-start | bytes 2359304 | tf_op jit(solution)/shard_map/ppermute | solution.py:392
  69.6 18.9 %copy-start.2 = (f32[13,2]{0,1:T(2,128)S(1)}, f32[13,2]{0,1:T(2,128)}, u32[]{:S(2)}) copy-start(f32[13,2]{0,1:T(2,128)} %param.32) | copy-start | bytes 316
  69.6 10.4 %copy-start = (bf16[3,1024,128]{2,1,0:T(8,128)(2,1)}, bf16[3,1024,128]{2,1,0:T(8,128)(2,1)S(1)}, u32[]{:S(2)}) copy-start(bf16[3,1024,128]{2,1,0:T(8,128)(2,1)S(1)} %collective-permute-done.other) | copy-start | bytes 2359300
  83.7 10.6 %all-to-all-start.3 = ((bf16[8,64,256]{2,1,0:T(8,128)(2,1)}), bf16[8,64,256]{2,1,0:T(8,128)(2,1)S(1)}, u32[]{:S(2)}, u32[]{:S(2)}) async-start(bf16[8,64,256]{2,1,0:T(8,128)(2,1)} %expert.1), calls=%async_computation.3 | async-start | bytes 524288 | tf_op jit(solution)/shard_map/all_to_all | solution.py:406
  95.0 18.7 %all-to-all-start.4 = ((bf16[32,2,256]{2,1,0:T(2,128)(2,1)}), bf16[32,2,256]{2,1,0:T(2,128)(2,1)S(1)}, u32[]{:S(2)}, u32[]{:S(2)}) async-start(bf16[32,2,256]{2,1,0:T(2,128)(2,1)} %reshape.47), calls=%async_computation.4 | async-start | bytes 65536 | tf_op jit(solution)/shard_map/all_to_all | solution.py:409

commit v4 on v3

--- a/solution.py
+++ b/solution.py
@@ -48,6 +48,7 @@
     pack,
     key_buf,
     value_buf,
+    pack_buf,
     cum_rows,
     token_rows,
     key_sems,
@@ -76,18 +77,19 @@
     key_copies = copies(keys, key_buf, key_sems)
     value_copies = copies(values, value_buf, value_sems)
     units = wg.shape[1]
-    pack_copies = [
-        pltpu.make_async_copy(wg, pack.at[0], pack_sems.at[0]),
-        pltpu.make_async_copy(wu, pack.at[1], pack_sems.at[1]),
+    pack_loads = [
+        pltpu.make_async_copy(wg, pack_buf.at[0], pack_sems.at[0]),
+        pltpu.make_async_copy(wu, pack_buf.at[1], pack_sems.at[1]),
     ] + [
         pltpu.make_async_copy(
             wd.at[:, pl.ds(j * units, units)],
-            pack.at[2, pl.ds(j * units, units), :],
+            pack_buf.at[2, pl.ds(j * units, units), :],
             pack_sems.at[2 + j],
         )
         for j in range(wd.shape[1] // units)
     ]
-    for copy in key_copies + value_copies + pack_copies:
+    pack_store = pltpu.make_async_copy(pack_buf, pack, pack_sems.at[len(pack_loads)])
+    for copy in key_copies + value_copies + pack_loads:
         copy.start()
 
     f32 = jnp.float32
@@ -142,6 +144,10 @@
         left = jnp.where(seq == row_seq, left, 0.0).astype(bf16)
         key_copies[i].wait()
         scores = scores + jnp.dot(left, key_buf[r : r + size, :], preferred_element_type=f32)
+
+    for copy in pack_loads:
+        copy.wait()
+    pack_store.start()
 
     limit = jnp.zeros((2 * pad, 1), jnp.int32)
     for b in range(seq_rows):
@@ -181,8 +187,7 @@
     cols = out.shape[2]
     for n in range(blocks):
         out[n] = partial[0:seq_rows, n * cols : (n + 1) * cols]
-    for copy in pack_copies:
-        copy.wait()
+    pack_store.wait()
 
 
 def attention_call(
@@ -223,11 +228,12 @@
         scratch_shapes=[
             pltpu.VMEM((seq_rows * HD, span), jnp.bfloat16),
             pltpu.VMEM((seq_rows * HD, span), jnp.bfloat16),
+            pltpu.VMEM((3,) + wg.shape, jnp.bfloat16),
             pltpu.VMEM((2 * pad, span), jnp.float32),
             pltpu.VMEM((pad, width), jnp.float32),
             pltpu.SemaphoreType.DMA((count,)),
             pltpu.SemaphoreType.DMA((count,)),
-            pltpu.SemaphoreType.DMA((2 + width // wg.shape[1],)),
+            pltpu.SemaphoreType.DMA((3 + width // wg.shape[1],)),
         ],
         name="attention",
     )(
@@ -392,8 +398,8 @@
     other_pack = lax.ppermute(own_pack, "core", [(0, 1), (1, 0)])
     blocks = lax.all_to_all(partial, "tp", 0, 0, tiled=True)
     mixed_cols = jnp.sum(blocks.astype(jnp.float32), axis=0)
-    token_f = tokens.astype(jnp.float32)
-    token_cols = lax.dynamic_slice_in_dim(token_f, tp_rank * cols, cols, 1)
+    token_cols = lax.dynamic_slice_in_dim(tokens, tp_rank * cols, cols, 1)
+    token_cols = lax.optimization_barrier(token_cols).astype(jnp.float32)
     residual_cols = (token_cols + mixed_cols).astype(jnp.bfloat16)
     place, weighted = slot_tables(routes, route_weights, experts, capacity)
     outgoing = jnp.dot(place, residual_cols, preferred_element_type=jnp.float32)

time: 115 us -> 93.9 us (0.82)
  Pallas kernels: 30.7 us -> 10.2 us
    pallas_call x1, Pallas kernels: 26.9 us -> 6.48 us  [attention_call(): pl.pallas_call(kernel, out_shape=(jax.ShapeDtypeStruct((blocks, seq_rows,...]
where the time goes in v4:
time: 93.9 us; the launch traced here: 93.3 us
  blocking collectives  42.1 us (45%)
  waiting for transfers between devices  22.4 us (24%)
  starting transfers between devices  15 us (16%)
  Pallas kernels  10.2 us (11%)
  local copies, waits for them, and re-layouts  1.94 us (2%)
  matrix products  1.2 us (1%)
    all_to_all x1, blocking collectives, body(): lax.all_to_all(outgoing, EXPERT_AXES, split_axis=0, concat_axis=0, tiled=...  31.8 us
    all_to_all x1, waiting for transfers between devices, body(): lax.all_to_all(summed, EXPERT_AXES, split_axis=0, concat_axis=0, tiled=True)  14.8 us
    all_to_all x1, blocking collectives, copy_for_each(): return lax.all_to_all(copies, axis, split_axis=0, concat_axis=0, tiled=True)  10.3 us
    pallas_call x1, Pallas kernels, attention_call(): pl.pallas_call(kernel, out_shape=(jax.ShapeDtypeStruct((blocks, seq_rows,...  6.48 us
    all_to_all x1, waiting for transfers between devices, body(): lax.all_to_all(part, GROUP_AXES, split_axis=0, concat_axis=0, tiled=True)  5.55 us
    all_to_all x1, starting transfers between devices, body(): lax.all_to_all(part, GROUP_AXES, split_axis=0, concat_axis=0, tiled=True)  4.74 us
    all_to_all x1, starting transfers between devices, body(): blocks = lax.all_to_all(partial, 'tp', 0, 0, tiled=True)  4.47 us
    all_to_all x1, starting transfers between devices, body(): lax.all_to_all(summed, EXPERT_AXES, split_axis=0, concat_axis=0, tiled=True)  3.85 us
  transfers between devices with their start and end apart: 4, of which 3 were waited for; matrix products, arithmetic and copies ran while one was open for 2% of the time, Pallas kernels for 0%

profile of v4, /device:TPU:2, one launch (start us, length us, event | category | flops | bytes accessed | tf_op | source)
XLA Modules:
  0.0 93.3 jit_solution(5491498427219834351)
XLA Ops:
  0.0 6.5 %attention.1 = (bf16[4,13,256]{2,1,0:T(8,128)(2,1)}, bf16[3,1024,128]{2,1,0:T(8,128)(2,1)}) custom-call(s32[13]{0:T(128)} %lengths.1, f32[2]{0:T(128)} %bias.1, bf16[13,1024]{1,0:T(8,128)(2,1)} %tokens.1, f32[1,1024]{1,0:T(1,128)} %bitcast.27, bf16[1024,128]{1,0:T(8,128)(2,1)} %wq.1, bf16[64,1024]{1,0:T(8,128)(2,1)} %bitcast.23, bf16[64,1024]{1,0:T(8,128)(2,1)} %bitcast.24, ...), custom_call_target="tpu_custom_call" | custom-call | tf_op jit(solution)/shard_map/attention/pallas_call | solution.py:220
  6.5 4.5 %all-to-all-start = ((bf16[4,13,256]{2,1,0:T(8,128)(2,1)}), bf16[4,13,256]{2,1,0:T(8,128)(2,1)S(1)}, u32[]{:S(2)}, u32[]{:S(2)}) async-start(bf16[4,13,256]{2,1,0:T(8,128)(2,1)} %get-tuple-element.9), calls=%async_computation | async-start | bytes 65536 | tf_op jit(solution)/shard_map/all_to_all | solution.py:399
  11.0 1.9 %collective-permute-start = (bf16[3,1024,128]{2,1,0:T(8,128)(2,1)}, bf16[3,1024,128]{2,1,0:T(8,128)(2,1)S(1)}, u32[]{:S(2)}, u32[]{:S(2)}) collective-permute-start(bf16[3,1024,128]{2,1,0:T(8,128)(2,1)} %get-tuple-element.10.own), channel_id=1, source_target_pairs={{0,4},{4,0},{1,5},{5,1},{2,6},{6,2},{3,7},{7,3},{8,12},{12,8},{9,1... | collective-permute-start | bytes 2359304 | tf_op jit(solution)/shard_map/ppermute | solution.py:398
  12.9 0.7 constant_dynamic-slice_fusion
  13.6 0.1 copy.31
  13.7 0.1 fusion.7
  13.8 0.2 fusion.8
  14.0 0.1 copy.34
  14.2 0.1 eq.45
  14.3 2.1 %all-to-all-done = bf16[4,13,256]{2,1,0:T(8,128)(2,1)S(1)} async-done(((bf16[4,13,256]{2,1,0:T(8,128)(2,1)}), bf16[4,13,256]{2,1,0:T(8,128)(2,1)S(1)}, u32[]{:S(2)}, u32[]{:S(2)}) %all-to-all-start) | async-done | bytes 26656 | tf_op jit(solution)/shard_map/all_to_all | solution.py:399
  16.4 0.2 convolution_convert_fusion
  16.7 31.8 %all_to_all.25 = bf16[32,2,256]{2,1,0:T(2,128)(2,1)S(1)} all-to-all(bf16[32,2,256]{2,1,0:T(2,128)(2,1)S(1)} %reshape.44), channel_id=1, replica_groups=mesh['z'=16,'xh'=2,'xl'=2,'core'=2,'tp'=4] {'z','xh'}, dimensions={0} | all-to-all | bytes 65536 | tf_op jit(solution)/shard_map/all_to_all | solution.py:407
  48.5 10.3 %all_to_all.26.rows = bf16[8,64,256]{2,1,0:T(8,128)(2,1)} all-to-all(bf16[8,64,256]{2,1,0:T(8,128)(2,1)S(1)} %broadcast_in_dim.36), channel_id=1, replica_groups=mesh['z'=16,'xh'=2,'xl'=2,'core'=2,'tp'=4] {'xl','tp'}, dimensions={0} | all-to-all | bytes 524288 | tf_op jit(solution)/shard_map/all_to_all | solution.py:28
  58.8 3.7 %expert.1 = bf16[8,64,256]{2,1,0:T(8,128)(2,1)} custom-call(bf16[8,64,256]{2,1,0:T(8,128)(2,1)} %all_to_all.26.rows, f32[1,1024]{1,0:T(1,128)} %bitcast.26, bf16[3,1024,128]{2,1,0:T(8,128)(2,1)} %get-tuple-element.10.own, bf16[3,1024,128]{2,1,0:T(8,128)(2,1)} %copy-done), custom_call_target="tpu_custom_call" | custom-call | tf_op jit(solution)/shard_map/expert/pallas_call | solution.py:319
  62.6 4.7 %all-to-all-start.3 = ((bf16[8,64,256]{2,1,0:T(8,128)(2,1)}), bf16[8,64,256]{2,1,0:T(8,128)(2,1)S(1)}, u32[]{:S(2)}, u32[]{:S(2)}) async-start(bf16[8,64,256]{2,1,0:T(8,128)(2,1)} %expert.1), calls=%async_computation.3 | async-start | bytes 524288 | tf_op jit(solution)/shard_map/all_to_all | solution.py:412
  67.3 0.1 copy.35
  67.4 0.1 select_reduce_fusion
  67.5 0.1 copy.36
  67.6 5.6 %all-to-all-done.3 = bf16[8,64,256]{2,1,0:T(8,128)(2,1)S(1)} async-done(((bf16[8,64,256]{2,1,0:T(8,128)(2,1)}), bf16[8,64,256]{2,1,0:T(8,128)(2,1)S(1)}, u32[]{:S(2)}, u32[]{:S(2)}) %all-to-all-start.3) | async-done | bytes 262176 | tf_op jit(solution)/shard_map/all_to_all | solution.py:412
  73.2 0.6 reshape.47
  73.8 3.9 %all-to-all-start.4 = ((bf16[32,2,256]{2,1,0:T(2,128)(2,1)}), bf16[32,2,256]{2,1,0:T(2,128)(2,1)S(1)}, u32[]{:S(2)}, u32[]{:S(2)}) async-start(bf16[32,2,256]{2,1,0:T(2,128)(2,1)} %reshape.47), calls=%async_computation.4 | async-start | bytes 65536 | tf_op jit(solution)/shard_map/all_to_all | solution.py:415
  77.7 0.1 and_select_fusion
  77.8 14.8 %all-to-all-done.4 = bf16[32,2,256]{2,1,0:T(2,128)(2,1)S(1)} async-done(((bf16[32,2,256]{2,1,0:T(2,128)(2,1)}), bf16[32,2,256]{2,1,0:T(2,128)(2,1)S(1)}, u32[]{:S(2)}, u32[]{:S(2)}) %all-to-all-start.4) | async-done | bytes 32800 | tf_op jit(solution)/shard_map/all_to_all | solution.py:415
  92.5 0.8 fusion.1
  (18 shorter events, 0.2 us)
Async XLA Ops:
  0.0 13.6 %copy-start.1 = (s32[13,2]{0,1:T(2,128)S(1)}, s32[13,2]{0,1:T(2,128)}, u32[]{:S(2)}) copy-start(s32[13,2]{0,1:T(2,128)} %param.31) | copy-start | bytes 316
  6.5 9.9 %all-to-all-start = ((bf16[4,13,256]{2,1,0:T(8,128)(2,1)}), bf16[4,13,256]{2,1,0:T(8,128)(2,1)S(1)}, u32[]{:S(2)}, u32[]{:S(2)}) async-start(bf16[4,13,256]{2,1,0:T(8,128)(2,1)} %get-tuple-element.9), calls=%async_computation | async-start | bytes 65536 | tf_op jit(solution)/shard_map/all_to_all | solution.py:399
  11.0 37.5 %collective-permute-start = (bf16[3,1024,128]{2,1,0:T(8,128)(2,1)}, bf16[3,1024,128]{2,1,0:T(8,128)(2,1)S(1)}, u32[]{:S(2)}, u32[]{:S(2)}) collective-permute-start(bf16[3,1024,128]{2,1,0:T(8,128)(2,1)} %get-tuple-element.10.own), channel_id=1, source_target_pairs={{0,4},{4,0},{1,5},{5,1},{2,6},{6,2},{3,7},{7,3},{8,12},{12,8},{9,1... | collective-permute-start | bytes 2359304 | tf_op jit(solution)/shard_map/ppermute | solution.py:398
  48.4 18.9 %copy-start.2 = (f32[13,2]{0,1:T(2,128)S(1)}, f32[13,2]{0,1:T(2,128)}, u32[]{:S(2)}) copy-start(f32[13,2]{0,1:T(2,128)} %param.32) | copy-start | bytes 316
  48.5 10.4 %copy-start = (bf16[3,1024,128]{2,1,0:T(8,128)(2,1)}, bf16[3,1024,128]{2,1,0:T(8,128)(2,1)S(1)}, u32[]{:S(2)}) copy-start(bf16[3,1024,128]{2,1,0:T(8,128)(2,1)S(1)} %collective-permute-done.other) | copy-start | bytes 2359300
  62.6 10.6 %all-to-all-start.3 = ((bf16[8,64,256]{2,1,0:T(8,128)(2,1)}), bf16[8,64,256]{2,1,0:T(8,128)(2,1)S(1)}, u32[]{:S(2)}, u32[]{:S(2)}) async-start(bf16[8,64,256]{2,1,0:T(8,128)(2,1)} %expert.1), calls=%async_computation.3 | async-start | bytes 524288 | tf_op jit(solution)/shard_map/all_to_all | solution.py:412
  73.8 18.7 %all-to-all-start.4 = ((bf16[32,2,256]{2,1,0:T(2,128)(2,1)}), bf16[32,2,256]{2,1,0:T(2,128)(2,1)S(1)}, u32[]{:S(2)}, u32[]{:S(2)}) async-start(bf16[32,2,256]{2,1,0:T(2,128)(2,1)} %reshape.47), calls=%async_computation.4 | async-start | bytes 65536 | tf_op jit(solution)/shard_map/all_to_all | solution.py:415

commit v5 on v3

--- a/solution.py
+++ b/solution.py
@@ -8,24 +8,20 @@
 from jax.sharding import Mesh
 from jax.sharding import PartitionSpec as P
 
-HEADS = 8
-KVH = 4
+
 HD = 64
 SLICES = 4
 TOP_K = 2
-STORED_SPAN = 1024
 
 
 EPSILON = 1e-06
 EXPERT_AXES = ("z", "xh")
 SLICE_AXES = ("xl", "core")
 EP_AXES = EXPERT_AXES + SLICE_AXES
-GROUP_AXES = ("xl", "tp")
-
-
-def copy_for_each(shard, axis):
-    copies = jnp.broadcast_to(shard, (lax.axis_size(axis), *shard.shape))
-    return lax.all_to_all(copies, axis, split_axis=0, concat_axis=0, tiled=True)
+
+
+def whole_exchange(blocks):
+    return lax.all_to_all(blocks, ("tp",) + EXPERT_AXES, split_axis=0, concat_axis=0, tiled=True)
 
 
 def attention_kernel(
@@ -76,7 +72,7 @@
     key_copies = copies(keys, key_buf, key_sems)
     value_copies = copies(values, value_buf, value_sems)
     units = wg.shape[1]
-    pack_copies = [
+    pack_loads = [
         pltpu.make_async_copy(wg, pack.at[0], pack_sems.at[0]),
         pltpu.make_async_copy(wu, pack.at[1], pack_sems.at[1]),
     ] + [
@@ -87,7 +83,7 @@
         )
         for j in range(wd.shape[1] // units)
     ]
-    for copy in key_copies + value_copies + pack_copies:
+    for copy in key_copies + value_copies + pack_loads:
         copy.start()
 
     f32 = jnp.float32
@@ -181,7 +177,7 @@
     cols = out.shape[2]
     for n in range(blocks):
         out[n] = partial[0:seq_rows, n * cols : (n + 1) * cols]
-    for copy in pack_copies:
+    for copy in pack_loads:
         copy.wait()
 
 
@@ -215,11 +211,11 @@
     return pl.pallas_call(
         kernel,
         out_shape=(
-            jax.ShapeDtypeStruct((blocks, seq_rows, width // blocks), jnp.bfloat16),
-            jax.ShapeDtypeStruct((3,) + wg.shape, jnp.bfloat16),
+            pltpu.VMEM((blocks, seq_rows, width // blocks), jnp.bfloat16),
+            pltpu.VMEM((3,) + wg.shape, jnp.bfloat16),
         ),
         in_specs=[smem, smem] + [vmem] * 8 + [hbm] * 5,
-        out_specs=(vmem, hbm),
+        out_specs=(vmem, vmem),
         scratch_shapes=[
             pltpu.VMEM((seq_rows * HD, span), jnp.bfloat16),
             pltpu.VMEM((seq_rows * HD, span), jnp.bfloat16),
@@ -249,82 +245,111 @@
     )
 
 
-def expert_kernel(
-    rows, gain, own, other, out, row_buf, own_buf, other_buf, row_sem, own_sems, other_sems
-):
+def expert_kernel(rows, gain, trio, far, out, far_buf, far_sems):
+    copies = [
+        pltpu.make_async_copy(far.at[i], far_buf.at[i], far_sems.at[i]) for i in range(3)
+    ]
+    for copy in copies:
+        copy.start()
     f32 = jnp.float32
     bf16 = jnp.bfloat16
-    peers, count, cols = rows.shape
+    blocks, count, cols = rows.shape
     width = gain.shape[1]
-    blocks = width // cols
-    groups = peers // blocks
-    units = own.shape[2]
-    row_copy = pltpu.make_async_copy(rows, row_buf, row_sem)
-    row_copy.start()
-    own_copies = [pltpu.make_async_copy(own.at[i], own_buf.at[i], own_sems.at[i]) for i in range(3)]
-    other_copies = [
-        pltpu.make_async_copy(other.at[i], other_buf.at[i], other_sems.at[i]) for i in range(3)
-    ]
-    for i in range(3):
-        own_copies[i].start()
-        other_copies[i].start()
-    row_copy.wait()
-    pieces = []
-    squares = 0.0
-    for n in range(blocks):
-        piece = jnp.concatenate([row_buf[s * blocks + n] for s in range(groups)], axis=0)
-        piece = piece.astype(f32)
-        squares = squares + jnp.sum(piece * piece, axis=-1, keepdims=True)
-        pieces.append(piece)
+    units = trio.shape[2]
+    capacity = out.shape[1]
+    pieces = [rows[n].astype(f32) for n in range(blocks)]
+    squares = sum(jnp.sum(piece * piece, axis=-1, keepdims=True) for piece in pieces)
     inv = lax.rsqrt(squares / width + EPSILON)
     flats = [
         (pieces[n] * inv * gain[:, n * cols : (n + 1) * cols]).astype(bf16) for n in range(blocks)
     ]
 
-    def projected(i):
-        own_copies[i].wait()
-        other_copies[i].wait()
+    def matrix(pack, i, span):
+        if pack == 3:
+            return far_buf[i, span, :]
+        return trio[3 * pack + i, span, :]
+
+    def projected(pair, i):
         total = 0.0
         for n in range(blocks):
             span = slice(n * cols, (n + 1) * cols)
-            weight = jnp.concatenate([own_buf[i, span, :], other_buf[i, span, :]], axis=1)
+            weight = jnp.concatenate([matrix(pack, i, span) for pack in pair], axis=1)
             total = total + jnp.dot(flats[n], weight, preferred_element_type=f32)
         return total
 
-    gate = projected(0)
-    up = projected(1)
-    hidden = (gate / (1.0 + jnp.exp(-gate)) * up).astype(bf16)
-    own_copies[2].wait()
-    other_copies[2].wait()
+    pairs = [(0, 1), (2, 3)]
+    hiddens = []
+    for pair in pairs:
+        if pair[1] == 3:
+            for copy in copies:
+                copy.wait()
+        gate = projected(pair, 0)
+        up = projected(pair, 1)
+        hiddens.append((gate / (1.0 + jnp.exp(-gate)) * up).astype(bf16))
     for n in range(blocks):
-        strips = []
-        for j in range(n * cols // units, (n + 1) * cols // units):
-            span = slice(j * units, (j + 1) * units)
-            strips.append(jnp.concatenate([own_buf[2, span, :], other_buf[2, span, :]], axis=0))
-        weight = jnp.concatenate(strips, axis=1)
-        part = jnp.dot(hidden, weight, preferred_element_type=f32).astype(bf16)
-        for s in range(groups):
-            out[s * blocks + n] = part[s * count : (s + 1) * count, :]
-
-
-def expert_call(rows, gain, own, other):
+        part = 0.0
+        for pair, hidden in zip(pairs, hiddens):
+            strips = []
+            for j in range(n * cols // units, (n + 1) * cols // units):
+                span = slice(j * units, (j + 1) * units)
+                strips.append(jnp.concatenate([matrix(pack, 2, span) for pack in pair], axis=0))
+            weight = jnp.concatenate(strips, axis=1)
+            part = part + jnp.dot(hidden, weight, preferred_element_type=f32)
+        slots = count // capacity
+        for e in range(slots):
+            out[n * slots + e] = part[e * capacity : (e + 1) * capacity, :].astype(bf16)
+
+
+def expert_call(rows, gain, trio, far, capacity):
     vmem = pl.BlockSpec(memory_space=pltpu.VMEM)
     hbm = pl.BlockSpec(memory_space=pl.ANY)
+    blocks, count, cols = rows.shape
     return pl.pallas_call(
         expert_kernel,
-        out_shape=jax.ShapeDtypeStruct(rows.shape, jnp.bfloat16),
-        in_specs=[hbm, vmem, hbm, hbm],
+        out_shape=pltpu.VMEM((blocks * count // capacity, capacity, cols), jnp.bfloat16),
+        in_specs=[vmem, vmem, vmem, hbm],
         out_specs=vmem,
         scratch_shapes=[
-            pltpu.VMEM(rows.shape, jnp.bfloat16),
-            pltpu.VMEM(own.shape, jnp.bfloat16),
-            pltpu.VMEM(own.shape, jnp.bfloat16),
-            pltpu.SemaphoreType.DMA,
-            pltpu.SemaphoreType.DMA((3,)),
+            pltpu.VMEM(far.shape, jnp.bfloat16),
             pltpu.SemaphoreType.DMA((3,)),
         ],
         name="expert",
-    )(rows, gain.reshape(1, -1), own, other)
+    )(in_vmem(rows), gain.reshape(1, -1), in_vmem(trio), far)
+
+
+def outgoing_kernel(partials, token_cols, place, out, kept):
+    f32 = jnp.float32
+    bf16 = jnp.bfloat16
+    mixed = sum(partials[n].astype(f32) for n in range(partials.shape[0]))
+    residual = (token_cols[...].astype(f32) + mixed).astype(bf16)
+    kept[...] = residual
+    spread = jnp.dot(place[...], residual, preferred_element_type=f32)
+    copies, capacity = out.shape[0], out.shape[1]
+    slots = place.shape[0] // capacity
+    for e in range(slots):
+        rows = spread[e * capacity : (e + 1) * capacity, :].astype(bf16)
+        for n in range(copies // slots):
+            out[n * slots + e] = rows
+
+
+def outgoing_call(partials, token_cols, place, capacity):
+    vmem = pl.BlockSpec(memory_space=pltpu.VMEM)
+    blocks, seq_rows, cols = partials.shape
+    total = blocks * place.shape[0] // capacity
+    return pl.pallas_call(
+        outgoing_kernel,
+        out_shape=(
+            pltpu.VMEM((total, capacity, cols), jnp.bfloat16),
+            pltpu.VMEM((seq_rows, cols), jnp.bfloat16),
+        ),
+        in_specs=[vmem] * 3,
+        out_specs=(vmem, vmem),
+        name="outgoing",
+    )(in_vmem(partials), in_vmem(token_cols), in_vmem(place))
+
+
+def in_vmem(array):
+    return pltpu.with_memory_space_constraint(array, pltpu.VMEM)
 
 
 def slot_tables(routes, route_weights, experts, capacity):
@@ -389,25 +414,21 @@
         down_weight[0],
         tp_count,
     )
-    other_pack = lax.ppermute(own_pack, "core", [(0, 1), (1, 0)])
     blocks = lax.all_to_all(partial, "tp", 0, 0, tiled=True)
-    mixed_cols = jnp.sum(blocks.astype(jnp.float32), axis=0)
-    token_f = tokens.astype(jnp.float32)
-    token_cols = lax.dynamic_slice_in_dim(token_f, tp_rank * cols, cols, 1)
-    residual_cols = (token_cols + mixed_cols).astype(jnp.bfloat16)
+    swap = [(0, 1), (1, 0)]
+    side_pack = lax.ppermute(own_pack, "xl", swap)
+    core_pack = lax.ppermute(own_pack, "core", swap)
+    far_pack = lax.ppermute(side_pack, "core", swap)
+    trio = jnp.concatenate([own_pack, core_pack, side_pack], axis=0)
+    token_cols = lax.dynamic_slice_in_dim(tokens, tp_rank * cols, cols, 1)
     place, weighted = slot_tables(routes, route_weights, experts, capacity)
-    outgoing = jnp.dot(place, residual_cols, preferred_element_type=jnp.float32)
-    outgoing = outgoing.astype(jnp.bfloat16).reshape(experts, capacity, cols)
-    arrived = lax.all_to_all(outgoing, EXPERT_AXES, split_axis=0, concat_axis=0, tiled=True)
-    arrived = arrived.reshape(experts * capacity, cols)
-    arrived, other_pack = lax.optimization_barrier((arrived, other_pack))
-    gathered = copy_for_each(arrived, GROUP_AXES)
-    part = expert_call(gathered, ffn_gain, own_pack, other_pack)
-    parts = lax.all_to_all(part, GROUP_AXES, split_axis=0, concat_axis=0, tiled=True)
-    summed = jnp.sum(parts.astype(jnp.float32), axis=0).astype(jnp.bfloat16)
-    summed = summed.reshape(experts, capacity, cols)
-    returned = lax.all_to_all(summed, EXPERT_AXES, split_axis=0, concat_axis=0, tiled=True)
-    returned = returned.reshape(experts * capacity, cols).astype(jnp.float32)
+    outgoing, residual_cols = outgoing_call(blocks, token_cols, place, capacity)
+    arrived = whole_exchange(outgoing)
+    arrived = arrived.reshape(tp_count, experts * capacity, cols)
+    part = expert_call(arrived, ffn_gain, trio, far_pack, capacity)
+    parts = whole_exchange(part)
+    parts = parts.reshape(tp_count, experts * capacity, cols)
+    returned = jnp.sum(parts.astype(jnp.float32), axis=0)
     routed = jnp.dot(
         weighted, returned, precision=lax.Precision.HIGHEST, preferred_element_type=jnp.float32
     )

time: 115 us -> 103 us (0.90)
  the two profiles are of different devices: /device:TPU:2 before, /device:TPU:1 now
where the time goes in v5:
time: 103 us; the launch traced here: 101 us
  blocking collectives  40.2 us (39%)
  starting transfers between devices  29 us (28%)
  waiting for transfers between devices  18.2 us (18%)
  Pallas kernels  9.56 us (9%)
  other arithmetic  1.95 us (2%)
  local copies, waits for them, and re-layouts  1.37 us (1%)
    all_to_all x1, blocking collectives, whole_exchange(): lax.all_to_all(blocks, ('tp',) + EXPERT_AXES, split_axis=0, concat_axis=0...  40.2 us
    all_to_all x1, waiting for transfers between devices, whole_exchange(): lax.all_to_all(blocks, ('tp',) + EXPERT_AXES, split_axis=0, concat_axis=0...  16.7 us
    ppermute x1, starting transfers between devices, body(): far_pack = lax.ppermute(side_pack, 'core', swap)  8.15 us
    all_to_all x1, starting transfers between devices, whole_exchange(): lax.all_to_all(blocks, ('tp',) + EXPERT_AXES, split_axis=0, concat_axis=0...  6.9 us
    ppermute x1, starting transfers between devices, body(): core_pack = lax.ppermute(own_pack, 'core', swap)  6.73 us
    pallas_call x1, Pallas kernels, attention_call(): pl.pallas_call(kernel, out_shape=(pltpu.VMEM((blocks, seq_rows, width //...  6.36 us
    ppermute x1, starting transfers between devices, body(): side_pack = lax.ppermute(own_pack, 'xl', swap)  3.94 us
    all_to_all x1, starting transfers between devices, body(): blocks = lax.all_to_all(partial, 'tp', 0, 0, tiled=True)  3.27 us
  transfers between devices with their start and end apart: 5, of which 2 were waited for; matrix products, arithmetic and copies ran while one was open for 3% of the time, Pallas kernels for 0%

profile of v5, /device:TPU:1, one launch (start us, length us, event | category | flops | bytes accessed | tf_op | source)
XLA Modules:
  0.0 101.4 jit_solution(12306534287232662269)
XLA Ops:
  0.0 6.4 %attention.1 = (bf16[4,13,256]{2,1,0:T(8,128)(2,1)}, bf16[3,1024,128]{2,1,0:T(8,128)(2,1)S(1)}) custom-call(s32[13]{0:T(128)} %lengths.1, f32[2]{0:T(128)} %bias.1, bf16[13,1024]{1,0:T(8,128)(2,1)} %tokens.1, f32[1,1024]{1,0:T(1,128)} %bitcast.24, bf16[1024,128]{1,0:T(8,128)(2,1)} %wq.1, bf16[64,1024]{1,0:T(8,128)(2,1)} %bitcast.19, ...), custom_call_target="tpu_custom_call" | custom-call | tf_op jit(solution)/shard_map/attention/pallas_call | solution.py:211
  6.4 3.9 %collective-permute-start.1 = (bf16[3,1024,128]{2,1,0:T(8,128)(2,1)S(1)}, bf16[3,1024,128]{2,1,0:T(8,128)(2,1)}, u32[]{:S(2)}, u32[]{:S(2)}) collective-permute-start(bf16[3,1024,128]{2,1,0:T(8,128)(2,1)S(1)} %get-tuple-element.12), channel_id=1, source_target_pairs={{0,8},{8,0},{1,9},{9,1},{2,10},{10,2},{3,11},{11,3},{4,12},{12,4},... | collective-permute-start | bytes 2359304 | tf_op jit(solution)/shard_map/ppermute | solution.py:419
  10.3 6.7 %collective-permute-start = (bf16[3,1024,128]{2,1,0:T(8,128)(2,1)S(1)}, bf16[3,1024,128]{2,1,0:T(8,128)(2,1)}, u32[]{:S(2)}, u32[]{:S(2)}) collective-permute-start(bf16[3,1024,128]{2,1,0:T(8,128)(2,1)S(1)} %get-tuple-element.12), channel_id=1, source_target_pairs={{0,4},{4,0},{1,5},{5,1},{2,6},{6,2},{3,7},{7,3},{8,12},{12,8},{9,1... | collective-permute-start | bytes 2359304 | tf_op jit(solution)/shard_map/ppermute | solution.py:420
  17.1 3.3 %all-to-all-start = ((bf16[4,13,256]{2,1,0:T(8,128)(2,1)}), bf16[4,13,256]{2,1,0:T(8,128)(2,1)S(1)}, u32[]{:S(2)}, u32[]{:S(2)}) async-start(bf16[4,13,256]{2,1,0:T(8,128)(2,1)} %get-tuple-element.9), calls=%async_computation | async-start | bytes 65536 | tf_op jit(solution)/shard_map/all_to_all | solution.py:417
  20.4 0.1 copy.25
  20.4 0.1 fusion.3
  20.6 0.1 copy.28
  20.8 0.1 eq.40
  20.9 0.2 fusion.4
  21.1 0.1 fusion.6
  21.2 1.5 %collective-permute-done.1 = bf16[3,1024,128]{2,1,0:T(8,128)(2,1)} collective-permute-done((bf16[3,1024,128]{2,1,0:T(8,128)(2,1)S(1)}, bf16[3,1024,128]{2,1,0:T(8,128)(2,1)}, u32[]{:S(2)}, u32[]{:S(2)}) %collective-permute-start.1) | collective-permute-done | bytes 786464 | tf_op jit(solution)/shard_map/ppermute | solution.py:419
  22.7 8.1 %collective-permute-start.2 = (bf16[3,1024,128]{2,1,0:T(8,128)(2,1)}, bf16[3,1024,128]{2,1,0:T(8,128)(2,1)}, u32[]{:S(2)}, u32[]{:S(2)}) collective-permute-start(bf16[3,1024,128]{2,1,0:T(8,128)(2,1)} %collective-permute-done.1), channel_id=1, source_target_pairs={{0,4},{4,0},{1,5},{5,1},{2,6},{6,2},{3,7},{7,3},{8,12},{12,8},{9,1... | collective-permute-start | bytes 2359304 | tf_op jit(solution)/shard_map/ppermute | solution.py:421
  30.8 0.7 constant_dynamic-slice_fusion.token_cols
  31.5 0.2 outgoing.1
  31.7 40.2 %all_to_all.15 = bf16[128,2,256]{2,1,0:T(2,128)(2,1)S(1)} all-to-all(bf16[128,2,256]{2,1,0:T(2,128)(2,1)S(1)} %get-tuple-element.11), channel_id=1, replica_groups=mesh['z'=16,'xh'=2,'xl'=2,'core'=2,'tp'=4] {'tp','z','xh'}, dimensions={0} | all-to-all | bytes 262144 | tf_op jit(solution)/shard_map/all_to_all | solution.py:24
  71.9 0.1 reshape.44.rows
  71.9 1.6 %pad_maximum_fusion.trio = bf16[9,1024,128]{2,1,0:T(8,128)(2,1)S(1)} fusion(bf16[3,1024,128]{2,1,0:T(8,128)(2,1)} %collective-permute-done.1, bf16[3,1024,128]{2,1,0:T(8,128)(2,1)} %collective-permute-done, bf16[3,1024,128]{2,1,0:T(8,128)(2,1)S(1)} %get-tuple-element.12), kind=kLoop, calls=%fused_computation | loop fusion | flops 2359296 | bytes 4718592 | tf_op jit(solution)/shard_map/concatenate | solution.py:422
  73.6 3.0 %expert.1 = bf16[128,2,256]{2,1,0:T(2,128)(2,1)} custom-call(bf16[4,64,256]{2,1,0:T(8,128)(2,1)S(1)} %reshape.44.rows, f32[1,1024]{1,0:T(1,128)} %bitcast.23, bf16[9,1024,128]{2,1,0:T(8,128)(2,1)S(1)} %pad_maximum_fusion.trio, bf16[3,1024,128]{2,1,0:T(8,128)(2,1)} %collective-permute-done.2.far), custom_call_target="tpu_custom_call" | custom-call | tf_op jit(solution)/shard_map/expert/pallas_call | solution.py:307
  76.6 6.9 %all-to-all-start.2 = ((bf16[128,2,256]{2,1,0:T(2,128)(2,1)}), bf16[128,2,256]{2,1,0:T(2,128)(2,1)S(1)}, u32[]{:S(2)}, u32[]{:S(2)}) async-start(bf16[128,2,256]{2,1,0:T(2,128)(2,1)} %expert.1), calls=%async_computation.2 | async-start | bytes 262144 | tf_op jit(solution)/shard_map/all_to_all | solution.py:24
  83.5 0.1 copy.29
  83.6 0.1 select_reduce_fusion
  83.8 0.1 copy.30
  83.8 16.7 %all-to-all-done.2 = bf16[128,2,256]{2,1,0:T(2,128)(2,1)S(1)} async-done(((bf16[128,2,256]{2,1,0:T(2,128)(2,1)}), bf16[128,2,256]{2,1,0:T(2,128)(2,1)S(1)}, u32[]{:S(2)}, u32[]{:S(2)}) %all-to-all-start.2) | async-done | bytes 131104 | tf_op jit(solution)/shard_map/all_to_all | solution.py:24
  100.6 0.8 fusion
  (16 shorter events, 0.2 us)
Async XLA Ops:
  0.0 20.3 %copy-start = (s32[13,2]{0,1:T(2,128)S(1)}, s32[13,2]{0,1:T(2,128)}, u32[]{:S(2)}) copy-start(s32[13,2]{0,1:T(2,128)} %param.31) | copy-start | bytes 316
  6.4 16.3 %collective-permute-start.1 = (bf16[3,1024,128]{2,1,0:T(8,128)(2,1)S(1)}, bf16[3,1024,128]{2,1,0:T(8,128)(2,1)}, u32[]{:S(2)}, u32[]{:S(2)}) collective-permute-start(bf16[3,1024,128]{2,1,0:T(8,128)(2,1)S(1)} %get-tuple-element.12), channel_id=1, source_target_pairs={{0,8},{8,0},{1,9},{9,1},{2,10},{10,2},{3,11},{11,3},{4,12},{12,4},... | collective-permute-start | bytes 2359304 | tf_op jit(solution)/shard_map/ppermute | solution.py:419
  10.3 61.6 %collective-permute-start = (bf16[3,1024,128]{2,1,0:T(8,128)(2,1)S(1)}, bf16[3,1024,128]{2,1,0:T(8,128)(2,1)}, u32[]{:S(2)}, u32[]{:S(2)}) collective-permute-start(bf16[3,1024,128]{2,1,0:T(8,128)(2,1)S(1)} %get-tuple-element.12), channel_id=1, source_target_pairs={{0,4},{4,0},{1,5},{5,1},{2,6},{6,2},{3,7},{7,3},{8,12},{12,8},{9,1... | collective-permute-start | bytes 2359304 | tf_op jit(solution)/shard_map/ppermute | solution.py:420
  17.1 14.5 %all-to-all-start = ((bf16[4,13,256]{2,1,0:T(8,128)(2,1)}), bf16[4,13,256]{2,1,0:T(8,128)(2,1)S(1)}, u32[]{:S(2)}, u32[]{:S(2)}) async-start(bf16[4,13,256]{2,1,0:T(8,128)(2,1)} %get-tuple-element.9), calls=%async_computation | async-start | bytes 65536 | tf_op jit(solution)/shard_map/all_to_all | solution.py:417
  22.7 50.9 %collective-permute-start.2 = (bf16[3,1024,128]{2,1,0:T(8,128)(2,1)}, bf16[3,1024,128]{2,1,0:T(8,128)(2,1)}, u32[]{:S(2)}, u32[]{:S(2)}) collective-permute-start(bf16[3,1024,128]{2,1,0:T(8,128)(2,1)} %collective-permute-done.1), channel_id=1, source_target_pairs={{0,4},{4,0},{1,5},{5,1},{2,6},{6,2},{3,7},{7,3},{8,12},{12,8},{9,1... | collective-permute-start | bytes 2359304 | tf_op jit(solution)/shard_map/ppermute | solution.py:421
  73.6 10.0 %copy-start.1 = (f32[13,2]{0,1:T(2,128)S(1)}, f32[13,2]{0,1:T(2,128)}, u32[]{:S(2)}) copy-start(f32[13,2]{0,1:T(2,128)} %param.32) | copy-start | bytes 316
  76.6 23.9 %all-to-all-start.2 = ((bf16[128,2,256]{2,1,0:T(2,128)(2,1)}), bf16[128,2,256]{2,1,0:T(2,128)(2,1)S(1)}, u32[]{:S(2)}, u32[]{:S(2)}) async-start(bf16[128,2,256]{2,1,0:T(2,128)(2,1)} %expert.1), calls=%async_computation.2 | async-start | bytes 262144 | tf_op jit(solution)/shard_map/all_to_all | solution.py:24

commit v6 on v5

--- a/solution.py
+++ b/solution.py
@@ -20,13 +20,24 @@
 EP_AXES = EXPERT_AXES + SLICE_AXES
 
 
-def whole_exchange(blocks):
-    return lax.all_to_all(blocks, ("tp",) + EXPERT_AXES, split_axis=0, concat_axis=0, tiled=True)
-
-
 def attention_kernel(
     lengths,
     bias,
+    tokens_hbm,
+    gain_hbm,
+    wq_hbm,
+    wk_hbm,
+    wv_hbm,
+    wf_hbm,
+    wo_hbm,
+    cumul_hbm,
+    keys,
+    values,
+    wg,
+    wu,
+    wd,
+    out,
+    pack,
     tokens,
     gain,
     wq,
@@ -35,17 +46,11 @@
     wf,
     wo,
     cumul,
-    keys,
-    values,
-    wg,
-    wu,
-    wd,
-    out,
-    pack,
     key_buf,
     value_buf,
     cum_rows,
     token_rows,
+    small_sems,
     key_sems,
     value_sems,
     pack_sems,
@@ -54,6 +59,23 @@
     pad,
     chunk,
 ):
+    small_copies = [
+        pltpu.make_async_copy(source, target, small_sems.at[i])
+        for i, (source, target) in enumerate(
+            [
+                (tokens_hbm, tokens),
+                (gain_hbm, gain),
+                (wq_hbm, wq),
+                (wk_hbm, wk),
+                (wv_hbm, wv),
+                (wf_hbm, wf),
+                (cumul_hbm, cumul),
+                (wo_hbm, wo),
+            ]
+        )
+    ]
+    for copy in small_copies[:7]:
+        copy.start()
     span = keys.shape[1]
     total_rows = seq_rows * HD
     width = tokens.shape[1]
@@ -83,19 +105,17 @@
         )
         for j in range(wd.shape[1] // units)
     ]
-    for copy in key_copies + value_copies + pack_loads:
+    for copy in key_copies + value_copies + small_copies[7:] + pack_loads:
         copy.start()
 
     f32 = jnp.float32
     bf16 = jnp.bfloat16
     nt = (((1,), (1,)), ((), ()))
     token_rows[...] = jnp.zeros_like(token_rows)
+    cum_rows[...] = jnp.zeros_like(cum_rows)
+    for copy in small_copies[:6]:
+        copy.wait()
     token_rows[0:seq_rows, :] = tokens[...].astype(f32)
-    cum_rows[...] = jnp.zeros_like(cum_rows)
-    for b in range(seq_rows):
-        pair = cumul[b]
-        cum_rows[b : b + 1, :] = pair[0:1, :]
-        cum_rows[pad + b : pad + b + 1, :] = pair[1:2, :]
 
     rows = token_rows[...]
     inv = lax.rsqrt(jnp.sum(rows * rows, axis=-1, keepdims=True) / width + EPSILON)
@@ -139,6 +159,11 @@
         key_copies[i].wait()
         scores = scores + jnp.dot(left, key_buf[r : r + size, :], preferred_element_type=f32)
 
+    small_copies[6].wait()
+    for b in range(seq_rows):
+        pair = cumul[b]
+        cum_rows[b : b + 1, :] = pair[0:1, :]
+        cum_rows[pad + b : pad + b + 1, :] = pair[1:2, :]
     limit = jnp.zeros((2 * pad, 1), jnp.int32)
     for b in range(seq_rows):
         limit = jnp.where(row_seq == b, lengths[b], limit)
@@ -172,11 +197,10 @@
         [jnp.concatenate([new_values, new_values], axis=1)] * 2, axis=0
     )
     heads = jnp.where(low, mixed[0:pad, :], mixed[pad : 2 * pad, :]).astype(bf16)
+    small_copies[7].wait()
     partial = jnp.dot(heads, wo[...], preferred_element_type=f32).astype(bf16)
-    blocks = out.shape[0]
-    cols = out.shape[2]
-    for n in range(blocks):
-        out[n] = partial[0:seq_rows, n * cols : (n + 1) * cols]
+    for n in range(out.shape[0]):
+        out[n] = partial[0:seq_rows, :]
     for copy in pack_loads:
         copy.wait()
 
@@ -211,16 +235,25 @@
     return pl.pallas_call(
         kernel,
         out_shape=(
-            pltpu.VMEM((blocks, seq_rows, width // blocks), jnp.bfloat16),
+            pltpu.VMEM((blocks, seq_rows, width), jnp.bfloat16),
             pltpu.VMEM((3,) + wg.shape, jnp.bfloat16),
         ),
-        in_specs=[smem, smem] + [vmem] * 8 + [hbm] * 5,
+        in_specs=[smem, smem] + [hbm] * 13,
         out_specs=(vmem, vmem),
         scratch_shapes=[
+            pltpu.VMEM(tokens.shape, jnp.bfloat16),
+            pltpu.VMEM((1, width), jnp.float32),
+            pltpu.VMEM(wq.shape, jnp.bfloat16),
+            pltpu.VMEM((HD, width), jnp.bfloat16),
+            pltpu.VMEM((HD, width), jnp.bfloat16),
+            pltpu.VMEM((2, width), jnp.bfloat16),
+            pltpu.VMEM(wo.shape, jnp.bfloat16),
+            pltpu.VMEM(cumul.shape, jnp.float32),
             pltpu.VMEM((seq_rows * HD, span), jnp.bfloat16),
             pltpu.VMEM((seq_rows * HD, span), jnp.bfloat16),
             pltpu.VMEM((2 * pad, span), jnp.float32),
             pltpu.VMEM((pad, width), jnp.float32),
+            pltpu.SemaphoreType.DMA((8,)),
             pltpu.SemaphoreType.DMA((count,)),
             pltpu.SemaphoreType.DMA((count,)),
             pltpu.SemaphoreType.DMA((2 + width // wg.shape[1],)),
@@ -245,7 +278,7 @@
     )
 
 
-def expert_kernel(rows, gain, trio, far, out, far_buf, far_sems):
+def expert_kernel(rows, trio, far, out, far_buf, far_sems, *, blocks):
     copies = [
         pltpu.make_async_copy(far.at[i], far_buf.at[i], far_sems.at[i]) for i in range(3)
     ]
@@ -253,16 +286,11 @@
         copy.start()
     f32 = jnp.float32
     bf16 = jnp.bfloat16
-    blocks, count, cols = rows.shape
-    width = gain.shape[1]
+    count, width = rows.shape
+    cols = width // blocks
     units = trio.shape[2]
     capacity = out.shape[1]
-    pieces = [rows[n].astype(f32) for n in range(blocks)]
-    squares = sum(jnp.sum(piece * piece, axis=-1, keepdims=True) for piece in pieces)
-    inv = lax.rsqrt(squares / width + EPSILON)
-    flats = [
-        (pieces[n] * inv * gain[:, n * cols : (n + 1) * cols]).astype(bf16) for n in range(blocks)
-    ]
+    flats = [rows[:, n * cols : (n + 1) * cols] for n in range(blocks)]
 
     def matrix(pack, i, span):
         if pack == 3:
@@ -297,55 +325,56 @@
             part = part + jnp.dot(hidden, weight, preferred_element_type=f32)
         slots = count // capacity
         for e in range(slots):
-            out[n * slots + e] = part[e * capacity : (e + 1) * capacity, :].astype(bf16)
-
-
-def expert_call(rows, gain, trio, far, capacity):
+            out[e * blocks + n] = part[e * capacity : (e + 1) * capacity, :].astype(bf16)
+
+
+def expert_call(rows, trio, far, blocks, capacity):
     vmem = pl.BlockSpec(memory_space=pltpu.VMEM)
     hbm = pl.BlockSpec(memory_space=pl.ANY)
-    blocks, count, cols = rows.shape
+    count, width = rows.shape
     return pl.pallas_call(
-        expert_kernel,
-        out_shape=pltpu.VMEM((blocks * count // capacity, capacity, cols), jnp.bfloat16),
-        in_specs=[vmem, vmem, vmem, hbm],
+        functools.partial(expert_kernel, blocks=blocks),
+        out_shape=pltpu.VMEM(
+            (blocks * count // capacity, capacity, width // blocks), jnp.bfloat16
+        ),
+        in_specs=[vmem, vmem, hbm],
         out_specs=vmem,
         scratch_shapes=[
             pltpu.VMEM(far.shape, jnp.bfloat16),
             pltpu.SemaphoreType.DMA((3,)),
         ],
         name="expert",
-    )(in_vmem(rows), gain.reshape(1, -1), in_vmem(trio), far)
-
-
-def outgoing_kernel(partials, token_cols, place, out, kept):
+    )(in_vmem(rows), in_vmem(trio), far)
+
+
+def outgoing_kernel(partials, tokens, gain, place, out, kept):
     f32 = jnp.float32
     bf16 = jnp.bfloat16
     mixed = sum(partials[n].astype(f32) for n in range(partials.shape[0]))
-    residual = (token_cols[...].astype(f32) + mixed).astype(bf16)
+    residual = (tokens[...].astype(f32) + mixed).astype(bf16)
     kept[...] = residual
-    spread = jnp.dot(place[...], residual, preferred_element_type=f32)
-    copies, capacity = out.shape[0], out.shape[1]
-    slots = place.shape[0] // capacity
-    for e in range(slots):
-        rows = spread[e * capacity : (e + 1) * capacity, :].astype(bf16)
-        for n in range(copies // slots):
-            out[n * slots + e] = rows
-
-
-def outgoing_call(partials, token_cols, place, capacity):
+    rows = residual.astype(f32)
+    inv = lax.rsqrt(jnp.sum(rows * rows, axis=-1, keepdims=True) / rows.shape[1] + EPSILON)
+    ffn_in = (rows * inv * gain[...]).astype(bf16)
+    spread = jnp.dot(place[...], ffn_in, preferred_element_type=f32)
+    capacity = out.shape[1]
+    for e in range(out.shape[0]):
+        out[e] = spread[e * capacity : (e + 1) * capacity, :].astype(bf16)
+
+
+def outgoing_call(partials, tokens, gain, place, capacity):
     vmem = pl.BlockSpec(memory_space=pltpu.VMEM)
-    blocks, seq_rows, cols = partials.shape
-    total = blocks * place.shape[0] // capacity
+    _, seq_rows, width = partials.shape
     return pl.pallas_call(
         outgoing_kernel,
         out_shape=(
-            pltpu.VMEM((total, capacity, cols), jnp.bfloat16),
-            pltpu.VMEM((seq_rows, cols), jnp.bfloat16),
+            pltpu.VMEM((place.shape[0] // capacity, capacity, width), jnp.bfloat16),
+            pltpu.VMEM((seq_rows, width), jnp.bfloat16),
         ),
-        in_specs=[vmem] * 3,
+        in_specs=[vmem] * 4,
         out_specs=(vmem, vmem),
         name="outgoing",
-    )(in_vmem(partials), in_vmem(token_cols), in_vmem(place))
+    )(in_vmem(partials), in_vmem(tokens), in_vmem(gain.reshape(1, -1)), in_vmem(place))
 
 
 def in_vmem(array):
@@ -420,15 +449,15 @@
     core_pack = lax.ppermute(own_pack, "core", swap)
     far_pack = lax.ppermute(side_pack, "core", swap)
     trio = jnp.concatenate([own_pack, core_pack, side_pack], axis=0)
-    token_cols = lax.dynamic_slice_in_dim(tokens, tp_rank * cols, cols, 1)
     place, weighted = slot_tables(routes, route_weights, experts, capacity)
-    outgoing, residual_cols = outgoing_call(blocks, token_cols, place, capacity)
-    arrived = whole_exchange(outgoing)
-    arrived = arrived.reshape(tp_count, experts * capacity, cols)
-    part = expert_call(arrived, ffn_gain, trio, far_pack, capacity)
-    parts = whole_exchange(part)
-    parts = parts.reshape(tp_count, experts * capacity, cols)
-    returned = jnp.sum(parts.astype(jnp.float32), axis=0)
+    outgoing, residual = outgoing_call(blocks, tokens, ffn_gain, place, capacity)
+    residual_cols = lax.dynamic_slice_in_dim(residual, tp_rank * cols, cols, 1)
+    arrived = lax.all_to_all(outgoing, EXPERT_AXES, split_axis=0, concat_axis=0, tiled=True)
+    arrived = arrived.reshape(experts * capacity, width)
+    part = expert_call(arrived, trio, far_pack, tp_count, capacity)
+    parts = lax.all_to_all(part, EXPERT_AXES + ("tp",), split_axis=0, concat_axis=0, tiled=True)
+    parts = parts.reshape(experts, tp_count, capacity, cols)
+    returned = jnp.sum(parts.astype(jnp.float32), axis=1).reshape(experts * capacity, cols)
     routed = jnp.dot(
         weighted, returned, precision=lax.Precision.HIGHEST, preferred_element_type=jnp.float32
     )

time: 103 us -> 97.5 us (0.947)
  the two profiles are of different devices: /device:TPU:1 before, /device:TPU:32 now
where the time goes in v6:
time: 97.5 us; the launch traced here: 97 us
  blocking collectives  34.3 us (35%)
  waiting for transfers between devices  29.2 us (30%)
  starting transfers between devices  20.5 us (21%)
  Pallas kernels  9.01 us (9%)
  other arithmetic  2.14 us (2%)
  matrix products  1.02 us (1%)
    all_to_all x1, blocking collectives, body(): lax.all_to_all(outgoing, EXPERT_AXES, split_axis=0, concat_axis=0, tiled=...  34.3 us
    all_to_all x1, waiting for transfers between devices, body(): lax.all_to_all(part, EXPERT_AXES + ('tp',), split_axis=0, concat_axis=0,...  18.4 us
    ppermute x1, waiting for transfers between devices, body(): side_pack = lax.ppermute(own_pack, 'xl', swap)  10.8 us
    all_to_all x1, starting transfers between devices, body(): lax.all_to_all(part, EXPERT_AXES + ('tp',), split_axis=0, concat_axis=0,...  8.81 us
    pallas_call x1, Pallas kernels, attention_call(): pl.pallas_call(kernel, out_shape=(pltpu.VMEM((blocks, seq_rows, width), j...  6.19 us
    all_to_all x1, starting transfers between devices, body(): blocks = lax.all_to_all(partial, 'tp', 0, 0, tiled=True)  4.48 us
    ppermute x1, starting transfers between devices, body(): side_pack = lax.ppermute(own_pack, 'xl', swap)  3.4 us
    pallas_call x1, Pallas kernels, expert_call(): pl.pallas_call(functools.partial(expert_kernel, blocks=blocks), out_shape...  2.54 us
  transfers between devices with their start and end apart: 5, of which 2 were waited for; matrix products, arithmetic and copies ran while one was open for 3% of the time, Pallas kernels for 0%

profile of v6, /device:TPU:32, one launch (start us, length us, event | category | flops | bytes accessed | tf_op | source)
XLA Modules:
  0.0 97.0 jit_solution(4230902754928201683)
XLA Ops:
  0.0 6.2 %attention.1 = (bf16[4,13,1024]{2,1,0:T(8,128)(2,1)}, bf16[3,1024,128]{2,1,0:T(8,128)(2,1)S(1)}) custom-call(s32[13]{0:T(128)} %lengths.1, f32[2]{0:T(128)} %bias.1, bf16[13,1024]{1,0:T(8,128)(2,1)} %tokens.1, f32[1,1024]{1,0:T(1,128)} %bitcast.30, bf16[1024,128]{1,0:T(8,128)(2,1)} %wq_hbm.1, bf16[64,1024]{1,0:T(8,128)(2,1)} %bitcast.27, ...), custom_call_target="tpu_custom_call" | custom-call | tf_op jit(solution)/shard_map/attention/pallas_call | solution.py:235
  6.2 3.4 %collective-permute-start.1 = (bf16[3,1024,128]{2,1,0:T(8,128)(2,1)S(1)}, bf16[3,1024,128]{2,1,0:T(8,128)(2,1)}, u32[]{:S(2)}, u32[]{:S(2)}) collective-permute-start(bf16[3,1024,128]{2,1,0:T(8,128)(2,1)S(1)} %get-tuple-element.12), channel_id=1, source_target_pairs={{0,8},{8,0},{1,9},{9,1},{2,10},{10,2},{3,11},{11,3},{4,12},{12,4},... | collective-permute-start | bytes 2359304 | tf_op jit(solution)/shard_map/ppermute | solution.py:448
  9.6 1.9 %collective-permute-start = (bf16[3,1024,128]{2,1,0:T(8,128)(2,1)S(1)}, bf16[3,1024,128]{2,1,0:T(8,128)(2,1)}, u32[]{:S(2)}, u32[]{:S(2)}) collective-permute-start(bf16[3,1024,128]{2,1,0:T(8,128)(2,1)S(1)} %get-tuple-element.12), channel_id=1, source_target_pairs={{0,4},{4,0},{1,5},{5,1},{2,6},{6,2},{3,7},{7,3},{8,12},{12,8},{9,1... | collective-permute-start | bytes 2359304 | tf_op jit(solution)/shard_map/ppermute | solution.py:449
  11.5 4.5 %all-to-all-start = ((bf16[4,13,1024]{2,1,0:T(8,128)(2,1)}), bf16[4,13,1024]{2,1,0:T(8,128)(2,1)S(1)}, u32[]{:S(2)}, u32[]{:S(2)}) async-start(bf16[4,13,1024]{2,1,0:T(8,128)(2,1)} %get-tuple-element.9), calls=%async_computation | async-start | bytes 262144 | tf_op jit(solution)/shard_map/all_to_all | solution.py:446
  16.0 0.1 copy.32
  16.1 0.1 fusion.4
  16.2 0.2 fusion.5
  16.4 0.1 copy.35
  16.6 0.1 eq.43
  16.7 10.8 %collective-permute-done.1 = bf16[3,1024,128]{2,1,0:T(8,128)(2,1)} collective-permute-done((bf16[3,1024,128]{2,1,0:T(8,128)(2,1)S(1)}, bf16[3,1024,128]{2,1,0:T(8,128)(2,1)}, u32[]{:S(2)}, u32[]{:S(2)}) %collective-permute-start.1) | collective-permute-done | bytes 786464 | tf_op jit(solution)/shard_map/ppermute | solution.py:448
  27.5 1.9 %collective-permute-start.2 = (bf16[3,1024,128]{2,1,0:T(8,128)(2,1)}, bf16[3,1024,128]{2,1,0:T(8,128)(2,1)}, u32[]{:S(2)}, u32[]{:S(2)}) collective-permute-start(bf16[3,1024,128]{2,1,0:T(8,128)(2,1)} %collective-permute-done.1), channel_id=1, source_target_pairs={{0,4},{4,0},{1,5},{5,1},{2,6},{6,2},{3,7},{7,3},{8,12},{12,8},{9,1... | collective-permute-start | bytes 2359304 | tf_op jit(solution)/shard_map/ppermute | solution.py:450
  29.4 0.1 and_convert_fusion.place
  29.5 0.3 outgoing.1
  29.8 34.3 %all_to_all.15 = bf16[32,2,1024]{2,1,0:T(2,128)(2,1)S(1)} all-to-all(bf16[32,2,1024]{2,1,0:T(2,128)(2,1)S(1)} %get-tuple-element.11), channel_id=1, replica_groups=mesh['z'=16,'xh'=2,'xl'=2,'core'=2,'tp'=4] {'z','xh'}, dimensions={0} | all-to-all | bytes 262144 | tf_op jit(solution)/shard_map/all_to_all | solution.py:455
  64.2 1.6 %pad_maximum_fusion.trio = bf16[9,1024,128]{2,1,0:T(8,128)(2,1)S(1)} fusion(bf16[3,1024,128]{2,1,0:T(8,128)(2,1)} %collective-permute-done.1, bf16[3,1024,128]{2,1,0:T(8,128)(2,1)} %collective-permute-done, bf16[3,1024,128]{2,1,0:T(8,128)(2,1)S(1)} %get-tuple-element.12), kind=kLoop, calls=%fused_computation | loop fusion | flops 2359296 | bytes 4718592 | tf_op jit(solution)/shard_map/concatenate | solution.py:451
  65.9 2.5 %expert.1 = bf16[128,2,256]{2,1,0:T(2,128)(2,1)} custom-call(bf16[64,1024]{1,0:T(8,128)(2,1)S(1)} %reshape.42.rows, bf16[9,1024,128]{2,1,0:T(8,128)(2,1)S(1)} %pad_maximum_fusion.trio, bf16[3,1024,128]{2,1,0:T(8,128)(2,1)} %collective-permute-done.2.far), custom_call_target="tpu_custom_call" | custom-call | tf_op jit(solution)/shard_map/expert/pallas_call | solution.py:335
  68.4 8.8 %all-to-all-start.2 = ((bf16[128,2,256]{2,1,0:T(2,128)(2,1)}), bf16[128,2,256]{2,1,0:T(2,128)(2,1)S(1)}, u32[]{:S(2)}, u32[]{:S(2)}) async-start(bf16[128,2,256]{2,1,0:T(2,128)(2,1)} %expert.1), calls=%async_computation.2 | async-start | bytes 262144 | tf_op jit(solution)/shard_map/all_to_all | solution.py:458
  77.2 0.1 copy.36
  77.3 0.1 select_reduce_fusion
  77.4 0.1 copy.37
  77.5 0.1 and_select_fusion
  77.6 18.4 %all-to-all-done.2 = bf16[128,2,256]{2,1,0:T(2,128)(2,1)S(1)} async-done(((bf16[128,2,256]{2,1,0:T(2,128)(2,1)}), bf16[128,2,256]{2,1,0:T(2,128)(2,1)S(1)}, u32[]{:S(2)}, u32[]{:S(2)}) %all-to-all-start.2) | async-done | bytes 131104 | tf_op jit(solution)/shard_map/all_to_all | solution.py:458
  96.0 0.1 convert_reduce_fusion
  96.1 0.8 fusion.1
  (18 shorter events, 0.2 us)
Async XLA Ops:
  0.0 16.0 %copy-start.2 = (s32[13,2]{0,1:T(2,128)S(1)}, s32[13,2]{0,1:T(2,128)}, u32[]{:S(2)}) copy-start(s32[13,2]{0,1:T(2,128)} %param.31) | copy-start | bytes 316
  0.0 29.5 %copy-start = (bf16[13,1024]{1,0:T(8,128)(2,1)S(1)}, bf16[13,1024]{1,0:T(8,128)(2,1)}, u32[]{:S(2)}) copy-start(bf16[13,1024]{1,0:T(8,128)(2,1)} %tokens.1) | copy-start | bytes 79876
  0.0 29.5 %copy-start.1 = (f32[1024]{0:T(1024)S(1)}, f32[1024]{0:T(1024)}, u32[]{:S(2)}) copy-start(f32[1024]{0:T(1024)} %param.30) | copy-start | bytes 12292
  6.2 21.3 %collective-permute-start.1 = (bf16[3,1024,128]{2,1,0:T(8,128)(2,1)S(1)}, bf16[3,1024,128]{2,1,0:T(8,128)(2,1)}, u32[]{:S(2)}, u32[]{:S(2)}) collective-permute-start(bf16[3,1024,128]{2,1,0:T(8,128)(2,1)S(1)} %get-tuple-element.12), channel_id=1, source_target_pairs={{0,8},{8,0},{1,9},{9,1},{2,10},{10,2},{3,11},{11,3},{4,12},{12,4},... | collective-permute-start | bytes 2359304 | tf_op jit(solution)/shard_map/ppermute | solution.py:448
  9.6 54.6 %collective-permute-start = (bf16[3,1024,128]{2,1,0:T(8,128)(2,1)S(1)}, bf16[3,1024,128]{2,1,0:T(8,128)(2,1)}, u32[]{:S(2)}, u32[]{:S(2)}) collective-permute-start(bf16[3,1024,128]{2,1,0:T(8,128)(2,1)S(1)} %get-tuple-element.12), channel_id=1, source_target_pairs={{0,4},{4,0},{1,5},{5,1},{2,6},{6,2},{3,7},{7,3},{8,12},{12,8},{9,1... | collective-permute-start | bytes 2359304 | tf_op jit(solution)/shard_map/ppermute | solution.py:449
  11.5 18.0 %all-to-all-start = ((bf16[4,13,1024]{2,1,0:T(8,128)(2,1)}), bf16[4,13,1024]{2,1,0:T(8,128)(2,1)S(1)}, u32[]{:S(2)}, u32[]{:S(2)}) async-start(bf16[4,13,1024]{2,1,0:T(8,128)(2,1)} %get-tuple-element.9), calls=%async_computation | async-start | bytes 262144 | tf_op jit(solution)/shard_map/all_to_all | solution.py:446
  27.5 38.4 %collective-permute-start.2 = (bf16[3,1024,128]{2,1,0:T(8,128)(2,1)}, bf16[3,1024,128]{2,1,0:T(8,128)(2,1)}, u32[]{:S(2)}, u32[]{:S(2)}) collective-permute-start(bf16[3,1024,128]{2,1,0:T(8,128)(2,1)} %collective-permute-done.1), channel_id=1, source_target_pairs={{0,4},{4,0},{1,5},{5,1},{2,6},{6,2},{3,7},{7,3},{8,12},{12,8},{9,1... | collective-permute-start | bytes 2359304 | tf_op jit(solution)/shard_map/ppermute | solution.py:450
  65.8 11.4 %copy-start.3 = (f32[13,2]{0,1:T(2,128)S(1)}, f32[13,2]{0,1:T(2,128)}, u32[]{:S(2)}) copy-start(f32[13,2]{0,1:T(2,128)} %param.32) | copy-start | bytes 316
  68.4 27.6 %all-to-all-start.2 = ((bf16[128,2,256]{2,1,0:T(2,128)(2,1)}), bf16[128,2,256]{2,1,0:T(2,128)(2,1)S(1)}, u32[]{:S(2)}, u32[]{:S(2)}) async-start(bf16[128,2,256]{2,1,0:T(2,128)(2,1)} %expert.1), calls=%async_computation.2 | async-start | bytes 262144 | tf_op jit(solution)/shard_map/all_to_all | solution.py:458

commit v7 on v6

--- a/solution.py
+++ b/solution.py
@@ -278,49 +278,46 @@
     )
 
 
-def expert_kernel(rows, trio, far, out, far_buf, far_sems, *, blocks):
-    copies = [
-        pltpu.make_async_copy(far.at[i], far_buf.at[i], far_sems.at[i]) for i in range(3)
-    ]
-    for copy in copies:
-        copy.start()
+def expert_kernel(rows, pair, far, out, far_buf, far_sems, *, blocks):
+    order = (0, 3, 1, 4, 2, 5)
+    copies = {i: pltpu.make_async_copy(far.at[i], far_buf.at[i], far_sems.at[i]) for i in order}
+    for i in order:
+        copies[i].start()
     f32 = jnp.float32
     bf16 = jnp.bfloat16
     count, width = rows.shape
     cols = width // blocks
-    units = trio.shape[2]
+    units = pair.shape[2]
     capacity = out.shape[1]
     flats = [rows[:, n * cols : (n + 1) * cols] for n in range(blocks)]
 
-    def matrix(pack, i, span):
-        if pack == 3:
-            return far_buf[i, span, :]
-        return trio[3 * pack + i, span, :]
-
-    def projected(pair, i):
+    def projected(packs, i):
         total = 0.0
         for n in range(blocks):
             span = slice(n * cols, (n + 1) * cols)
-            weight = jnp.concatenate([matrix(pack, i, span) for pack in pair], axis=1)
+            weight = jnp.concatenate([packs[i, span, :], packs[3 + i, span, :]], axis=1)
             total = total + jnp.dot(flats[n], weight, preferred_element_type=f32)
         return total
 
-    pairs = [(0, 1), (2, 3)]
     hiddens = []
-    for pair in pairs:
-        if pair[1] == 3:
-            for copy in copies:
-                copy.wait()
-        gate = projected(pair, 0)
-        up = projected(pair, 1)
+    for packs in (pair, far_buf):
+        factors = []
+        for i in range(2):
+            if packs is far_buf:
+                copies[i].wait()
+                copies[3 + i].wait()
+            factors.append(projected(packs, i))
+        gate, up = factors
         hiddens.append((gate / (1.0 + jnp.exp(-gate)) * up).astype(bf16))
+    copies[2].wait()
+    copies[5].wait()
     for n in range(blocks):
         part = 0.0
-        for pair, hidden in zip(pairs, hiddens):
+        for packs, hidden in zip((pair, far_buf), hiddens):
             strips = []
             for j in range(n * cols // units, (n + 1) * cols // units):
                 span = slice(j * units, (j + 1) * units)
-                strips.append(jnp.concatenate([matrix(pack, 2, span) for pack in pair], axis=0))
+                strips.append(jnp.concatenate([packs[2, span, :], packs[5, span, :]], axis=0))
             weight = jnp.concatenate(strips, axis=1)
             part = part + jnp.dot(hidden, weight, preferred_element_type=f32)
         slots = count // capacity
@@ -328,7 +325,7 @@
             out[e * blocks + n] = part[e * capacity : (e + 1) * capacity, :].astype(bf16)
 
 
-def expert_call(rows, trio, far, blocks, capacity):
+def expert_call(rows, pair, far, blocks, capacity):
     vmem = pl.BlockSpec(memory_space=pltpu.VMEM)
     hbm = pl.BlockSpec(memory_space=pl.ANY)
     count, width = rows.shape
@@ -341,10 +338,10 @@
         out_specs=vmem,
         scratch_shapes=[
             pltpu.VMEM(far.shape, jnp.bfloat16),
-            pltpu.SemaphoreType.DMA((3,)),
+            pltpu.SemaphoreType.DMA((6,)),
         ],
         name="expert",
-    )(in_vmem(rows), in_vmem(trio), far)
+    )(in_vmem(rows), in_vmem(pair), far)
 
 
 def outgoing_kernel(partials, tokens, gain, place, out, kept):
@@ -446,15 +443,14 @@
     blocks = lax.all_to_all(partial, "tp", 0, 0, tiled=True)
     swap = [(0, 1), (1, 0)]
     side_pack = lax.ppermute(own_pack, "xl", swap)
-    core_pack = lax.ppermute(own_pack, "core", swap)
-    far_pack = lax.ppermute(side_pack, "core", swap)
-    trio = jnp.concatenate([own_pack, core_pack, side_pack], axis=0)
+    pair = jnp.concatenate([own_pack, side_pack], axis=0)
+    far_pair = lax.ppermute(pair, "core", swap)
     place, weighted = slot_tables(routes, route_weights, experts, capacity)
     outgoing, residual = outgoing_call(blocks, tokens, ffn_gain, place, capacity)
     residual_cols = lax.dynamic_slice_in_dim(residual, tp_rank * cols, cols, 1)
     arrived = lax.all_to_all(outgoing, EXPERT_AXES, split_axis=0, concat_axis=0, tiled=True)
     arrived = arrived.reshape(experts * capacity, width)
-    part = expert_call(arrived, trio, far_pack, tp_count, capacity)
+    part = expert_call(arrived, pair, far_pair, tp_count, capacity)
     parts = lax.all_to_all(part, EXPERT_AXES + ("tp",), split_axis=0, concat_axis=0, tiled=True)
     parts = parts.reshape(experts, tp_count, capacity, cols)
     returned = jnp.sum(parts.astype(jnp.float32), axis=1).reshape(experts * capacity, cols)

time: 97.5 us -> 103 us (1.056)
  waiting for transfers between devices: 29.2 us -> 41 us
  starting transfers between devices: 20.5 us -> 16.7 us
  other arithmetic: 2.14 us -> 0.51 us
  blocking collectives: 34.3 us -> 32.8 us
    ppermute x1, waiting for transfers between devices: 10.8 us -> 17.7 us  [body(): side_pack = lax.ppermute(own_pack, 'xl', swap)]
    all_to_all x1, waiting for transfers between devices: 0.01 us -> 5.17 us  [body(): blocks = lax.all_to_all(partial, 'tp', 0, 0, tiled=True)]
    all_to_all x1, starting transfers between devices: 8.81 us -> 6.82 us  [body(): lax.all_to_all(part, EXPERT_AXES + ('tp',), split_axis=0, concat_axis=0,...]
    ppermute x2 -> x1, starting transfers between devices: 3.83 us -> 1.92 us  [body(): far_pair = lax.ppermute(pair, 'core', swap)]
    concatenate x1 -> x0, other arithmetic: 1.63 us -> none  [body(): trio = jnp.concatenate([own_pack, core_pack, side_pack], axis=0)]
    all_to_all x1, blocking collectives: 34.3 us -> 32.8 us  [body(): lax.all_to_all(outgoing, EXPERT_AXES, split_axis=0, concat_axis=0, tiled=...]
  transfers between devices with their start and end apart: 5 -> 4, of which waited for: 2 -> 3; matrix products, arithmetic and copies ran while one was open for 3% -> 1% of each run, Pallas kernels for 0% -> 0%
where the time goes in v7:
time: 103 us; the launch traced here: 102 us
  waiting for transfers between devices  41 us (40%)
  blocking collectives  32.8 us (32%)
  starting transfers between devices  16.7 us (16%)
  Pallas kernels  9.1 us (9%)
    all_to_all x1, blocking collectives, body(): lax.all_to_all(outgoing, EXPERT_AXES, split_axis=0, concat_axis=0, tiled=...  32.8 us
    all_to_all x1, waiting for transfers between devices, body(): lax.all_to_all(part, EXPERT_AXES + ('tp',), split_axis=0, concat_axis=0,...  18.1 us
    ppermute x1, waiting for transfers between devices, body(): side_pack = lax.ppermute(own_pack, 'xl', swap)  17.7 us
    all_to_all x1, starting transfers between devices, body(): lax.all_to_all(part, EXPERT_AXES + ('tp',), split_axis=0, concat_axis=0,...  6.82 us
    pallas_call x1, Pallas kernels, attention_call(): pl.pallas_call(kernel, out_shape=(pltpu.VMEM((blocks, seq_rows, width), j...  6.06 us
    all_to_all x1, waiting for transfers between devices, body(): blocks = lax.all_to_all(partial, 'tp', 0, 0, tiled=True)  5.17 us
    all_to_all x1, starting transfers between devices, body(): blocks = lax.all_to_all(partial, 'tp', 0, 0, tiled=True)  4.48 us
    ppermute x1, starting transfers between devices, body(): side_pack = lax.ppermute(own_pack, 'xl', swap)  3.53 us
  transfers between devices with their start and end apart: 4, of which 3 were waited for; matrix products, arithmetic and copies ran while one was open for 1% of the time, Pallas kernels for 0%

profile of v7, /device:TPU:32, one launch (start us, length us, event | category | flops | bytes accessed | tf_op | source)
XLA Modules:
  0.0 102.2 jit_solution(16396952661255409233)
XLA Ops:
  0.0 6.1 %attention.1 = (bf16[4,13,1024]{2,1,0:T(8,128)(2,1)}, bf16[3,1024,128]{2,1,0:T(8,128)(2,1)S(1)}) custom-call(s32[13]{0:T(128)} %lengths.1, f32[2]{0:T(128)} %bias.1, bf16[13,1024]{1,0:T(8,128)(2,1)} %tokens.1, f32[1,1024]{1,0:T(1,128)} %bitcast.30, bf16[1024,128]{1,0:T(8,128)(2,1)} %wq_hbm.1, bf16[64,1024]{1,0:T(8,128)(2,1)} %bitcast.27, ...), custom_call_target="tpu_custom_call" | custom-call | tf_op jit(solution)/shard_map/attention/pallas_call | solution.py:235
  6.1 3.5 %collective-permute-start = (bf16[3,1024,128]{2,1,0:T(8,128)(2,1)S(1)}, bf16[3,1024,128]{2,1,0:T(8,128)(2,1)S(1)}, u32[]{:S(2)}, u32[]{:S(2)}) collective-permute-start(bf16[3,1024,128]{2,1,0:T(8,128)(2,1)S(1)} %get-tuple-element.12), channel_id=1, source_target_pairs={{0,8},{8,0},{1,9},{9,1},{2,10},{10,2},{3,11},{11,3},{4,12},{12,4},... | collective-permute-start | bytes 2359304 | tf_op jit(solution)/shard_map/ppermute | solution.py:445
  9.7 17.7 %collective-permute-done = bf16[3,1024,128]{2,1,0:T(8,128)(2,1)S(1)} collective-permute-done((bf16[3,1024,128]{2,1,0:T(8,128)(2,1)S(1)}, bf16[3,1024,128]{2,1,0:T(8,128)(2,1)S(1)}, u32[]{:S(2)}, u32[]{:S(2)}) %collective-permute-start) | collective-permute-done | bytes 786464 | tf_op jit(solution)/shard_map/ppermute | solution.py:445
  27.4 0.1 constant_dynamic-update-slice_fusion.pair
  27.5 1.9 %collective-permute-start.1 = (bf16[6,1024,128]{2,1,0:T(8,128)(2,1)S(1)}, bf16[6,1024,128]{2,1,0:T(8,128)(2,1)}, u32[]{:S(2)}, u32[]{:S(2)}) collective-permute-start(bf16[6,1024,128]{2,1,0:T(8,128)(2,1)S(1)} %constant_dynamic-update-slice_fusion.pair), channel_id=1, source_target_pairs={{0,4},{4,0},{1,5},{5,1},{2,6},{6,2},{3,7},{7,3},{8,12},{12,8},{9,1... | collective-permute-start | bytes 4718600 | tf_op jit(solution)/shard_map/ppermute | solution.py:447
  29.4 4.5 %all-to-all-start = ((bf16[4,13,1024]{2,1,0:T(8,128)(2,1)}), bf16[4,13,1024]{2,1,0:T(8,128)(2,1)S(1)}, u32[]{:S(2)}, u32[]{:S(2)}) async-start(bf16[4,13,1024]{2,1,0:T(8,128)(2,1)} %get-tuple-element.9), calls=%async_computation | async-start | bytes 262144 | tf_op jit(solution)/shard_map/all_to_all | solution.py:443
  33.9 0.1 copy.32
  34.0 0.1 fusion.4
  34.1 0.1 copy.35
  34.3 0.1 eq.43
  34.4 0.2 fusion.5
  34.6 0.1 and_convert_fusion.place
  34.7 5.2 %all-to-all-done.partials = bf16[4,13,1024]{2,1,0:T(8,128)(2,1)S(1)} async-done(((bf16[4,13,1024]{2,1,0:T(8,128)(2,1)}), bf16[4,13,1024]{2,1,0:T(8,128)(2,1)S(1)}, u32[]{:S(2)}, u32[]{:S(2)}) %all-to-all-start) | async-done | bytes 106528 | tf_op jit(solution)/shard_map/all_to_all | solution.py:443
  39.9 0.3 outgoing.1
  40.2 32.8 %all_to_all.15 = bf16[32,2,1024]{2,1,0:T(2,128)(2,1)S(1)} all-to-all(bf16[32,2,1024]{2,1,0:T(2,128)(2,1)S(1)} %get-tuple-element.11), channel_id=1, replica_groups=mesh['z'=16,'xh'=2,'xl'=2,'core'=2,'tp'=4] {'z','xh'}, dimensions={0} | all-to-all | bytes 262144 | tf_op jit(solution)/shard_map/all_to_all | solution.py:451
  73.1 2.8 %expert.1 = bf16[128,2,256]{2,1,0:T(2,128)(2,1)} custom-call(bf16[64,1024]{1,0:T(8,128)(2,1)S(1)} %reshape.42.rows, bf16[6,1024,128]{2,1,0:T(8,128)(2,1)S(1)} %constant_dynamic-update-slice_fusion.pair, bf16[6,1024,128]{2,1,0:T(8,128)(2,1)} %collective-permute-done.1.far), custom_call_target="tpu_custom_call" | custom-call | tf_op jit(solution)/shard_map/expert/pallas_call | solution.py:332
  75.9 6.8 %all-to-all-start.2 = ((bf16[128,2,256]{2,1,0:T(2,128)(2,1)}), bf16[128,2,256]{2,1,0:T(2,128)(2,1)S(1)}, u32[]{:S(2)}, u32[]{:S(2)}) async-start(bf16[128,2,256]{2,1,0:T(2,128)(2,1)} %expert.1), calls=%async_computation.2 | async-start | bytes 262144 | tf_op jit(solution)/shard_map/all_to_all | solution.py:454
  82.7 0.1 copy.36
  82.8 0.1 select_reduce_fusion
  82.9 0.1 copy.37
  83.0 0.1 and_select_fusion
  83.1 18.1 %all-to-all-done.2 = bf16[128,2,256]{2,1,0:T(2,128)(2,1)S(1)} async-done(((bf16[128,2,256]{2,1,0:T(2,128)(2,1)}), bf16[128,2,256]{2,1,0:T(2,128)(2,1)S(1)}, u32[]{:S(2)}, u32[]{:S(2)}) %all-to-all-start.2) | async-done | bytes 131104 | tf_op jit(solution)/shard_map/all_to_all | solution.py:454
  101.2 0.1 convert_reduce_fusion
  101.4 0.8 fusion.1
  (17 shorter events, 0.2 us)
Async XLA Ops:
  6.1 27.9 %copy-start.2 = (s32[13,2]{0,1:T(2,128)S(1)}, s32[13,2]{0,1:T(2,128)}, u32[]{:S(2)}) copy-start(s32[13,2]{0,1:T(2,128)} %param.31) | copy-start | bytes 316
  6.1 33.8 %copy-start = (bf16[13,1024]{1,0:T(8,128)(2,1)S(1)}, bf16[13,1024]{1,0:T(8,128)(2,1)}, u32[]{:S(2)}) copy-start(bf16[13,1024]{1,0:T(8,128)(2,1)} %tokens.1) | copy-start | bytes 79876
  6.1 33.8 %copy-start.1 = (f32[1024]{0:T(1024)S(1)}, f32[1024]{0:T(1024)}, u32[]{:S(2)}) copy-start(f32[1024]{0:T(1024)} %param.30) | copy-start | bytes 12292
  6.1 21.3 %collective-permute-start = (bf16[3,1024,128]{2,1,0:T(8,128)(2,1)S(1)}, bf16[3,1024,128]{2,1,0:T(8,128)(2,1)S(1)}, u32[]{:S(2)}, u32[]{:S(2)}) collective-permute-start(bf16[3,1024,128]{2,1,0:T(8,128)(2,1)S(1)} %get-tuple-element.12), channel_id=1, source_target_pairs={{0,8},{8,0},{1,9},{9,1},{2,10},{10,2},{3,11},{11,3},{4,12},{12,4},... | collective-permute-start | bytes 2359304 | tf_op jit(solution)/shard_map/ppermute | solution.py:445
  27.5 45.6 %collective-permute-start.1 = (bf16[6,1024,128]{2,1,0:T(8,128)(2,1)S(1)}, bf16[6,1024,128]{2,1,0:T(8,128)(2,1)}, u32[]{:S(2)}, u32[]{:S(2)}) collective-permute-start(bf16[6,1024,128]{2,1,0:T(8,128)(2,1)S(1)} %constant_dynamic-update-slice_fusion.pair), channel_id=1, source_target_pairs={{0,4},{4,0},{1,5},{5,1},{2,6},{6,2},{3,7},{7,3},{8,12},{12,8},{9,1... | collective-permute-start | bytes 4718600 | tf_op jit(solution)/shard_map/ppermute | solution.py:447
  29.4 10.5 %all-to-all-start = ((bf16[4,13,1024]{2,1,0:T(8,128)(2,1)}), bf16[4,13,1024]{2,1,0:T(8,128)(2,1)S(1)}, u32[]{:S(2)}, u32[]{:S(2)}) async-start(bf16[4,13,1024]{2,1,0:T(8,128)(2,1)} %get-tuple-element.9), calls=%async_computation | async-start | bytes 262144 | tf_op jit(solution)/shard_map/all_to_all | solution.py:443
  73.1 9.6 %copy-start.3 = (f32[13,2]{0,1:T(2,128)S(1)}, f32[13,2]{0,1:T(2,128)}, u32[]{:S(2)}) copy-start(f32[13,2]{0,1:T(2,128)} %param.32) | copy-start | bytes 316
  75.9 25.4 %all-to-all-start.2 = ((bf16[128,2,256]{2,1,0:T(2,128)(2,1)}), bf16[128,2,256]{2,1,0:T(2,128)(2,1)S(1)}, u32[]{:S(2)}, u32[]{:S(2)}) async-start(bf16[128,2,256]{2,1,0:T(2,128)(2,1)} %expert.1), calls=%async_computation.2 | async-start | bytes 262144 | tf_op jit(solution)/shard_map/all_to_all | solution.py:454

commit v8 on v6

--- a/solution.py
+++ b/solution.py
@@ -21,8 +21,8 @@
 
 
 def attention_kernel(
-    lengths,
-    bias,
+    lengths_hbm,
+    bias_hbm,
     tokens_hbm,
     gain_hbm,
     wq_hbm,
@@ -38,6 +38,8 @@
     wd,
     out,
     pack,
+    lengths,
+    bias,
     tokens,
     gain,
     wq,
@@ -71,10 +73,12 @@
                 (wf_hbm, wf),
                 (cumul_hbm, cumul),
                 (wo_hbm, wo),
+                (lengths_hbm, lengths),
+                (bias_hbm, bias),
             ]
         )
     ]
-    for copy in small_copies[:7]:
+    for copy in small_copies[:7] + small_copies[8:]:
         copy.start()
     span = keys.shape[1]
     total_rows = seq_rows * HD
@@ -105,7 +109,7 @@
         )
         for j in range(wd.shape[1] // units)
     ]
-    for copy in key_copies + value_copies + small_copies[7:] + pack_loads:
+    for copy in key_copies + value_copies + small_copies[7:8]:
         copy.start()
 
     f32 = jnp.float32
@@ -113,7 +117,7 @@
     nt = (((1,), (1,)), ((), ()))
     token_rows[...] = jnp.zeros_like(token_rows)
     cum_rows[...] = jnp.zeros_like(cum_rows)
-    for copy in small_copies[:6]:
+    for copy in small_copies[:6] + small_copies[8:]:
         copy.wait()
     token_rows[0:seq_rows, :] = tokens[...].astype(f32)
 
@@ -129,7 +133,7 @@
     wf_rows = wf[...].astype(f32)
     forget = []
     for g in range(2):
-        raw = jnp.sum(normed_f * wf_rows[g : g + 1, :], axis=-1, keepdims=True) + bias[g]
+        raw = jnp.sum(normed_f * wf_rows[g : g + 1, :], axis=-1, keepdims=True) + bias[:, g : g + 1]
         forget.append(jnp.minimum(raw, 0.0) - jnp.log1p(jnp.exp(-jnp.abs(raw))))
     log_forget = jnp.concatenate(forget, axis=0)
 
@@ -159,14 +163,17 @@
         key_copies[i].wait()
         scores = scores + jnp.dot(left, key_buf[r : r + size, :], preferred_element_type=f32)
 
+    for copy in pack_loads:
+        copy.start()
     small_copies[6].wait()
     for b in range(seq_rows):
         pair = cumul[b]
         cum_rows[b : b + 1, :] = pair[0:1, :]
         cum_rows[pad + b : pad + b + 1, :] = pair[1:2, :]
-    limit = jnp.zeros((2 * pad, 1), jnp.int32)
-    for b in range(seq_rows):
-        limit = jnp.where(row_seq == b, lengths[b], limit)
+    seq_lane = lax.broadcasted_iota(jnp.int32, (1, seq_rows), 1)
+    counts = lengths[...].astype(f32)
+    limit = jnp.sum(jnp.where(seq_lane == row_seq, counts, 0.0), axis=-1, keepdims=True)
+    limit = limit.astype(jnp.int32)
     position = lax.broadcasted_iota(jnp.int32, (1, span), 1)
     cum = cum_rows[...]
     last = jnp.sum(jnp.where(position == limit - 1, cum, 0.0), axis=-1, keepdims=True)
@@ -226,10 +233,9 @@
     seq_rows, width = tokens.shape
     span = keys.shape[3]
     pad = 16
-    chunk = 4 * HD
+    chunk = 2 * HD * -(-seq_rows // 2)
     count = -(-seq_rows * HD // chunk)
     vmem = pl.BlockSpec(memory_space=pltpu.VMEM)
-    smem = pl.BlockSpec(memory_space=pltpu.SMEM)
     hbm = pl.BlockSpec(memory_space=pl.ANY)
     kernel = functools.partial(attention_kernel, seq_rows=seq_rows, pad=pad, chunk=chunk)
     return pl.pallas_call(
@@ -238,9 +244,11 @@
             pltpu.VMEM((blocks, seq_rows, width), jnp.bfloat16),
             pltpu.VMEM((3,) + wg.shape, jnp.bfloat16),
         ),
-        in_specs=[smem, smem] + [hbm] * 13,
+        in_specs=[hbm] * 15,
         out_specs=(vmem, vmem),
         scratch_shapes=[
+            pltpu.VMEM((1, seq_rows), jnp.int32),
+            pltpu.VMEM((1, bias.shape[0]), jnp.float32),
             pltpu.VMEM(tokens.shape, jnp.bfloat16),
             pltpu.VMEM((1, width), jnp.float32),
             pltpu.VMEM(wq.shape, jnp.bfloat16),
@@ -253,15 +261,15 @@
             pltpu.VMEM((seq_rows * HD, span), jnp.bfloat16),
             pltpu.VMEM((2 * pad, span), jnp.float32),
             pltpu.VMEM((pad, width), jnp.float32),
-            pltpu.SemaphoreType.DMA((8,)),
+            pltpu.SemaphoreType.DMA((10,)),
             pltpu.SemaphoreType.DMA((count,)),
             pltpu.SemaphoreType.DMA((count,)),
             pltpu.SemaphoreType.DMA((2 + width // wg.shape[1],)),
         ],
         name="attention",
     )(
-        lengths,
-        bias,
+        lengths.reshape(1, seq_rows),
+        bias.reshape(1, -1),
         tokens,
         gain.reshape(1, width),
         wq,

time: 97.5 us -> 95.8 us (0.983)
  Pallas kernels: 9.01 us -> 7.43 us
    pallas_call x1, Pallas kernels: 6.19 us -> 4.61 us  [attention_call(): pl.pallas_call(kernel, out_shape=(pltpu.VMEM((blocks, seq_rows, width), j...]
where the time goes in v8:
time: 95.8 us; the launch traced here: 95.4 us
  blocking collectives  34.3 us (36%)
  waiting for transfers between devices  29.2 us (30%)
  starting transfers between devices  20.5 us (21%)
  Pallas kernels  7.43 us (8%)
  other arithmetic  2.14 us (2%)
  matrix products  1.02 us (1%)
    all_to_all x1, blocking collectives, body(): lax.all_to_all(outgoing, EXPERT_AXES, split_axis=0, concat_axis=0, tiled=...  34.3 us
    all_to_all x1, waiting for transfers between devices, body(): lax.all_to_all(part, EXPERT_AXES + ('tp',), split_axis=0, concat_axis=0,...  18.4 us
    ppermute x1, waiting for transfers between devices, body(): side_pack = lax.ppermute(own_pack, 'xl', swap)  10.8 us
    all_to_all x1, starting transfers between devices, body(): lax.all_to_all(part, EXPERT_AXES + ('tp',), split_axis=0, concat_axis=0,...  8.81 us
    pallas_call x1, Pallas kernels, attention_call(): pl.pallas_call(kernel, out_shape=(pltpu.VMEM((blocks, seq_rows, width), j...  4.61 us
    all_to_all x1, starting transfers between devices, body(): blocks = lax.all_to_all(partial, 'tp', 0, 0, tiled=True)  4.47 us
    ppermute x1, starting transfers between devices, body(): side_pack = lax.ppermute(own_pack, 'xl', swap)  3.4 us
    pallas_call x1, Pallas kernels, expert_call(): pl.pallas_call(functools.partial(expert_kernel, blocks=blocks), out_shape...  2.54 us
  transfers between devices with their start and end apart: 5, of which 2 were waited for; matrix products, arithmetic and copies ran while one was open for 3% of the time, Pallas kernels for 0%

profile of v8, /device:TPU:32, one launch (start us, length us, event | category | flops | bytes accessed | tf_op | source)
XLA Modules:
  0.0 95.4 jit_solution(15142310776447322486)
XLA Ops:
  0.0 4.6 %attention.1 = (bf16[4,13,1024]{2,1,0:T(8,128)(2,1)}, bf16[3,1024,128]{2,1,0:T(8,128)(2,1)S(1)}) custom-call(s32[1,13]{1,0:T(1,128)} %bitcast.34, f32[1,2]{1,0:T(1,128)} %bitcast.35, bf16[13,1024]{1,0:T(8,128)(2,1)} %tokens.1, f32[1,1024]{1,0:T(1,128)} %bitcast.32, bf16[1024,128]{1,0:T(8,128)(2,1)} %wq_hbm.1, bf16[64,1024]{1,0:T(8,128)(2,1)} %bitcast.29, ...), custom_call_target="tpu_custom_call" | custom-call | tf_op jit(solution)/shard_map/attention/pallas_call | solution.py:241
  4.6 3.4 %collective-permute-start.1 = (bf16[3,1024,128]{2,1,0:T(8,128)(2,1)S(1)}, bf16[3,1024,128]{2,1,0:T(8,128)(2,1)}, u32[]{:S(2)}, u32[]{:S(2)}) collective-permute-start(bf16[3,1024,128]{2,1,0:T(8,128)(2,1)S(1)} %get-tuple-element.12), channel_id=1, source_target_pairs={{0,8},{8,0},{1,9},{9,1},{2,10},{10,2},{3,11},{11,3},{4,12},{12,4},... | collective-permute-start | bytes 2359304 | tf_op jit(solution)/shard_map/ppermute | solution.py:456
  8.0 1.9 %collective-permute-start = (bf16[3,1024,128]{2,1,0:T(8,128)(2,1)S(1)}, bf16[3,1024,128]{2,1,0:T(8,128)(2,1)}, u32[]{:S(2)}, u32[]{:S(2)}) collective-permute-start(bf16[3,1024,128]{2,1,0:T(8,128)(2,1)S(1)} %get-tuple-element.12), channel_id=1, source_target_pairs={{0,4},{4,0},{1,5},{5,1},{2,6},{6,2},{3,7},{7,3},{8,12},{12,8},{9,1... | collective-permute-start | bytes 2359304 | tf_op jit(solution)/shard_map/ppermute | solution.py:457
  10.0 4.5 %all-to-all-start = ((bf16[4,13,1024]{2,1,0:T(8,128)(2,1)}), bf16[4,13,1024]{2,1,0:T(8,128)(2,1)S(1)}, u32[]{:S(2)}, u32[]{:S(2)}) async-start(bf16[4,13,1024]{2,1,0:T(8,128)(2,1)} %get-tuple-element.9), calls=%async_computation | async-start | bytes 262144 | tf_op jit(solution)/shard_map/all_to_all | solution.py:454
  14.4 0.1 copy.32
  14.5 0.1 fusion.4
  14.7 0.2 fusion.5
  14.9 0.1 copy.35
  15.0 0.1 eq.43
  15.1 10.8 %collective-permute-done.1 = bf16[3,1024,128]{2,1,0:T(8,128)(2,1)} collective-permute-done((bf16[3,1024,128]{2,1,0:T(8,128)(2,1)S(1)}, bf16[3,1024,128]{2,1,0:T(8,128)(2,1)}, u32[]{:S(2)}, u32[]{:S(2)}) %collective-permute-start.1) | collective-permute-done | bytes 786464 | tf_op jit(solution)/shard_map/ppermute | solution.py:456
  25.9 1.9 %collective-permute-start.2 = (bf16[3,1024,128]{2,1,0:T(8,128)(2,1)}, bf16[3,1024,128]{2,1,0:T(8,128)(2,1)}, u32[]{:S(2)}, u32[]{:S(2)}) collective-permute-start(bf16[3,1024,128]{2,1,0:T(8,128)(2,1)} %collective-permute-done.1), channel_id=1, source_target_pairs={{0,4},{4,0},{1,5},{5,1},{2,6},{6,2},{3,7},{7,3},{8,12},{12,8},{9,1... | collective-permute-start | bytes 2359304 | tf_op jit(solution)/shard_map/ppermute | solution.py:458
  27.8 0.1 and_convert_fusion.place
  28.0 0.3 outgoing.1
  28.3 34.3 %all_to_all.15 = bf16[32,2,1024]{2,1,0:T(2,128)(2,1)S(1)} all-to-all(bf16[32,2,1024]{2,1,0:T(2,128)(2,1)S(1)} %get-tuple-element.11), channel_id=1, replica_groups=mesh['z'=16,'xh'=2,'xl'=2,'core'=2,'tp'=4] {'z','xh'}, dimensions={0} | all-to-all | bytes 262144 | tf_op jit(solution)/shard_map/all_to_all | solution.py:463
  62.6 1.6 %pad_maximum_fusion.trio = bf16[9,1024,128]{2,1,0:T(8,128)(2,1)S(1)} fusion(bf16[3,1024,128]{2,1,0:T(8,128)(2,1)} %collective-permute-done.1, bf16[3,1024,128]{2,1,0:T(8,128)(2,1)} %collective-permute-done, bf16[3,1024,128]{2,1,0:T(8,128)(2,1)S(1)} %get-tuple-element.12), kind=kLoop, calls=%fused_computation | loop fusion | flops 2359296 | bytes 4718592 | tf_op jit(solution)/shard_map/concatenate | solution.py:459
  64.3 2.5 %expert.1 = bf16[128,2,256]{2,1,0:T(2,128)(2,1)} custom-call(bf16[64,1024]{1,0:T(8,128)(2,1)S(1)} %reshape.50.rows, bf16[9,1024,128]{2,1,0:T(8,128)(2,1)S(1)} %pad_maximum_fusion.trio, bf16[3,1024,128]{2,1,0:T(8,128)(2,1)} %collective-permute-done.2.far), custom_call_target="tpu_custom_call" | custom-call | tf_op jit(solution)/shard_map/expert/pallas_call | solution.py:343
  66.8 8.8 %all-to-all-start.2 = ((bf16[128,2,256]{2,1,0:T(2,128)(2,1)}), bf16[128,2,256]{2,1,0:T(2,128)(2,1)S(1)}, u32[]{:S(2)}, u32[]{:S(2)}) async-start(bf16[128,2,256]{2,1,0:T(2,128)(2,1)} %expert.1), calls=%async_computation.2 | async-start | bytes 262144 | tf_op jit(solution)/shard_map/all_to_all | solution.py:466
  75.7 0.1 copy.36
  75.8 0.1 select_reduce_fusion
  75.9 0.1 copy.37
  76.0 0.1 and_select_fusion
  76.1 18.4 %all-to-all-done.2 = bf16[128,2,256]{2,1,0:T(2,128)(2,1)S(1)} async-done(((bf16[128,2,256]{2,1,0:T(2,128)(2,1)}), bf16[128,2,256]{2,1,0:T(2,128)(2,1)S(1)}, u32[]{:S(2)}, u32[]{:S(2)}) %all-to-all-start.2) | async-done | bytes 131104 | tf_op jit(solution)/shard_map/all_to_all | solution.py:466
  94.5 0.1 convert_reduce_fusion
  94.6 0.8 fusion.1
  (18 shorter events, 0.2 us)
Async XLA Ops:
  0.0 14.4 %copy-start.2 = (s32[13,2]{0,1:T(2,128)S(1)}, s32[13,2]{0,1:T(2,128)}, u32[]{:S(2)}) copy-start(s32[13,2]{0,1:T(2,128)} %param.31) | copy-start | bytes 316
  0.0 27.9 %copy-start = (bf16[13,1024]{1,0:T(8,128)(2,1)S(1)}, bf16[13,1024]{1,0:T(8,128)(2,1)}, u32[]{:S(2)}) copy-start(bf16[13,1024]{1,0:T(8,128)(2,1)} %tokens.1) | copy-start | bytes 79876
  0.0 27.9 %copy-start.1 = (f32[1024]{0:T(1024)S(1)}, f32[1024]{0:T(1024)}, u32[]{:S(2)}) copy-start(f32[1024]{0:T(1024)} %param.30) | copy-start | bytes 12292
  4.6 21.3 %collective-permute-start.1 = (bf16[3,1024,128]{2,1,0:T(8,128)(2,1)S(1)}, bf16[3,1024,128]{2,1,0:T(8,128)(2,1)}, u32[]{:S(2)}, u32[]{:S(2)}) collective-permute-start(bf16[3,1024,128]{2,1,0:T(8,128)(2,1)S(1)} %get-tuple-element.12), channel_id=1, source_target_pairs={{0,8},{8,0},{1,9},{9,1},{2,10},{10,2},{3,11},{11,3},{4,12},{12,4},... | collective-permute-start | bytes 2359304 | tf_op jit(solution)/shard_map/ppermute | solution.py:456
  8.0 54.6 %collective-permute-start = (bf16[3,1024,128]{2,1,0:T(8,128)(2,1)S(1)}, bf16[3,1024,128]{2,1,0:T(8,128)(2,1)}, u32[]{:S(2)}, u32[]{:S(2)}) collective-permute-start(bf16[3,1024,128]{2,1,0:T(8,128)(2,1)S(1)} %get-tuple-element.12), channel_id=1, source_target_pairs={{0,4},{4,0},{1,5},{5,1},{2,6},{6,2},{3,7},{7,3},{8,12},{12,8},{9,1... | collective-permute-start | bytes 2359304 | tf_op jit(solution)/shard_map/ppermute | solution.py:457
  10.0 18.0 %all-to-all-start = ((bf16[4,13,1024]{2,1,0:T(8,128)(2,1)}), bf16[4,13,1024]{2,1,0:T(8,128)(2,1)S(1)}, u32[]{:S(2)}, u32[]{:S(2)}) async-start(bf16[4,13,1024]{2,1,0:T(8,128)(2,1)} %get-tuple-element.9), calls=%async_computation | async-start | bytes 262144 | tf_op jit(solution)/shard_map/all_to_all | solution.py:454
  25.9 38.4 %collective-permute-start.2 = (bf16[3,1024,128]{2,1,0:T(8,128)(2,1)}, bf16[3,1024,128]{2,1,0:T(8,128)(2,1)}, u32[]{:S(2)}, u32[]{:S(2)}) collective-permute-start(bf16[3,1024,128]{2,1,0:T(8,128)(2,1)} %collective-permute-done.1), channel_id=1, source_target_pairs={{0,4},{4,0},{1,5},{5,1},{2,6},{6,2},{3,7},{7,3},{8,12},{12,8},{9,1... | collective-permute-start | bytes 2359304 | tf_op jit(solution)/shard_map/ppermute | solution.py:458
  64.3 11.4 %copy-start.3 = (f32[13,2]{0,1:T(2,128)S(1)}, f32[13,2]{0,1:T(2,128)}, u32[]{:S(2)}) copy-start(f32[13,2]{0,1:T(2,128)} %param.32) | copy-start | bytes 316
  66.8 27.6 %all-to-all-start.2 = ((bf16[128,2,256]{2,1,0:T(2,128)(2,1)}), bf16[128,2,256]{2,1,0:T(2,128)(2,1)S(1)}, u32[]{:S(2)}, u32[]{:S(2)}) async-start(bf16[128,2,256]{2,1,0:T(2,128)(2,1)} %expert.1), calls=%async_computation.2 | async-start | bytes 262144 | tf_op jit(solution)/shard_map/all_to_all | solution.py:466
